TPU v7x, 32 devices: a whole 2x2x4 slice. The times are simulated.
32 devices in a mesh: grp: 2 (over y), sp: 4 (over z), tp: 4 (over x, core).
Axes of the slice: x: 2, y: 2, z: 4, core: 2. Of those that a mesh axis runs over, the one named last changes fastest.
Arguments:
- stream: bfloat16 [2048, 2048], P(('grp', 'sp')), parts along dimension 0, may hold values from -6 to 6
- doc_ids: int32 [2048], P(('grp', 'sp')), parts along dimension 0, may hold values from 0 to 1, never falling along the last dimension, each value on 1 to 768 neighbouring positions
- norm_gain: float32 [2, 2048], replicated, may hold values from 0.1 to 1.9
- query_weight: bfloat16 [2, 2048, 1024], P(None, 'sp', 'tp'), may hold values from -0.125 to 0.125
- key_weight: bfloat16 [2, 2048, 1024], P(None, 'sp', 'tp'), may hold values from -0.125 to 0.125
- value_weight: bfloat16 [2, 2048, 1024], P(None, 'sp', 'tp'), may hold values from -0.125 to 0.125
- out_weight: bfloat16 [2, 1024, 2048], P(None, 'sp', 'tp'), may hold values from -0.75 to 0.75
- query_gain: float32 [2, 64], replicated, may hold values from 0.1 to 1.9
- key_gain: float32 [2, 64], replicated, may hold values from 0.1 to 1.9
- rel_bias: float32 [16, 513], P('tp'), may hold values from -4 to 250
Outputs:
- encoded: bfloat16 [2048, 2048], P(('grp', 'sp')), parts along dimension 0
There are 2 independent parts, one for each index of `grp`. A program takes and returns all parts, laid end to end along the dimension named above; an argument that names none is the same for every part. Nothing has to cross between parts.
Inputs may be any that keep to these rules, and one draw needn't show every extreme that they name: doc_ids never fall along the sequence; each document has at most 768 positions.
All inputs are finite; a program needn't handle non-finite values.
Results may differ from a plain program's by a relative error of at most 0.011.
Values may be sent and summed in bfloat16 or wider, within the bound.
No kernel may reach another device: no remote copies, remote signals or barrier semaphores. Data moves between devices by JAX's collectives and lax.ppermute only.
A program may use at most 64 MiB of HBM per device.

v0:
```python
import jax
import jax.numpy as jnp
from jax import lax
from jax.sharding import PartitionSpec as P

SEG = 64
LEFT = 8
MAXREL = 256
LAYERS = 2


epsilon = 1e-06


def shifted(value, axis, steps):
    count = lax.axis_size(axis)
    initial, last = (max(0, -steps), min(count, count - steps))
    return lax.ppermute(value, axis, [(source, source + steps) for source in range(initial, last)])


def row_norm(values, gain):
    return values * lax.rsqrt(jnp.mean(values * values, axis=-1, keepdims=True) + epsilon) * gain


def bias_table(rel_bias):
    heads_here = rel_bias.shape[0]
    reach = LEFT * SEG
    width = (LEFT + 1) * SEG
    highest = reach + SEG - 1
    reversed_bias = rel_bias[:, ::-1]
    upper_fill = jnp.broadcast_to(rel_bias[:, -1:], (heads_here, highest - MAXREL))
    flat_row = jnp.concatenate([upper_fill, reversed_bias[:, : MAXREL + SEG]], axis=1)
    lines = [
        flat_row[:, SEG - 1 - position : SEG - 1 - position + width] for position in range(SEG)
    ]
    return jnp.stack(lines, axis=1)


def attend(query, ext_keys, ext_values, ext_docs, own_docs, offset, table):
    rows, heads_here, head_size = query.shape
    count = rows // SEG
    width = (LEFT + 1) * SEG
    blocks = query.reshape(count, SEG, heads_here, head_size)
    key_blocks = ext_keys.reshape(count + LEFT, SEG, heads_here, head_size)
    value_blocks = ext_values.reshape(count + LEFT, SEG, heads_here, head_size)
    doc_blocks = ext_docs.reshape(count + LEFT, SEG)
    score_parts = [
        jnp.einsum(
            "nqhd,nkhd->nhqk",
            blocks,
            key_blocks[earlier : earlier + count],
            preferred_element_type=jnp.float32,
        )
        for earlier in range(LEFT + 1)
    ]
    scores = jnp.concatenate(score_parts, axis=-1)
    scores = scores * head_size ** (-0.5) + table[None]
    doc_band = jnp.concatenate(
        [doc_blocks[earlier : earlier + count] for earlier in range(LEFT + 1)], axis=1
    )
    key_pos = (
        offset
        + SEG * jnp.arange(count, dtype=jnp.int32)[:, None]
        - LEFT * SEG
        + jnp.arange(width, dtype=jnp.int32)[None, :]
    )
    allowed = (key_pos >= 0)[:, None, None, :] & (
        doc_band[:, None, None, :] == own_docs.reshape(count, SEG)[:, None, :, None]
    )
    scores = jnp.where(allowed, scores, -1e30)
    peak = jnp.max(scores, axis=-1, keepdims=True)
    expo = jnp.exp(scores - peak)
    weights = (expo / jnp.sum(expo, axis=-1, keepdims=True)).astype(jnp.bfloat16)
    mixed = jnp.zeros((count, SEG, heads_here, head_size), jnp.float32)
    for earlier in range(LEFT + 1):
        part_weights = weights[..., earlier * SEG : (earlier + 1) * SEG]
        mixed = mixed + jnp.einsum(
            "nhqk,nkhd->nqhd",
            part_weights,
            value_blocks[earlier : earlier + count],
            preferred_element_type=jnp.float32,
        )
    return mixed.astype(jnp.bfloat16).reshape(rows, heads_here * head_size)


def on_device(
    stream,
    doc_ids,
    norm_gain,
    query_weight,
    key_weight,
    value_weight,
    out_weight,
    query_gain,
    key_gain,
    rel_bias,
):
    rows = stream.shape[0]
    heads_here = rel_bias.shape[0]
    head_size = query_gain.shape[1]
    local_width = heads_here * head_size
    reach = LEFT * SEG
    depth = -(-reach // rows)
    offset = lax.axis_index("sp") * rows
    col_width = out_weight.shape[2]
    col_start = lax.axis_index("tp") * col_width
    table = bias_table(rel_bias)
    x = stream
    for layer in range(LAYERS):
        widened = x.astype(jnp.float32)
        normed = row_norm(widened, norm_gain[layer]).astype(jnp.bfloat16)
        own_cols = normed
        q_raw = jnp.dot(
            own_cols,
            lax.all_gather(query_weight[layer], "sp", axis=0, tiled=True),
            preferred_element_type=jnp.float32,
        )
        k_raw = jnp.dot(
            normed,
            lax.all_gather(key_weight[layer], "sp", axis=0, tiled=True),
            preferred_element_type=jnp.float32,
        )
        v_raw = jnp.dot(
            normed,
            lax.all_gather(value_weight[layer], "sp", axis=0, tiled=True),
            preferred_element_type=jnp.float32,
        )
        query = row_norm(q_raw.reshape(rows, heads_here, head_size), query_gain[layer]).astype(
            jnp.bfloat16
        )
        keys = row_norm(
            k_raw.reshape(normed.shape[0], heads_here, head_size), key_gain[layer]
        ).astype(jnp.bfloat16)
        values = v_raw.astype(jnp.bfloat16)
        flat_keys = keys.reshape(rows, local_width)
        tail = (flat_keys, values, doc_ids)
        received = [
            shifted((tail[0], tail[1], tail[2]), "sp", distance_back)
            for distance_back in range(depth, 0, -1)
        ]
        ext_keys = jnp.concatenate([item[0] for item in received] + [flat_keys], axis=0)
        ext_values = jnp.concatenate([item[1] for item in received] + [values], axis=0)
        ext_docs = jnp.concatenate([item[2] for item in received] + [doc_ids], axis=0)
        ext_keys = ext_keys.reshape(reach + rows, heads_here, head_size)
        ext_values = ext_values.reshape(reach + rows, heads_here, head_size)
        attended = attend(query, ext_keys, ext_values, ext_docs, doc_ids, offset, table)
        all_heads = lax.all_gather(attended, "tp", axis=1, tiled=True)
        projected = jnp.dot(
            all_heads,
            lax.all_gather(out_weight[layer], "sp", axis=0, tiled=True),
            preferred_element_type=jnp.float32,
        )
        own_cols = lax.dynamic_slice_in_dim(widened, col_start, col_width, 1)
        new_cols = (own_cols + projected).astype(jnp.bfloat16)
        x = lax.all_gather(new_cols, "tp", axis=1, tiled=True)
    return x


def solution(mesh):
    placed = (
        P(("grp", "sp"), None),
        P(("grp", "sp")),
        P(),
        P(None, "sp", "tp"),
        P(None, "sp", "tp"),
        P(None, "sp", "tp"),
        P(None, "sp", "tp"),
        P(),
        P(),
        P("tp", None),
    )
    return jax.shard_map(
        on_device, mesh=mesh, in_specs=placed, out_specs=P(("grp", "sp"), None), check_vma=False
    )
```

profile of v0, /device:TPU:25, one launch (start us, length us, event | category | flops | bytes accessed | tf_op | source)
XLA Modules:
  0.0 336.7 jit_solution(15381538330978030332)
XLA Ops:
  6.5 2.0 fusion.257
  8.6 2.0 fusion.256
  11.6 1.3 collective-permute-start.1
  12.9 1.3 collective-permute-start.2
  21.6 1.6 convert_element_type.52
  23.8 12.5 %all-gather.27.cloned.1.call-done = bf16[1,2048,256]{2,1,0:T(8,128)(2,1)} async-done(((bf16[1,512,256]{2,1,0:T(8,128)(2,1)}), bf16[1,2048,256]{2,1,0:T(8,128)(2,1)}) %all-gather.27.cloned.1.call-update) | async-done | bytes 1048592 | tf_op jit(solution)/shard_map/all_gather | solution.py:120
  36.2 1.9 bitcast_reduce_fusion.2
  38.3 1.3 collective-permute-start.3
  39.6 1.3 collective-permute-start.4
  41.0 28.2 %all-gather.23.cloned.1.call-done = bf16[1,2048,256]{2,1,0:T(8,128)(2,1)} async-done(((bf16[1,512,256]{2,1,0:T(8,128)(2,1)}), bf16[1,2048,256]{2,1,0:T(8,128)(2,1)}) %all-gather.23.cloned.1.call-update) | async-done | bytes 1048592 | tf_op jit(solution)/shard_map/all_gather | solution.py:125
  69.3 1.7 convolution_convert_fusion.1
  71.0 1.3 collective-permute-start.5
  72.3 1.5 collective-permute-start
  74.6 26.2 %all-gather.25.cloned.1.call-done = bf16[1,2048,256]{2,1,0:T(8,128)(2,1)} async-done(((bf16[1,512,256]{2,1,0:T(8,128)(2,1)}), bf16[1,2048,256]{2,1,0:T(8,128)(2,1)}) %all-gather.25.cloned.1.call-update) | async-done | bytes 1048592 | tf_op jit(solution)/shard_map/all_gather | solution.py:115
  100.8 1.9 bitcast_reduce_fusion.3
  118.5 3.6 %concatenate.92 = f32[4,4,64,576]{3,2,1,0:T(8,128)S(1)} concatenate(f32[4,4,64,64]{3,2,1,0:T(8,128)} %fusion.114, f32[4,4,64,64]{3,2,1,0:T(8,128)} %fusion.112, f32[4,4,64,64]{3,2,1,0:T(8,128)} %fusion.110, f32[4,4,64,64]{3,2,1,0:T(8,128)} %fusion.108, f32[4,4,64,64]{3,2,1,0:T(8,128)} %fusion.106, f32[4,4,64,64]{3,2,1,0:T(8,128)} %fusion.104, f32[4,4,64,64]{3,2,1,0:T(8,128)} %fusion.102, ...), dimensions={3} | concatenate | bytes 4718592 | tf_op jit(solution)/shard_map/concatenate | solution.py:56
  124.8 1.8 slice.569
  126.6 1.3 fusion.15
  127.8 1.3 fusion.49
  129.2 1.8 slice.670
  133.1 1.8 slice.672
  134.9 1.3 convolution_add_fusion.12
  136.2 1.3 fusion.14
  139.2 8.4 %all_gather.39 = bf16[256,1024]{1,0:T(8,128)(2,1)S(1)} all-gather(bf16[256,256]{1,0:T(8,128)(2,1)S(1)} %reshape.224), channel_id=1, replica_groups=mesh['grp'=2,'sp'=4,'tp'=4] {'tp'}, dimensions={1}, use_global_device_ids=true | all-gather | bytes 655360 | tf_op jit(solution)/shard_map/all_gather | solution.py:147
  147.6 2.5 fusion.16
  153.0 14.5 %all-gather.19.cloned.1.call-done = bf16[256,2048]{1,0:T(8,128)(2,1)} async-done(((bf16[256,512]{1,0:T(8,128)(2,1)}), bf16[256,2048]{1,0:T(8,128)(2,1)}) %all-gather.19.cloned.1.call-update) | async-done | bytes 1048592 | tf_op jit(solution)/shard_map/all_gather | solution.py:155
  167.5 1.5 multiply_reduce_fusion
  169.0 25.9 %all-gather.35.cloned.1.call-done = bf16[1,2048,256]{2,1,0:T(8,128)(2,1)} async-done(((bf16[1,512,256]{2,1,0:T(8,128)(2,1)}), bf16[1,2048,256]{2,1,0:T(8,128)(2,1)}) %all-gather.35.cloned.1.call-update) | async-done | bytes 1048592 | tf_op jit(solution)/shard_map/all_gather | solution.py:120
  194.9 2.2 bitcast_reduce_fusion
  197.2 1.3 collective-permute-start.7
  198.5 1.3 collective-permute-start.8
  200.0 28.2 %all-gather.31.cloned.1.call-done = bf16[1,2048,256]{2,1,0:T(8,128)(2,1)} async-done(((bf16[1,512,256]{2,1,0:T(8,128)(2,1)}), bf16[1,2048,256]{2,1,0:T(8,128)(2,1)}) %all-gather.31.cloned.1.call-update) | async-done | bytes 1048592 | tf_op jit(solution)/shard_map/all_gather | solution.py:125
  228.2 2.4 convolution_convert_fusion
  230.6 1.3 collective-permute-start.9
  231.9 1.5 collective-permute-start.6
  233.4 1.8 slice.729
  235.2 25.4 %all-gather.33.cloned.1.call-done = bf16[1,2048,256]{2,1,0:T(8,128)(2,1)} async-done(((bf16[1,512,256]{2,1,0:T(8,128)(2,1)}), bf16[1,2048,256]{2,1,0:T(8,128)(2,1)}) %all-gather.33.cloned.1.call-update) | async-done | bytes 1048592 | tf_op jit(solution)/shard_map/all_gather | solution.py:115
  260.7 1.9 bitcast_reduce_fusion.1
  263.3 1.6 convert_element_type.60
  267.2 1.3 pad_maximum_fusion.1
  277.9 3.6 %concatenate.98 = f32[4,4,64,576]{3,2,1,0:T(8,128)S(1)} concatenate(f32[4,4,64,64]{3,2,1,0:T(8,128)} %fusion.87, f32[4,4,64,64]{3,2,1,0:T(8,128)} %fusion.85, f32[4,4,64,64]{3,2,1,0:T(8,128)} %fusion.83, f32[4,4,64,64]{3,2,1,0:T(8,128)} %fusion.81, f32[4,4,64,64]{3,2,1,0:T(8,128)} %fusion.79, f32[4,4,64,64]{3,2,1,0:T(8,128)} %fusion.77, f32[4,4,64,64]{3,2,1,0:T(8,128)} %fusion.75, ...), dimensions={3} | concatenate | bytes 4718592 | tf_op jit(solution)/shard_map/concatenate | solution.py:56
  281.5 2.3 fusion.267
  284.9 1.8 pad_maximum_fusion
  291.8 1.3 fusion.13
  299.3 8.3 %all_gather.45 = bf16[256,1024]{1,0:T(8,128)(2,1)S(1)} all-gather(bf16[256,256]{1,0:T(8,128)(2,1)S(1)} %reshape.226), channel_id=1, replica_groups=mesh['grp'=2,'sp'=4,'tp'=4] {'tp'}, dimensions={1}, use_global_device_ids=true | all-gather | bytes 655360 | tf_op jit(solution)/shard_map/all_gather | solution.py:147
  307.6 2.5 fusion.17
  310.1 17.4 %all-gather.21.cloned.1.call-done = bf16[256,2048]{1,0:T(8,128)(2,1)} async-done(((bf16[256,512]{1,0:T(8,128)(2,1)}), bf16[256,2048]{1,0:T(8,128)(2,1)}) %all-gather.21.cloned.1.call-update) | async-done | bytes 1048592 | tf_op jit(solution)/shard_map/all_gather | solution.py:155
  327.5 2.3 copy.233
  (259 shorter events, 59.8 us)
Async XLA Ops:
  6.5 4.1 %copy-start.12 = (bf16[2,512,256]{2,1,0:T(8,128)(2,1)S(1)}, bf16[2,512,256]{2,1,0:T(8,128)(2,1)}, u32[]{:S(2)}) copy-start(bf16[2,512,256]{2,1,0:T(8,128)(2,1)} %param.13) | copy-start | bytes 1572868
  6.5 5.0 %copy-start.17 = (s32[256]{0:T(256)S(1)}, s32[256]{0:T(256)}, u32[]{:S(2)}) copy-start(s32[256]{0:T(256)} %param.11) | copy-start | bytes 3076
  6.5 7.6 %copy-start.13 = (bf16[2,256,512]{2,1,0:T(8,128)(2,1)S(1)}, bf16[2,256,512]{2,1,0:T(8,128)(2,1)}, u32[]{:S(2)}) copy-start(bf16[2,256,512]{2,1,0:T(8,128)(2,1)} %param.16) | copy-start | bytes 1572868
  6.5 29.7 %all-gather.27.cloned.1.call-start = ((), (), s32[]{:S(2)}) async-start(), calls=%async_computation.4 | async-start | bytes 1310720 | tf_op jit(solution)/shard_map/all_gather | solution.py:120
  8.5 6.6 %copy-start.16 = (f32[4,513]{1,0:T(4,128)S(1)}, f32[4,513]{1,0:T(4,128)}, u32[]{:S(2)}) copy-start(f32[4,513]{1,0:T(4,128)} %param.19) | copy-start | bytes 24628
  8.5 6.8 %copy-start.15 = (f32[2,2048]{1,0:T(2,128)S(1)}, f32[2,2048]{1,0:T(2,128)}, u32[]{:S(2)}) copy-start(f32[2,2048]{1,0:T(2,128)} %param.12) | copy-start | bytes 49156
  8.5 6.8 %copy-start.3 = (bf16[256,2048]{1,0:T(8,128)(2,1)S(1)}, bf16[256,2048]{1,0:T(8,128)(2,1)}, u32[]{:S(2)}) copy-start(bf16[256,2048]{1,0:T(8,128)(2,1)} %param.10) | copy-start | bytes 3145732
  8.5 60.7 %all-gather.23.cloned.1.call-start = ((), (), s32[]{:S(2)}) async-start(), calls=%async_computation.2 | async-start | bytes 1310720 | tf_op jit(solution)/shard_map/all_gather | solution.py:125
  10.5 5.1 %copy-start.18 = (f32[2,64]{1,0:T(2,128)S(1)}, f32[2,64]{1,0:T(2,128)}, u32[]{:S(2)}) copy-start(f32[2,64]{1,0:T(2,128)} %param.17) | copy-start | bytes 1540
  10.5 5.1 %copy-start.19 = (f32[2,64]{1,0:T(2,128)S(1)}, f32[2,64]{1,0:T(2,128)}, u32[]{:S(2)}) copy-start(f32[2,64]{1,0:T(2,128)} %param.18) | copy-start | bytes 1540
  10.6 90.3 %all-gather.25.cloned.1.call-start = ((), (), s32[]{:S(2)}) async-start(), calls=%async_computation.3 | async-start | bytes 1310720 | tf_op jit(solution)/shard_map/all_gather | solution.py:115
  11.5 136.1 %all-gather.29.cloned.1.call-start = ((), (), s32[]{:S(2)}) async-start(), calls=%async_computation.5 | async-start | bytes 1310720 | tf_op jit(solution)/shard_map/all_gather | solution.py:150
  11.6 11.7 %collective-permute-start.1 = (s32[256]{0:T(256)S(1)}, s32[256]{0:T(256)S(1)}, u32[]{:S(2)}, u32[]{:S(2)}) collective-permute-start(s32[256]{0:T(256)S(1)} %copy-done.17), channel_id=1, source_target_pairs={{0,8},{4,12},{1,9},{5,13},{2,10},{6,14},{3,11},{7,15},{16,24},{20,... | collective-permute-start | bytes 3080 | tf_op jit(solution)/shard_map/ppermute | solution.py:18
  12.9 10.5 %collective-permute-start.2 = (s32[256]{0:T(256)S(1)}, s32[256]{0:T(256)S(1)}, u32[]{:S(2)}, u32[]{:S(2)}) collective-permute-start(s32[256]{0:T(256)S(1)} %copy-done.17), channel_id=1, source_target_pairs={{0,4},{4,8},{8,12},{1,5},{5,9},{9,13},{2,6},{6,10},{10,14},{3,7},{... | collective-permute-start | bytes 3080 | tf_op jit(solution)/shard_map/ppermute | solution.py:18
  15.0 152.5 %all-gather.19.cloned.1.call-start = ((), (), s32[]{:S(2)}) async-start(), calls=%async_computation | async-start | bytes 1310720 | tf_op jit(solution)/shard_map/all_gather | solution.py:155
  23.8 98.3 %copy-start.5 = (pred[4,64,576]{2,1,0:T(8,128)(4,1)}, pred[4,64,576]{2,1,0:T(8,128)(4,1)S(1)}, u32[]{:S(2)}) copy-start(pred[4,64,576]{2,1,0:T(8,128)(4,1)S(1)} %compare_and_fusion) | copy-start | bytes 442372
  38.3 66.3 %collective-permute-start.3 = (bf16[256,256]{0,1:T(8,128)(2,1)S(1)}, bf16[256,256]{0,1:T(8,128)(2,1)S(1)}, u32[]{:S(2)}, u32[]{:S(2)}) collective-permute-start(bf16[256,256]{0,1:T(8,128)(2,1)S(1)} %fusion.61), channel_id=1, source_target_pairs={{0,8},{4,12},{1,9},{5,13},{2,10},{6,14},{3,11},{7,15},{16,24},{20,... | collective-permute-start | bytes 393224 | tf_op jit(solution)/shard_map/ppermute | solution.py:18
  39.6 66.2 %collective-permute-start.4 = (bf16[256,256]{0,1:T(8,128)(2,1)S(1)}, bf16[256,256]{0,1:T(8,128)(2,1)S(1)}, u32[]{:S(2)}, u32[]{:S(2)}) collective-permute-start(bf16[256,256]{0,1:T(8,128)(2,1)S(1)} %fusion.61), channel_id=1, source_target_pairs={{0,4},{4,8},{8,12},{1,5},{5,9},{9,13},{2,6},{6,10},{10,14},{3,7},{... | collective-permute-start | bytes 393224 | tf_op jit(solution)/shard_map/ppermute | solution.py:18
  71.0 43.4 %collective-permute-start.5 = (bf16[256,256]{1,0:T(8,128)(2,1)S(1)}, bf16[256,256]{1,0:T(8,128)(2,1)S(1)}, u32[]{:S(2)}, u32[]{:S(2)}) collective-permute-start(bf16[256,256]{1,0:T(8,128)(2,1)S(1)} %convolution_convert_fusion.1), channel_id=1, source_target_pairs={{0,4},{4,8},{8,12},{1,5},{5,9},{9,13},{2,6},{6,10},{10,14},{3,7},{... | collective-permute-start | bytes 393224 | tf_op jit(solution)/shard_map/ppermute | solution.py:18
  72.3 42.1 %collective-permute-start = (bf16[256,256]{1,0:T(8,128)(2,1)S(1)}, bf16[256,256]{1,0:T(8,128)(2,1)S(1)}, u32[]{:S(2)}, u32[]{:S(2)}) collective-permute-start(bf16[256,256]{1,0:T(8,128)(2,1)S(1)} %convolution_convert_fusion.1), channel_id=1, source_target_pairs={{0,8},{4,12},{1,9},{5,13},{2,10},{6,14},{3,11},{7,15},{16,24},{20,... | collective-permute-start | bytes 393224 | tf_op jit(solution)/shard_map/ppermute | solution.py:18
  114.4 3.2 copy-start.11
  114.4 3.2 copy-start.14
  123.1 1.0 copy-start.9
  123.1 1.3 copy-start.10
  137.5 1.0 copy-start.8
  150.1 44.8 %all-gather.35.cloned.1.call-start = ((), (), s32[]{:S(2)}) async-start(), calls=%async_computation.8 | async-start | bytes 1310720 | tf_op jit(solution)/shard_map/all_gather | solution.py:120
  150.7 77.6 %all-gather.31.cloned.1.call-start = ((), (), s32[]{:S(2)}) async-start(), calls=%async_computation.6 | async-start | bytes 1310720 | tf_op jit(solution)/shard_map/all_gather | solution.py:125
  151.4 109.2 %all-gather.33.cloned.1.call-start = ((), (), s32[]{:S(2)}) async-start(), calls=%async_computation.7 | async-start | bytes 1310720 | tf_op jit(solution)/shard_map/all_gather | solution.py:115
  152.2 155.4 %all-gather.37.cloned.1.call-start = ((), (), s32[]{:S(2)}) async-start(), calls=%async_computation.9 | async-start | bytes 1310720 | tf_op jit(solution)/shard_map/all_gather | solution.py:150
  152.9 174.6 %all-gather.21.cloned.1.call-start = ((), (), s32[]{:S(2)}) async-start(), calls=%async_computation.1 | async-start | bytes 1310720 | tf_op jit(solution)/shard_map/all_gather | solution.py:155
  169.0 59.2 %copy-start.4 = (bf16[256,2048]{1,0:T(8,128)(2,1)S(1)}, bf16[256,2048]{1,0:T(8,128)(2,1)}, u32[]{:S(2)}) copy-start(bf16[256,2048]{1,0:T(8,128)(2,1)} %all-gather.19.cloned.1.call-done) | copy-start | bytes 3145732
  197.2 68.7 %collective-permute-start.7 = (bf16[256,256]{0,1:T(8,128)(2,1)S(1)}, bf16[256,256]{0,1:T(8,128)(2,1)S(1)}, u32[]{:S(2)}, u32[]{:S(2)}) collective-permute-start(bf16[256,256]{0,1:T(8,128)(2,1)S(1)} %fusion.59), channel_id=1, source_target_pairs={{0,8},{4,12},{1,9},{5,13},{2,10},{6,14},{3,11},{7,15},{16,24},{20,... | collective-permute-start | bytes 393224 | tf_op jit(solution)/shard_map/ppermute | solution.py:18
  198.5 68.6 %collective-permute-start.8 = (bf16[256,256]{0,1:T(8,128)(2,1)S(1)}, bf16[256,256]{0,1:T(8,128)(2,1)}, u32[]{:S(2)}, u32[]{:S(2)}) collective-permute-start(bf16[256,256]{0,1:T(8,128)(2,1)S(1)} %fusion.59), channel_id=1, source_target_pairs={{0,4},{4,8},{8,12},{1,5},{5,9},{9,13},{2,6},{6,10},{10,14},{3,7},{... | collective-permute-start | bytes 393224 | tf_op jit(solution)/shard_map/ppermute | solution.py:18
  230.6 54.3 %collective-permute-start.9 = (bf16[256,256]{1,0:T(8,128)(2,1)}, bf16[256,256]{1,0:T(8,128)(2,1)}, u32[]{:S(2)}, u32[]{:S(2)}) collective-permute-start(bf16[256,256]{1,0:T(8,128)(2,1)} %convolution_convert_fusion), channel_id=1, source_target_pairs={{0,4},{4,8},{8,12},{1,5},{5,9},{9,13},{2,6},{6,10},{10,14},{3,7},{... | collective-permute-start | bytes 393224 | tf_op jit(solution)/shard_map/ppermute | solution.py:18
  231.9 51.9 %collective-permute-start.6 = (bf16[256,256]{1,0:T(8,128)(2,1)}, bf16[256,256]{1,0:T(8,128)(2,1)}, u32[]{:S(2)}, u32[]{:S(2)}) collective-permute-start(bf16[256,256]{1,0:T(8,128)(2,1)} %convolution_convert_fusion), channel_id=1, source_target_pairs={{0,8},{4,12},{1,9},{5,13},{2,10},{6,14},{3,11},{7,15},{16,24},{20,... | collective-permute-start | bytes 393224 | tf_op jit(solution)/shard_map/ppermute | solution.py:18
  277.8 3.6 %copy-start.6 = (pred[4,64,576]{2,1,0:T(8,128)(4,1)S(1)}, pred[4,64,576]{2,1,0:T(8,128)(4,1)}, u32[]{:S(2)}) copy-start(pred[4,64,576]{2,1,0:T(8,128)(4,1)} %copy-done.5) | copy-start | bytes 442372
  283.8 5.1 %copy-start = (f32[4,4,64,576]{3,2,1,0:T(8,128)S(1)}, f32[4,4,64,576]{3,2,1,0:T(8,128)}, u32[]{:S(2)}) copy-start(f32[4,4,64,576]{3,2,1,0:T(8,128)} %get-tuple-element.66) | copy-start | bytes 7077892
  289.1 1.1 copy-start.1
  290.6 2.5 copy-start.2
  297.6 1.0 copy-start.7
Sparse Core Ops, SparseCore 0:
  8.9 27.2 all-gather.26
  37.8 31.4 all-gather.22
  70.8 29.9 all-gather.24
  102.3 27.9 all-gather.28
  150.2 17.2 all-gather.18
  168.9 25.9 all-gather.34
  196.5 31.7 all-gather.30
  229.8 30.8 all-gather.32
  262.2 27.9 all-gather.36
  310.2 17.2 all-gather.20
where the time goes:
time: 339 us; the launch traced here: 337 us
  waiting for transfers between devices  181 us (53%)
  matrix products  46.2 us (14%)
  local copies, waits for them, and re-layouts  45.5 us (13%)
  other arithmetic  19 us (6%)
  blocking collectives  16.7 us (5%)
  between operations  14.5 us (4%)
  starting transfers between devices  13.7 us (4%)
    all_gather x2, waiting for transfers between devices, on_device(): lax.all_gather(value_weight[layer], 'sp', axis=0, tiled=True)  56.5 us
    all_gather x2, waiting for transfers between devices, on_device(): lax.all_gather(query_weight[layer], 'sp', axis=0, tiled=True)  51.7 us
    all_gather x2, waiting for transfers between devices, on_device(): lax.all_gather(key_weight[layer], 'sp', axis=0, tiled=True)  38.3 us
    all_gather x2, waiting for transfers between devices, on_device(): x = lax.all_gather(new_cols, 'tp', axis=1, tiled=True)  31.9 us
    slice x20, local copies, waits for them, and re-layouts, attend(): value_blocks[earlier:earlier + count]  20.2 us
    dot_general x18, matrix products, attend(): jnp.einsum('nqhd,nkhd->nhqk', blocks, key_blocks[earlier:earlier + count]...  18.4 us
    all_gather x2, blocking collectives, on_device(): all_heads = lax.all_gather(attended, 'tp', axis=1, tiled=True)  16.7 us
    ppermute x10, starting transfers between devices, shifted(): lax.ppermute(value, axis, [(source, source + steps) for source in range(i...  13.3 us
  transfers between devices with their start and end apart: 20, of which 8 were waited for; matrix products, arithmetic and copies ran while one was open for 30% of the time, Pallas kernels for 0%

commit v1 on v0

--- a/solution.py
+++ b/solution.py
@@ -1,6 +1,8 @@
 import jax
 import jax.numpy as jnp
 from jax import lax
+from jax.experimental import pallas as pl
+from jax.experimental.pallas import tpu as pltpu
 from jax.sharding import PartitionSpec as P
 
 SEG = 64
@@ -83,7 +85,7 @@
     return mixed.astype(jnp.bfloat16).reshape(rows, heads_here * head_size)
 
 
-def on_device(
+def on_device_general(
     stream,
     doc_ids,
     norm_gain,
@@ -156,6 +158,313 @@
     return x
 
 
+VMEM = pltpu.MemorySpace.VMEM
+SMEM = pltpu.MemorySpace.SMEM
+f32 = jnp.float32
+bf16 = jnp.bfloat16
+
+
+def folded_ring(count):
+    return list(range(0, count, 2)) + list(range(1, count, 2))[::-1]
+
+
+def ring_step(value, ring):
+    count = len(ring)
+    return lax.ppermute(value, "sp", [(ring[i], ring[(i + 1) % count]) for i in range(count)])
+
+
+def swap_groups(value):
+    return lax.ppermute(value, "grp", [(0, 1), (1, 0)])
+
+
+def gather_halves(half, ring):
+    from_ring, from_group = [], []
+    piece = half
+    for _ in range(len(ring) - 1):
+        piece = ring_step(piece, ring)
+        from_ring.append(piece)
+        from_group.append(swap_groups(piece))
+    return from_ring, from_group
+
+
+def exchange_columns(block, count):
+    pieces = {0: block}
+    step = count // 2
+    while step:
+        pairs = [(i, i ^ step) for i in range(count)]
+        pieces.update({j ^ step: lax.ppermute(p, "tp", pairs) for j, p in list(pieces.items())})
+        step //= 2
+    return [pieces[j] for j in range(count)]
+
+
+def full_spec(array):
+    return pl.BlockSpec(array.shape, lambda i, n=array.ndim: (0,) * n)
+
+
+def window_spec(shape, index):
+    return pl.BlockSpec(shape, lambda i: index)
+
+
+def call(kernel, order, operands, specs, out_shapes, scratch):
+    return pl.pallas_call(
+        kernel,
+        grid=(1,),
+        in_specs=[pl.BlockSpec(memory_space=SMEM)] + specs,
+        out_specs=[pl.BlockSpec(o.shape, lambda i, n=len(o.shape): (0,) * n) for o in out_shapes],
+        out_shape=out_shapes,
+        scratch_shapes=scratch,
+        compiler_params=pltpu.CompilerParams(vmem_limit_bytes=48 << 20),
+    )(order, *operands)
+
+
+def head_norm(raw, gain, head_size):
+    parts = []
+    for start in range(0, raw.shape[1], head_size):
+        part = raw[:, start : start + head_size]
+        parts.append(row_norm(part, gain))
+    return jnp.concatenate(parts, axis=1)
+
+
+def project(x_pieces, gain, q_gain, k_gain, own, pieces, piece_col, order, count):
+    rows, piece_width = x_pieces[0].shape
+    half = own[0].shape[0] // 2
+    width = own[0].shape[1]
+    dims = len(x_pieces) * piece_width
+    blocks = dims // half
+    per_piece = piece_width // half
+    head_size = q_gain.shape[1]
+    gain_blocks = gain.reshape(blocks, 1, half)
+    operands = list(x_pieces) + [gain_blocks, q_gain, k_gain] + list(own)
+    specs = [full_spec(a) for a in operands]
+    for piece in pieces:
+        for j in range(3):
+            operands.append(piece)
+            specs.append(window_spec((half, width), (0, piece_col + j)))
+    n_x, n_p = len(x_pieces), len(pieces)
+
+    def kernel(order_ref, *refs):
+        x_refs, refs = refs[:n_x], refs[n_x:]
+        gain_ref, qg_ref, kg_ref = refs[:3]
+        own_refs, refs = refs[3:6], refs[6:]
+        piece_refs, refs = refs[: 3 * n_p], refs[3 * n_p :]
+        q_ref, kv_ref, xs = refs
+        total = jnp.zeros((rows, 1), f32)
+        for x_ref in x_refs:
+            wide = x_ref[...].astype(f32)
+            total = total + jnp.sum(wide * wide, axis=-1, keepdims=True)
+        scale = lax.rsqrt(total / dims + epsilon)
+        t = order_ref[count + 1]
+        for j, x_ref in enumerate(x_refs):
+            first = (t ^ j) * per_piece if n_x > 1 else 0
+            for b in range(per_piece):
+                wide = x_ref[:, b * half : (b + 1) * half].astype(f32)
+                xs[first + b] = (wide * scale * gain_ref[first + b]).astype(bf16)
+        grp = order_ref[count]
+        sums = []
+        for j in range(3):
+            src = order_ref[0]
+            acc = jnp.dot(xs[2 * src], own_refs[j][:half], preferred_element_type=f32)
+            acc += jnp.dot(xs[2 * src + 1], own_refs[j][half:], preferred_element_type=f32)
+            for k in range(n_p):
+                src = order_ref[k // 2 + 1]
+                part = grp if k % 2 == 0 else 1 - grp
+                acc += jnp.dot(xs[2 * src + part], piece_refs[3 * k + j][...], preferred_element_type=f32)
+            sums.append(acc)
+        q_ref[...] = head_norm(sums[0], qg_ref[...], head_size).astype(bf16)
+        kv_ref[:, :width] = head_norm(sums[1], kg_ref[...], head_size).astype(bf16)
+        kv_ref[:, width:] = sums[2].astype(bf16)
+
+    return call(
+        kernel, order, operands, specs,
+        [jax.ShapeDtypeStruct((rows, width), bf16), jax.ShapeDtypeStruct((rows, 2 * width), bf16)],
+        [pltpu.VMEM((blocks, rows, half), bf16)],
+    )
+
+
+def attend_kernel(query, kv_parts, doc_col, doc_row, flat_bias, order, count, head_size):
+    rows, width = query.shape
+    reach = LEFT * SEG
+    span = reach + rows
+    depth = len(kv_parts) - 1
+    extent = flat_bias.shape[-1]
+    operands = [query] + list(kv_parts) + [doc_col, doc_row, flat_bias]
+    specs = [full_spec(a) for a in operands]
+
+    def kernel(order_ref, q_ref, *refs):
+        kv_refs, refs = refs[: depth + 1], refs[depth + 1 :]
+        dc_ref, dr_ref, fb_ref, out_ref = refs
+        offset = order_ref[0] * rows
+        seg_q = lax.broadcasted_iota(jnp.int32, (rows, span), 0) // SEG
+        col = lax.broadcasted_iota(jnp.int32, (rows, span), 1)
+        seg_k = col // SEG - LEFT
+        allowed = (
+            (seg_k <= seg_q) & (seg_k >= seg_q - LEFT) & (col >= reach - offset)
+            & (dc_ref[...] == dr_ref[...])
+        )
+        outs = []
+        for h in range(width // head_size):
+            lo = h * head_size
+            keys = jnp.concatenate([r[:, lo : lo + head_size] for r in kv_refs], axis=0)
+            vals = jnp.concatenate([r[:, width + lo : width + lo + head_size] for r in kv_refs], axis=0)
+            scores = lax.dot_general(
+                q_ref[:, lo : lo + head_size], keys, (((1,), (1,)), ((), ())),
+                preferred_element_type=f32,
+            ) * head_size ** (-0.5)
+            line = jnp.broadcast_to(fb_ref[h], (rows, extent))
+            bias = pltpu.roll(line, 0, 1, stride=1, stride_axis=0)[:, :span]
+            scores = jnp.where(allowed, scores + bias, -1e30)
+            peak = jnp.max(scores, axis=-1, keepdims=True)
+            expo = jnp.exp(scores - peak)
+            weights = (expo / jnp.sum(expo, axis=-1, keepdims=True)).astype(bf16)
+            outs.append(jnp.dot(weights, vals, preferred_element_type=f32))
+        out_ref[...] = jnp.concatenate(outs, axis=1).astype(bf16)
+
+    return call(kernel, order, operands, specs, [jax.ShapeDtypeStruct((rows, width), bf16)], [])[0]
+
+
+def output(attended, residual, own, pieces, layer, order, count):
+    rows, dims = attended.shape
+    half = own.shape[0] // 2
+    cols = own.shape[1]
+    blocks = dims // half
+    operands = [attended, residual, own] + list(pieces)
+    specs = [full_spec(a) for a in operands[:3]]
+    specs += [window_spec((half, cols), (layer, 0)) for _ in pieces]
+
+    def kernel(order_ref, a_ref, r_ref, own_ref, *refs):
+        piece_refs, (out_ref, xs) = refs[: len(pieces)], refs[len(pieces) :]
+        for b in range(blocks):
+            xs[b] = a_ref[:, b * half : (b + 1) * half]
+        grp = order_ref[count]
+        src = order_ref[0]
+        acc = jnp.dot(xs[2 * src], own_ref[:half], preferred_element_type=f32)
+        acc += jnp.dot(xs[2 * src + 1], own_ref[half:], preferred_element_type=f32)
+        for k in range(len(pieces)):
+            src = order_ref[k // 2 + 1]
+            part = grp if k % 2 == 0 else 1 - grp
+            acc += jnp.dot(xs[2 * src + part], piece_refs[k][...], preferred_element_type=f32)
+        out_ref[...] = (r_ref[...].astype(f32) + acc).astype(bf16)
+
+    return call(
+        kernel, order, operands, specs, [jax.ShapeDtypeStruct((rows, cols), bf16)],
+        [pltpu.VMEM((blocks, rows, half), bf16)],
+    )[0]
+
+
+def assemble(pieces, order, count):
+    rows, cols = pieces[0].shape
+
+    def kernel(order_ref, *refs):
+        t = order_ref[count + 1]
+        for j in range(len(pieces)):
+            start = pl.multiple_of((t ^ j) * cols, cols)
+            refs[-1][:, pl.ds(start, cols)] = refs[j][...]
+
+    return call(
+        kernel, order, pieces, [full_spec(a) for a in pieces],
+        [jax.ShapeDtypeStruct((rows, cols * len(pieces)), bf16)], [],
+    )[0]
+
+
+def flat_biases(rel_bias, rows):
+    reach = LEFT * SEG
+    heads_here = rel_bias.shape[0]
+    extent = 128 * (-(-(reach + 2 * rows - 1) // 128))
+    far = jnp.broadcast_to(rel_bias[:, -1:], (heads_here, reach - MAXREL))
+    near = rel_bias[:, MAXREL - rows + 1 :][:, ::-1]
+    tail = jnp.broadcast_to(rel_bias[:, -1:], (heads_here, extent - reach - rows))
+    return jnp.concatenate([far, near, tail], axis=1)[:, None, :]
+
+
+def interleave(ring_pieces, group_pieces):
+    return [p for pair in zip(ring_pieces, group_pieces) for p in pair]
+
+
+def on_device_fast(
+    stream, doc_ids, norm_gain, query_weight, key_weight, value_weight, out_weight,
+    query_gain, key_gain, rel_bias,
+):
+    rows = stream.shape[0]
+    count = lax.axis_size("sp")
+    tp_count = lax.axis_size("tp")
+    grp = lax.axis_index("grp")
+    place = lax.axis_index("sp")
+    t = lax.axis_index("tp")
+    head_size = query_gain.shape[1]
+    reach = LEFT * SEG
+    depth = -(-reach // rows)
+    cols = out_weight.shape[2]
+    ring = folded_ring(count)
+    slots = jnp.array([ring.index(i) for i in range(count)], jnp.int32)
+    ring_of = jnp.array(ring, jnp.int32)
+    steps = jnp.arange(count, dtype=jnp.int32)
+    sources = ring_of[(slots[place] - steps) % count]
+    order = jnp.concatenate([sources, jnp.stack([grp, t]).astype(jnp.int32)])
+
+    in_half = query_weight.shape[1] // 2
+    out_half = out_weight.shape[1] // 2
+
+    def half_of(weight, size):
+        return lax.dynamic_slice_in_dim(weight, grp * size, size, 0)
+
+    first = jnp.concatenate(
+        [half_of(w[0], in_half) for w in (query_weight, key_weight, value_weight)], axis=1
+    )
+    outs = jnp.concatenate([half_of(out_weight[l], out_half) for l in range(LAYERS)], axis=0)
+    second = jnp.concatenate(
+        [outs] + [half_of(w[1], in_half) for w in (query_weight, key_weight, value_weight)], axis=1
+    )
+    a_ring, a_group = gather_halves(first, ring)
+    second, _ = lax.optimization_barrier((second, a_ring[-1]))
+    b_ring, b_group = gather_halves(second, ring)
+    a_pieces = interleave(a_ring, a_group)
+    b_pieces = interleave(b_ring, b_group)
+
+    all_docs = lax.all_gather(doc_ids, "sp", axis=0, tiled=True)
+    padded = jnp.concatenate([jnp.full((reach,), -1, jnp.int32), all_docs])
+    doc_row = lax.dynamic_slice_in_dim(padded, place * rows, reach + rows, 0)[None, :]
+    doc_col = doc_ids[:, None]
+    flat = flat_biases(rel_bias, rows)
+
+    residual = lax.dynamic_slice_in_dim(stream, t * cols, cols, 1)
+    x_pieces = [stream]
+    for layer in range(LAYERS):
+        own = [w[layer] for w in (query_weight, key_weight, value_weight)]
+        pieces = a_pieces if layer == 0 else b_pieces
+        col = 0 if layer == 0 else cols // own[0].shape[1]
+        query, kv = project(
+            x_pieces, norm_gain[layer], query_gain[layer][None], key_gain[layer][None],
+            own, pieces, col, order, count,
+        )
+        received = [shifted(kv, "sp", back) for back in range(depth, 0, -1)]
+        attended = attend_kernel(
+            query, received + [kv], doc_col, doc_row, flat, order, count, head_size
+        )
+        all_heads = lax.all_gather(attended, "tp", axis=1, tiled=True)
+        block = output(all_heads, residual, out_weight[layer], b_pieces, layer, order, count)
+        x_pieces = exchange_columns(block, tp_count)
+        residual = block
+    return assemble(x_pieces, order, count)
+
+
+def on_device(*arrays):
+    stream, query_weight, out_weight = arrays[0], arrays[3], arrays[6]
+    rows, dims = stream.shape
+    count, tp_count = lax.axis_size("sp"), lax.axis_size("tp")
+    in_rows, width = query_weight.shape[1:]
+    out_rows, cols = out_weight.shape[1:]
+    fits = (
+        lax.axis_size("grp") == 2 and LAYERS == 2
+        and 2 < count <= 4 and tp_count & (tp_count - 1) == 0
+        and in_rows % 256 == 0 and out_rows % 256 == 0
+        and 2 * (out_rows // 2) == in_rows // 2
+        and width % 128 == 0 and cols % width == 0
+        and cols % (in_rows // 2) == 0 and tp_count > 1
+        and rows <= MAXREL and (LEFT * SEG) % rows == 0 and rows % SEG == 0
+    )
+    return on_device_fast(*arrays) if fits else on_device_general(*arrays)
+
+
 def solution(mesh):
     placed = (
         P(("grp", "sp"), None),

time: 339 us -> 198 us (0.58)
  waiting for transfers between devices: 181 us -> 94.9 us
  matrix products: 46.2 us -> 0 us
  local copies, waits for them, and re-layouts: 45.5 us -> 19.4 us
  Pallas kernels: 0 us -> 21.9 us
  blocking collectives: 16.7 us -> 35.6 us
  other arithmetic: 19 us -> 0.73 us
  between operations: 14.5 us -> 0.34 us
  starting transfers between devices: 13.7 us -> 24.3 us
    all_gather x10 -> x0, waiting for transfers between devices: 178 us -> none  [the longest x2 56.5 us: on_device(): lax.all_gather(value_weight[layer], 'sp', axis=0, tiled=True)]
    ppermute x0 -> x18, waiting for transfers between devices: none -> 70.4 us  [the longest x6 48.3 us: ring_step(): lax.ppermute(value, 'sp', [(ring[i], ring[(i + 1) % count]) for i in rang...]
    dot_general x44 -> x0, matrix products: 46.2 us -> none  [the longest x18 18.4 us: attend(): jnp.einsum('nqhd,nkhd->nhqk', blocks, key_blocks[earlier:earlier + count]...]
    slice x48 -> x4, local copies, waits for them, and re-layouts: 30 us -> 1.4 us  [the longest x1 0.61 us: on_device_fast(): norm_gain[layer]]
    ppermute x10 -> x4, waiting for transfers between devices: 0.03 us -> 24.5 us  [shifted(): lax.ppermute(value, axis, [(source, source + steps) for source in range(i...]
    pallas_call x0 -> x7, Pallas kernels: none -> 21.9 us  [call(): pl.pallas_call(kernel, grid=(1,), in_specs=[pl.BlockSpec(memory_space=SME...]
    all_gather x2 -> x3, blocking collectives: 16.7 us -> 35.6 us  [the longest x2 28.9 us: on_device_fast(): all_heads = lax.all_gather(attended, 'tp', axis=1, tiled=True)]
    ppermute x0 -> x18, starting transfers between devices: none -> 18.8 us  [the longest x6 8.82 us: ring_step(): lax.ppermute(value, 'sp', [(ring[i], ring[(i + 1) % count]) for i in rang...]
  transfers between devices with their start and end apart: 20 -> 22, of which waited for: 8 -> 16; matrix products, arithmetic and copies ran while one was open for 30% -> 4% of each run, Pallas kernels for 0% -> 5%
where the time goes in v1:
time: 198 us; the launch traced here: 197 us
  waiting for transfers between devices  94.9 us (48%)
  blocking collectives  35.6 us (18%)
  starting transfers between devices  24.3 us (12%)
  Pallas kernels  21.9 us (11%)
  local copies, waits for them, and re-layouts  19.4 us (10%)
    ppermute x6, waiting for transfers between devices, ring_step(): lax.ppermute(value, 'sp', [(ring[i], ring[(i + 1) % count]) for i in rang...  48.3 us
    all_gather x2, blocking collectives, on_device_fast(): all_heads = lax.all_gather(attended, 'tp', axis=1, tiled=True)  28.9 us
    ppermute x4, waiting for transfers between devices, shifted(): lax.ppermute(value, axis, [(source, source + steps) for source in range(i...  24.5 us
    pallas_call x7, Pallas kernels, call(): pl.pallas_call(kernel, grid=(1,), in_specs=[pl.BlockSpec(memory_space=SME...  21.9 us
    ppermute x6, waiting for transfers between devices, exchange_columns(): lax.ppermute(p, 'tp', pairs)  15.4 us
    unnamed x64, local copies, waits for them, and re-layouts  9.17 us
    ppermute x6, starting transfers between devices, ring_step(): lax.ppermute(value, 'sp', [(ring[i], ring[(i + 1) % count]) for i in rang...  8.82 us
    ppermute x6, waiting for transfers between devices, swap_groups(): return lax.ppermute(value, 'grp', [(0, 1), (1, 0)])  6.72 us
  transfers between devices with their start and end apart: 22, of which 16 were waited for; matrix products, arithmetic and copies ran while one was open for 4% of the time, Pallas kernels for 5%

profile of v1, /device:TPU:25, one launch (start us, length us, event | category | flops | bytes accessed | tf_op | source)
XLA Modules:
  0.0 197.3 jit_solution(10576936140368066329)
XLA Ops:
  0.0 2.0 %slice_bitcast_fusion.2 = (bf16[512,256]{1,0:T(8,128)(2,1)}, bf16[512,256]{1,0:T(8,128)(2,1)}, bf16[1,512,256]{2,1,0:T(8,128)(2,1)S(1)}, bf16[1,512,256]{2,1,0:T(8,128)(2,1)S(1)}) fusion(bf16[2,512,256]{2,1,0:T(8,128)(2,1)} %param.15), kind=kLoop, calls=%fused_computation.25 | loop fusion | bytes 1572864 | tf_op jit(solution)/shard_map/squeeze | solution.py:415
  4.3 9.9 %collective-permute-done.refs_7_.refs_8_.refs_9_ = bf16[256,768]{1,0:T(8,128)(2,1)S(1)} collective-permute-done((bf16[256,768]{1,0:T(8,128)(2,1)S(1)}, bf16[256,768]{1,0:T(8,128)(2,1)S(1)}, u32[]{:S(2)}, u32[]{:S(2)}) %collective-permute-start) | collective-permute-done | bytes 393248 | tf_op jit(solution)/shard_map/ppermute | solution.py:173
  14.2 1.0 collective-permute-start.2
  16.1 7.3 %collective-permute-done.2.refs_13_.refs_14_.refs_15_ = bf16[256,768]{1,0:T(8,128)(2,1)} collective-permute-done((bf16[256,768]{1,0:T(8,128)(2,1)S(1)}, bf16[256,768]{1,0:T(8,128)(2,1)}, u32[]{:S(2)}, u32[]{:S(2)}) %collective-permute-start.2) | collective-permute-done | bytes 393248 | tf_op jit(solution)/shard_map/ppermute | solution.py:173
  23.5 1.9 collective-permute-start.4
  25.5 7.4 %collective-permute-done.4.refs_19_.refs_20_.refs_21_ = bf16[256,768]{1,0:T(8,128)(2,1)} collective-permute-done((bf16[256,768]{1,0:T(8,128)(2,1)}, bf16[256,768]{1,0:T(8,128)(2,1)}, u32[]{:S(2)}, u32[]{:S(2)}) %collective-permute-start.4) | collective-permute-done | bytes 393248 | tf_op jit(solution)/shard_map/ppermute | solution.py:173
  32.9 2.0 collective-permute-start.8
  34.8 12.0 %collective-permute-done.8.refs_0_.refs_10_.refs_11_.refs_12_ = bf16[256,1280]{1,0:T(8,128)(2,1)S(1)} collective-permute-done((bf16[256,1280]{1,0:T(8,128)(2,1)S(1)}, bf16[256,1280]{1,0:T(8,128)(2,1)S(1)}, u32[]{:S(2)}, u32[]{:S(2)}) %collective-permute-start.8) | collective-permute-done | bytes 655392 | tf_op jit(solution)/shard_map/ppermute | solution.py:173
  46.8 2.0 collective-permute-start.10
  48.8 11.2 %collective-permute-done.10.refs_2_.refs_16_.refs_17_.refs_18_ = bf16[256,1280]{1,0:T(8,128)(2,1)S(1)} collective-permute-done((bf16[256,1280]{1,0:T(8,128)(2,1)S(1)}, bf16[256,1280]{1,0:T(8,128)(2,1)S(1)}, u32[]{:S(2)}, u32[]{:S(2)}) %collective-permute-start.10) | collective-permute-done | bytes 655392 | tf_op jit(solution)/shard_map/ppermute | solution.py:173
  60.0 2.0 collective-permute-start.12
  63.8 1.3 collective-permute-start.1
  65.9 1.2 collective-permute-start.5
  68.1 2.7 %collective-permute-done.1.refs_10_.refs_11_.refs_12_ = bf16[256,768]{1,0:T(8,128)(2,1)S(1)} collective-permute-done((bf16[256,768]{1,0:T(8,128)(2,1)S(1)}, bf16[256,768]{1,0:T(8,128)(2,1)S(1)}, u32[]{:S(2)}, u32[]{:S(2)}) %collective-permute-start.1) | collective-permute-done | bytes 393248 | tf_op jit(solution)/shard_map/ppermute | solution.py:177
  71.5 1.2 collective-permute-start.11
  73.2 1.2 collective-permute-start.13
  74.4 6.7 %all-gather = s32[4,1,256]{2,1,0:T(1,128)S(1)} all-gather(s32[1,1,256]{2,1,0:T(1,128)S(1)} %bitcast.46), channel_id=1, replica_groups=mesh['grp'=2,'sp'=4,'tp'=4] {'sp'}, dimensions={0}, use_global_device_ids=true | all-gather | bytes 5120 | tf_op jit(solution)/shard_map/all_gather | solution.py:423
  81.2 4.1 %collective-permute-done.5.refs_22_.refs_23_.refs_24_ = bf16[256,768]{1,0:T(8,128)(2,1)} collective-permute-done((bf16[256,768]{1,0:T(8,128)(2,1)}, bf16[256,768]{1,0:T(8,128)(2,1)}, u32[]{:S(2)}, u32[]{:S(2)}) %collective-permute-start.5) | collective-permute-done | bytes 393248 | tf_op jit(solution)/shard_map/ppermute | solution.py:177
  85.3 1.0 copy-done.1
  86.3 1.0 copy-done.3
  87.3 1.2 copy-done.4
  88.5 0.9 copy-done.8
  90.4 0.9 copy-done.10
  92.0 4.7 %shard_map.118 = (bf16[256,256]{1,0:T(8,128)(2,1)S(1)}, bf16[256,512]{1,0:T(8,128)(2,1)}) custom-call(s32[6]{0:T(128)S(1)} %pad_add_fusion.order_ref, bf16[256,2048]{1,0:T(8,128)(2,1)S(1)} %copy-done.4, f32[8,1,256]{2,1,0:T(1,128)S(1)} %bitcast.43, f32[1,64]{1,0:T(1,128)S(1)} %copy-done.21, f32[1,64]{1,0:T(1,128)S(1)} %get-tuple-element.34.refs_3_, ...), custom_call_target="tpu_custom_call" | custom-call | tf_op jit(solution)/shard_map/pallas_call | solution.py:209
  96.7 1.3 collective-permute-start.7
  98.0 1.3 collective-permute-start.6
  101.4 1.0 constant_dynamic-slice_fusion.r_ref
  102.4 2.0 collective-permute-done.7.refs_1_
  104.3 5.5 %collective-permute-done.6.refs_0_ = bf16[256,512]{1,0:T(8,128)(2,1)} collective-permute-done((bf16[256,512]{1,0:T(8,128)(2,1)}, bf16[256,512]{1,0:T(8,128)(2,1)}, u32[]{:S(2)}, u32[]{:S(2)}) %collective-permute-start.6) | collective-permute-done | bytes 262176 | tf_op jit(solution)/shard_map/ppermute | solution.py:20
  111.2 4.6 %shard_map.119 = bf16[256,256]{1,0:T(8,128)(2,1)S(1)} custom-call(s32[6]{0:T(128)S(1)} %copy-done.15, bf16[256,256]{1,0:T(8,128)(2,1)S(1)} %get-tuple-element.10.q_ref, bf16[256,512]{1,0:T(8,128)(2,1)} %collective-permute-done.6.refs_0_, bf16[256,512]{1,0:T(8,128)(2,1)} %collective-permute-done.7.refs_1_, bf16[256,512]{1,0:T(8,128)(2,1)} %get-tuple-element.11.refs_2_, ...), custom_call_target="tpu_custom_call" | custom-call | tf_op jit(solution)/shard_map/pallas_call | solution.py:209
  115.7 21.3 %all_gather.10.a_ref = bf16[256,1024]{1,0:T(8,128)(2,1)S(1)} all-gather(bf16[256,256]{1,0:T(8,128)(2,1)S(1)} %shard_map.119), channel_id=1, replica_groups=mesh['grp'=2,'sp'=4,'tp'=4] {'tp'}, dimensions={1}, use_global_device_ids=true | all-gather | bytes 655360 | tf_op jit(solution)/shard_map/all_gather | solution.py:443
  137.2 1.8 shard_map.120.refs_0_.r_ref
  140.0 6.7 %collective-permute-done.15.refs_2_ = bf16[256,512]{1,0:T(8,128)(2,1)S(1)} collective-permute-done((bf16[256,512]{1,0:T(8,128)(2,1)S(1)}, bf16[256,512]{1,0:T(8,128)(2,1)S(1)}, u32[]{:S(2)}, u32[]{:S(2)}) %collective-permute-start.15) | collective-permute-done | bytes 262176 | tf_op jit(solution)/shard_map/ppermute | solution.py:195
  146.7 1.0 collective-permute-start.16
  147.7 1.2 collective-permute-done.16.refs_3_
  148.9 3.6 %shard_map.121 = (bf16[256,256]{1,0:T(8,128)(2,1)S(1)}, bf16[256,512]{1,0:T(8,128)(2,1)S(1)}) custom-call(s32[6]{0:T(128)S(1)} %copy-done.16, bf16[256,512]{1,0:T(8,128)(2,1)S(1)} %shard_map.120.refs_0_.r_ref, bf16[256,512]{1,0:T(8,128)(2,1)S(1)} %collective-permute-done.14.refs_1_, bf16[256,512]{1,0:T(8,128)(2,1)S(1)} %collective-permute-done.15.refs_2_, ...), custom_call_target="tpu_custom_call" | custom-call | tf_op jit(solution)/shard_map/pallas_call | solution.py:209
  152.5 1.4 collective-permute-start.18
  154.0 1.5 collective-permute-start.17
  155.4 6.9 %collective-permute-done.18.refs_1_ = bf16[256,512]{1,0:T(8,128)(2,1)S(1)} collective-permute-done((bf16[256,512]{1,0:T(8,128)(2,1)S(1)}, bf16[256,512]{1,0:T(8,128)(2,1)S(1)}, u32[]{:S(2)}, u32[]{:S(2)}) %collective-permute-start.18) | collective-permute-done | bytes 262176 | tf_op jit(solution)/shard_map/ppermute | solution.py:20
  162.3 10.1 %collective-permute-done.17.refs_0_ = bf16[256,512]{1,0:T(8,128)(2,1)S(1)} collective-permute-done((bf16[256,512]{1,0:T(8,128)(2,1)S(1)}, bf16[256,512]{1,0:T(8,128)(2,1)S(1)}, u32[]{:S(2)}, u32[]{:S(2)}) %collective-permute-start.17) | collective-permute-done | bytes 262176 | tf_op jit(solution)/shard_map/ppermute | solution.py:20
  172.4 4.0 %shard_map.122 = bf16[256,256]{1,0:T(8,128)(2,1)S(1)} custom-call(s32[6]{0:T(128)S(1)} %copy-done.16, bf16[256,256]{1,0:T(8,128)(2,1)S(1)} %get-tuple-element.13.q_ref, bf16[256,512]{1,0:T(8,128)(2,1)S(1)} %collective-permute-done.17.refs_0_, bf16[256,512]{1,0:T(8,128)(2,1)S(1)} %collective-permute-done.18.refs_1_, ...), custom_call_target="tpu_custom_call" | custom-call | tf_op jit(solution)/shard_map/pallas_call | solution.py:209
  176.4 7.6 %all_gather.11.a_ref = bf16[256,1024]{1,0:T(8,128)(2,1)S(1)} all-gather(bf16[256,256]{1,0:T(8,128)(2,1)S(1)} %shard_map.122), channel_id=1, replica_groups=mesh['grp'=2,'sp'=4,'tp'=4] {'tp'}, dimensions={1}, use_global_device_ids=true | all-gather | bytes 655360 | tf_op jit(solution)/shard_map/all_gather | solution.py:443
  184.0 1.7 shard_map.123.refs_0_
  185.8 1.0 collective-permute-start.20
  187.2 6.3 %collective-permute-done.20.refs_2_ = bf16[256,512]{1,0:T(8,128)(2,1)S(1)} collective-permute-done((bf16[256,512]{1,0:T(8,128)(2,1)S(1)}, bf16[256,512]{1,0:T(8,128)(2,1)S(1)}, u32[]{:S(2)}, u32[]{:S(2)}) %collective-permute-start.20) | collective-permute-done | bytes 262176 | tf_op jit(solution)/shard_map/ppermute | solution.py:195
  193.5 1.0 collective-permute-start.21
  194.6 1.2 collective-permute-done.21.refs_3_
  195.7 1.6 shard_map.124
  (98 shorter events, 14.7 us)
Async XLA Ops:
  0.0 2.0 %copy-start.23 = (bf16[2,512,256]{2,1,0:T(8,128)(2,1)S(1)}, bf16[2,512,256]{2,1,0:T(8,128)(2,1)}, u32[]{:S(2)}) copy-start(bf16[2,512,256]{2,1,0:T(8,128)(2,1)} %param.16) | copy-start | bytes 1572868
  2.0 1.2 copy-start.24
  4.1 11.1 %copy-start.25 = (bf16[2,256,512]{2,1,0:T(8,128)(2,1)S(1)}, bf16[2,256,512]{2,1,0:T(8,128)(2,1)}, u32[]{:S(2)}) copy-start(bf16[2,256,512]{2,1,0:T(8,128)(2,1)} %param.18) | copy-start | bytes 1572868
  4.2 10.1 %collective-permute-start = (bf16[256,768]{1,0:T(8,128)(2,1)S(1)}, bf16[256,768]{1,0:T(8,128)(2,1)S(1)}, u32[]{:S(2)}, u32[]{:S(2)}) collective-permute-start(bf16[256,768]{1,0:T(8,128)(2,1)S(1)} %pad_maximum_fusion.1), channel_id=1, source_target_pairs={{0,8},{8,12},{12,4},{4,0},{1,9},{9,13},{13,5},{5,1},{2,10},{10,14}... | collective-permute-start | bytes 1179656 | tf_op jit(solution)/shard_map/ppermute | solution.py:173
  14.2 49.5 %copy-start = (bf16[256,768]{1,0:T(8,128)(2,1)}, bf16[256,768]{1,0:T(8,128)(2,1)S(1)}, u32[]{:S(2)}) copy-start(bf16[256,768]{1,0:T(8,128)(2,1)S(1)} %collective-permute-done.refs_7_.refs_8_.refs_9_) | copy-start | bytes 1179652
  14.2 9.2 %collective-permute-start.2 = (bf16[256,768]{1,0:T(8,128)(2,1)S(1)}, bf16[256,768]{1,0:T(8,128)(2,1)}, u32[]{:S(2)}, u32[]{:S(2)}) collective-permute-start(bf16[256,768]{1,0:T(8,128)(2,1)S(1)} %collective-permute-done.refs_7_.refs_8_.refs_9_), channel_id=1, source_target_pairs={{0,8},{8,12},{12,4},{4,0},{1,9},{9,13},{13,5},{5,1},{2,10},{10,14}... | collective-permute-start | bytes 1179656 | tf_op jit(solution)/shard_map/ppermute | solution.py:173
  23.5 9.4 %collective-permute-start.4 = (bf16[256,768]{1,0:T(8,128)(2,1)}, bf16[256,768]{1,0:T(8,128)(2,1)}, u32[]{:S(2)}, u32[]{:S(2)}) collective-permute-start(bf16[256,768]{1,0:T(8,128)(2,1)} %collective-permute-done.2.refs_13_.refs_14_.refs_15_), channel_id=1, source_target_pairs={{0,8},{8,12},{12,4},{4,0},{1,9},{9,13},{13,5},{5,1},{2,10},{10,14}... | collective-permute-start | bytes 1179656 | tf_op jit(solution)/shard_map/ppermute | solution.py:173
  25.3 36.6 %copy-start.26 = (f32[2,2048]{1,0:T(2,128)S(1)}, f32[2,2048]{1,0:T(2,128)}, u32[]{:S(2)}) copy-start(f32[2,2048]{1,0:T(2,128)} %param.14) | copy-start | bytes 49156
  25.3 37.3 %copy-start.31 = (s32[4]{0:T(128)S(1)}, s32[4]{0:T(128)}, u32[]{:S(2)}) copy-start(s32[4]{0:T(128)} %constant.55.clone) | copy-start | bytes 52
  25.3 39.7 %copy-start.22 = (s32[4]{0:T(128)S(1)}, s32[4]{0:T(128)}, u32[]{:S(2)}) copy-start(s32[4]{0:T(128)} %constant.56.clone) | copy-start | bytes 52
  25.4 41.9 %copy-start.29 = (f32[2,64]{1,0:T(2,128)S(1)}, f32[2,64]{1,0:T(2,128)}, u32[]{:S(2)}) copy-start(f32[2,64]{1,0:T(2,128)} %param.20) | copy-start | bytes 1540
  25.4 41.9 %copy-start.30 = (f32[2,64]{1,0:T(2,128)S(1)}, f32[2,64]{1,0:T(2,128)}, u32[]{:S(2)}) copy-start(f32[2,64]{1,0:T(2,128)} %param.19) | copy-start | bytes 1540
  25.4 49.0 %copy-start.28 = (s32[256]{0:T(256)S(1)}, s32[256]{0:T(256)}, u32[]{:S(2)}) copy-start(s32[256]{0:T(256)} %param.13) | copy-start | bytes 3076
  32.9 13.9 %collective-permute-start.8 = (bf16[256,1280]{1,0:T(8,128)(2,1)S(1)}, bf16[256,1280]{1,0:T(8,128)(2,1)S(1)}, u32[]{:S(2)}, u32[]{:S(2)}) collective-permute-start(bf16[256,1280]{1,0:T(8,128)(2,1)S(1)} %pad_maximum_fusion), channel_id=1, source_target_pairs={{0,8},{8,12},{12,4},{4,0},{1,9},{9,13},{13,5},{5,1},{2,10},{10,14}... | collective-permute-start | bytes 1966088 | tf_op jit(solution)/shard_map/ppermute | solution.py:173
  46.8 13.2 %collective-permute-start.10 = (bf16[256,1280]{1,0:T(8,128)(2,1)S(1)}, bf16[256,1280]{1,0:T(8,128)(2,1)S(1)}, u32[]{:S(2)}, u32[]{:S(2)}) collective-permute-start(bf16[256,1280]{1,0:T(8,128)(2,1)S(1)} %collective-permute-done.8.refs_0_.refs_10_.refs_11_.refs_12_), channel_id=1, source_target_pairs={{0,8},{8,12},{12,4},{4,0},{1,9},{9,13},{13,5},{5,1},{2,10},{10,14}... | collective-permute-start | bytes 1966088 | tf_op jit(solution)/shard_map/ppermute | solution.py:173
  60.0 13.2 %collective-permute-start.12 = (bf16[256,1280]{1,0:T(8,128)(2,1)S(1)}, bf16[256,1280]{1,0:T(8,128)(2,1)S(1)}, u32[]{:S(2)}, u32[]{:S(2)}) collective-permute-start(bf16[256,1280]{1,0:T(8,128)(2,1)S(1)} %collective-permute-done.10.refs_2_.refs_16_.refs_17_.refs_18_), channel_id=1, source_target_pairs={{0,8},{8,12},{12,4},{4,0},{1,9},{9,13},{13,5},{5,1},{2,10},{10,14}... | collective-permute-start | bytes 1966088 | tf_op jit(solution)/shard_map/ppermute | solution.py:173
  63.8 7.0 %collective-permute-start.1 = (bf16[256,768]{1,0:T(8,128)(2,1)S(1)}, bf16[256,768]{1,0:T(8,128)(2,1)S(1)}, u32[]{:S(2)}, u32[]{:S(2)}) collective-permute-start(bf16[256,768]{1,0:T(8,128)(2,1)S(1)} %collective-permute-done.refs_7_.refs_8_.refs_9_), channel_id=1, source_target_pairs={{0,16},{16,0},{1,17},{17,1},{2,18},{18,2},{3,19},{19,3},{4,20},{20... | collective-permute-start | bytes 1179656 | tf_op jit(solution)/shard_map/ppermute | solution.py:177
  65.7 15.5 %collective-permute-start.3 = (bf16[256,768]{1,0:T(8,128)(2,1)}, bf16[256,768]{1,0:T(8,128)(2,1)}, u32[]{:S(2)}, u32[]{:S(2)}) collective-permute-start(bf16[256,768]{1,0:T(8,128)(2,1)} %collective-permute-done.2.refs_13_.refs_14_.refs_15_), channel_id=1, source_target_pairs={{0,16},{16,0},{1,17},{17,1},{2,18},{18,2},{3,19},{19,3},{4,20},{20... | collective-permute-start | bytes 1179656 | tf_op jit(solution)/shard_map/ppermute | solution.py:177
  65.9 19.3 %collective-permute-start.5 = (bf16[256,768]{1,0:T(8,128)(2,1)}, bf16[256,768]{1,0:T(8,128)(2,1)}, u32[]{:S(2)}, u32[]{:S(2)}) collective-permute-start(bf16[256,768]{1,0:T(8,128)(2,1)} %collective-permute-done.4.refs_19_.refs_20_.refs_21_), channel_id=1, source_target_pairs={{0,16},{16,0},{1,17},{17,1},{2,18},{18,2},{3,19},{19,3},{4,20},{20... | collective-permute-start | bytes 1179656 | tf_op jit(solution)/shard_map/ppermute | solution.py:177
  67.3 29.5 %copy-start.14 = (s32[6]{0:T(128)}, s32[6]{0:T(128)S(1)}, u32[]{:S(2)}) copy-start(s32[6]{0:T(128)S(1)} %pad_add_fusion.order_ref) | copy-start | bytes 76
  67.9 69.2 %collective-permute-start.9 = (bf16[256,1280]{1,0:T(8,128)(2,1)S(1)}, bf16[256,1280]{1,0:T(8,128)(2,1)S(1)}, u32[]{:S(2)}, u32[]{:S(2)}) collective-permute-start(bf16[256,1280]{1,0:T(8,128)(2,1)S(1)} %collective-permute-done.8.refs_0_.refs_10_.refs_11_.refs_12_), channel_id=1, source_target_pairs={{0,16},{16,0},{1,17},{17,1},{2,18},{18,2},{3,19},{19,3},{4,20},{20... | collective-permute-start | bytes 1966088 | tf_op jit(solution)/shard_map/ppermute | solution.py:177
  71.5 65.6 %collective-permute-start.11 = (bf16[256,1280]{1,0:T(8,128)(2,1)S(1)}, bf16[256,1280]{1,0:T(8,128)(2,1)S(1)}, u32[]{:S(2)}, u32[]{:S(2)}) collective-permute-start(bf16[256,1280]{1,0:T(8,128)(2,1)S(1)} %collective-permute-done.10.refs_2_.refs_16_.refs_17_.refs_18_), channel_id=1, source_target_pairs={{0,16},{16,0},{1,17},{17,1},{2,18},{18,2},{3,19},{19,3},{4,20},{20... | collective-permute-start | bytes 1966088 | tf_op jit(solution)/shard_map/ppermute | solution.py:177
  73.2 63.9 %collective-permute-start.13 = (bf16[256,1280]{1,0:T(8,128)(2,1)S(1)}, bf16[256,1280]{1,0:T(8,128)(2,1)}, u32[]{:S(2)}, u32[]{:S(2)}) collective-permute-start(bf16[256,1280]{1,0:T(8,128)(2,1)S(1)} %collective-permute-done.12.refs_4_.refs_22_.refs_23_.refs_24_), channel_id=1, source_target_pairs={{0,16},{16,0},{1,17},{17,1},{2,18},{18,2},{3,19},{19,3},{4,20},{20... | collective-permute-start | bytes 1966088 | tf_op jit(solution)/shard_map/ppermute | solution.py:177
  85.3 1.0 copy-start.1
  86.3 1.0 copy-start.3
  87.3 1.2 copy-start.4
  88.5 0.9 copy-start.8
  92.0 7.3 %copy-start.27 = (f32[4,513]{1,0:T(4,128)S(1)}, f32[4,513]{1,0:T(4,128)}, u32[]{:S(2)}) copy-start(f32[4,513]{1,0:T(4,128)} %param.21) | copy-start | bytes 24628
  96.7 7.6 %collective-permute-start.7 = (bf16[256,512]{1,0:T(8,128)(2,1)}, bf16[256,512]{1,0:T(8,128)(2,1)}, u32[]{:S(2)}, u32[]{:S(2)}) collective-permute-start(bf16[256,512]{1,0:T(8,128)(2,1)} %get-tuple-element.11.refs_2_), channel_id=1, source_target_pairs={{0,4},{4,8},{8,12},{1,5},{5,9},{9,13},{2,6},{6,10},{10,14},{3,7},{... | collective-permute-start | bytes 786440 | tf_op jit(solution)/shard_map/ppermute | solution.py:20
  98.0 11.9 %collective-permute-start.6 = (bf16[256,512]{1,0:T(8,128)(2,1)}, bf16[256,512]{1,0:T(8,128)(2,1)}, u32[]{:S(2)}, u32[]{:S(2)}) collective-permute-start(bf16[256,512]{1,0:T(8,128)(2,1)} %get-tuple-element.11.refs_2_), channel_id=1, source_target_pairs={{0,8},{4,12},{1,9},{5,13},{2,10},{6,14},{3,11},{7,15},{16,24},{20,... | collective-permute-start | bytes 786440 | tf_op jit(solution)/shard_map/ppermute | solution.py:20
  101.4 35.7 %copy-start.16 = (s32[6]{0:T(128)S(1)}, s32[6]{0:T(128)}, u32[]{:S(2)}) copy-start(s32[6]{0:T(128)} %copy-done.14) | copy-start | bytes 76
  102.4 34.7 %copy-start.12 = (bf16[256,512]{1,0:T(8,128)(2,1)S(1)}, bf16[256,512]{1,0:T(8,128)(2,1)}, u32[]{:S(2)}) copy-start(bf16[256,512]{1,0:T(8,128)(2,1)} %get-tuple-element.16.own_ref) | copy-start | bytes 786436
  137.1 11.8 %copy-start.5 = (bf16[512,256]{1,0:T(8,128)(2,1)S(1)}, bf16[512,256]{1,0:T(8,128)(2,1)}, u32[]{:S(2)}) copy-start(bf16[512,256]{1,0:T(8,128)(2,1)} %get-tuple-element.27.refs_7_) | copy-start | bytes 786436
  137.1 11.8 %copy-start.6 = (bf16[512,256]{1,0:T(8,128)(2,1)S(1)}, bf16[512,256]{1,0:T(8,128)(2,1)}, u32[]{:S(2)}) copy-start(bf16[512,256]{1,0:T(8,128)(2,1)} %get-tuple-element.23.refs_8_) | copy-start | bytes 786436
  137.1 11.8 %copy-start.7 = (bf16[512,256]{1,0:T(8,128)(2,1)S(1)}, bf16[512,256]{1,0:T(8,128)(2,1)}, u32[]{:S(2)}) copy-start(bf16[512,256]{1,0:T(8,128)(2,1)} %get-tuple-element.19.refs_9_) | copy-start | bytes 786436
  137.1 11.8 %copy-start.13 = (f32[1,2048]{1,0:T(1,128)S(1)}, f32[1,2048]{1,0:T(1,128)}, u32[]{:S(2)}) copy-start(f32[1,2048]{1,0:T(1,128)} %get-tuple-element.31) | copy-start | bytes 24580
  137.1 11.8 %copy-start.19 = (f32[1,64]{1,0:T(1,128)S(1)}, f32[1,64]{1,0:T(1,128)}, u32[]{:S(2)}) copy-start(f32[1,64]{1,0:T(1,128)} %get-tuple-element.33.refs_6_) | copy-start | bytes 772
  137.2 11.8 %copy-start.20 = (f32[1,64]{1,0:T(1,128)S(1)}, f32[1,64]{1,0:T(1,128)}, u32[]{:S(2)}) copy-start(f32[1,64]{1,0:T(1,128)} %get-tuple-element.42.refs_5_) | copy-start | bytes 772
  139.0 7.8 %collective-permute-start.15 = (bf16[256,512]{1,0:T(8,128)(2,1)S(1)}, bf16[256,512]{1,0:T(8,128)(2,1)S(1)}, u32[]{:S(2)}, u32[]{:S(2)}) collective-permute-start(bf16[256,512]{1,0:T(8,128)(2,1)S(1)} %shard_map.120.refs_0_.r_ref), channel_id=1, source_target_pairs={{0,2},{1,3},{2,0},{3,1},{4,6},{5,7},{6,4},{7,5},{8,10},{9,11},{10,... | collective-permute-start | bytes 786440 | tf_op jit(solution)/shard_map/ppermute | solution.py:195
  139.6 8.2 %collective-permute-start.14 = (bf16[256,512]{1,0:T(8,128)(2,1)S(1)}, bf16[256,512]{1,0:T(8,128)(2,1)S(1)}, u32[]{:S(2)}, u32[]{:S(2)}) collective-permute-start(bf16[256,512]{1,0:T(8,128)(2,1)S(1)} %shard_map.120.refs_0_.r_ref), channel_id=1, source_target_pairs={{0,1},{1,0},{2,3},{3,2},{4,5},{5,4},{6,7},{7,6},{8,9},{9,8},{10,11... | collective-permute-start | bytes 786440 | tf_op jit(solution)/shard_map/ppermute | solution.py:195
  146.7 2.2 %collective-permute-start.16 = (bf16[256,512]{1,0:T(8,128)(2,1)S(1)}, bf16[256,512]{1,0:T(8,128)(2,1)S(1)}, u32[]{:S(2)}, u32[]{:S(2)}) collective-permute-start(bf16[256,512]{1,0:T(8,128)(2,1)S(1)} %collective-permute-done.15.refs_2_), channel_id=1, source_target_pairs={{0,1},{1,0},{2,3},{3,2},{4,5},{5,4},{6,7},{7,6},{8,9},{9,8},{10,11... | collective-permute-start | bytes 786440 | tf_op jit(solution)/shard_map/ppermute | solution.py:195
  148.9 23.5 %copy-start.18 = (s32[1,768]{1,0:T(1,128)S(1)}, s32[1,768]{1,0:T(1,128)}, u32[]{:S(2)}) copy-start(s32[1,768]{1,0:T(1,128)} %broadcast_in_dim.22.refs_4_) | copy-start | bytes 9220
  152.5 31.5 %copy-start.11 = (bf16[256,512]{1,0:T(8,128)(2,1)S(1)}, bf16[256,512]{1,0:T(8,128)(2,1)}, u32[]{:S(2)}) copy-start(bf16[256,512]{1,0:T(8,128)(2,1)} %get-tuple-element.15.own_ref) | copy-start | bytes 786436
  152.5 9.8 %collective-permute-start.18 = (bf16[256,512]{1,0:T(8,128)(2,1)S(1)}, bf16[256,512]{1,0:T(8,128)(2,1)S(1)}, u32[]{:S(2)}, u32[]{:S(2)}) collective-permute-start(bf16[256,512]{1,0:T(8,128)(2,1)S(1)} %get-tuple-element.14.refs_2_), channel_id=1, source_target_pairs={{0,4},{4,8},{8,12},{1,5},{5,9},{9,13},{2,6},{6,10},{10,14},{3,7},{... | collective-permute-start | bytes 786440 | tf_op jit(solution)/shard_map/ppermute | solution.py:20
  154.0 18.5 %collective-permute-start.17 = (bf16[256,512]{1,0:T(8,128)(2,1)S(1)}, bf16[256,512]{1,0:T(8,128)(2,1)S(1)}, u32[]{:S(2)}, u32[]{:S(2)}) collective-permute-start(bf16[256,512]{1,0:T(8,128)(2,1)S(1)} %get-tuple-element.14.refs_2_), channel_id=1, source_target_pairs={{0,8},{4,12},{1,9},{5,13},{2,10},{6,14},{3,11},{7,15},{16,24},{20,... | collective-permute-start | bytes 786440 | tf_op jit(solution)/shard_map/ppermute | solution.py:20
  185.8 7.8 %collective-permute-start.20 = (bf16[256,512]{1,0:T(8,128)(2,1)S(1)}, bf16[256,512]{1,0:T(8,128)(2,1)S(1)}, u32[]{:S(2)}, u32[]{:S(2)}) collective-permute-start(bf16[256,512]{1,0:T(8,128)(2,1)S(1)} %shard_map.123.refs_0_), channel_id=1, source_target_pairs={{0,2},{1,3},{2,0},{3,1},{4,6},{5,7},{6,4},{7,5},{8,10},{9,11},{10,... | collective-permute-start | bytes 786440 | tf_op jit(solution)/shard_map/ppermute | solution.py:195
  186.8 7.8 %collective-permute-start.19 = (bf16[256,512]{1,0:T(8,128)(2,1)S(1)}, bf16[256,512]{1,0:T(8,128)(2,1)S(1)}, u32[]{:S(2)}, u32[]{:S(2)}) collective-permute-start(bf16[256,512]{1,0:T(8,128)(2,1)S(1)} %shard_map.123.refs_0_), channel_id=1, source_target_pairs={{0,1},{1,0},{2,3},{3,2},{4,5},{5,4},{6,7},{7,6},{8,9},{9,8},{10,11... | collective-permute-start | bytes 786440 | tf_op jit(solution)/shard_map/ppermute | solution.py:195
  193.5 2.2 %collective-permute-start.21 = (bf16[256,512]{1,0:T(8,128)(2,1)S(1)}, bf16[256,512]{1,0:T(8,128)(2,1)S(1)}, u32[]{:S(2)}, u32[]{:S(2)}) collective-permute-start(bf16[256,512]{1,0:T(8,128)(2,1)S(1)} %collective-permute-done.20.refs_2_), channel_id=1, source_target_pairs={{0,1},{1,0},{2,3},{3,2},{4,5},{5,4},{6,7},{7,6},{8,9},{9,8},{10,11... | collective-permute-start | bytes 786440 | tf_op jit(solution)/shard_map/ppermute | solution.py:195
  (6 other events, 4.6 us)

commit v2 on v1

--- a/solution.py
+++ b/solution.py
@@ -173,18 +173,12 @@
     return lax.ppermute(value, "sp", [(ring[i], ring[(i + 1) % count]) for i in range(count)])
 
 
+def tie(value, *others):
+    return lax.optimization_barrier((value,) + others)[0]
+
+
 def swap_groups(value):
     return lax.ppermute(value, "grp", [(0, 1), (1, 0)])
-
-
-def gather_halves(half, ring):
-    from_ring, from_group = [], []
-    piece = half
-    for _ in range(len(ring) - 1):
-        piece = ring_step(piece, ring)
-        from_ring.append(piece)
-        from_group.append(swap_groups(piece))
-    return from_ring, from_group
 
 
 def exchange_columns(block, count):
@@ -322,14 +316,16 @@
     return call(kernel, order, operands, specs, [jax.ShapeDtypeStruct((rows, width), bf16)], [])[0]
 
 
-def output(attended, residual, own, pieces, layer, order, count):
+def output(attended, residual, own, pieces, order, count):
     rows, dims = attended.shape
     half = own.shape[0] // 2
     cols = own.shape[1]
     blocks = dims // half
     operands = [attended, residual, own] + list(pieces)
     specs = [full_spec(a) for a in operands[:3]]
-    specs += [window_spec((half, cols), (layer, 0)) for _ in pieces]
+    packed = pieces[0].shape[0] != half
+    shape = (2 * half, cols // 2) if packed else (half, cols)
+    specs += [window_spec(shape, (0, 0)) for _ in pieces]
 
     def kernel(order_ref, a_ref, r_ref, own_ref, *refs):
         piece_refs, (out_ref, xs) = refs[: len(pieces)], refs[len(pieces) :]
@@ -342,7 +338,10 @@
         for k in range(len(pieces)):
             src = order_ref[k // 2 + 1]
             part = grp if k % 2 == 0 else 1 - grp
-            acc += jnp.dot(xs[2 * src + part], piece_refs[k][...], preferred_element_type=f32)
+            weight = piece_refs[k][...]
+            if packed:
+                weight = jnp.concatenate([weight[:half], weight[half:]], axis=1)
+            acc += jnp.dot(xs[2 * src + part], weight, preferred_element_type=f32)
         out_ref[...] = (r_ref[...].astype(f32) + acc).astype(bf16)
 
     return call(
@@ -407,42 +406,70 @@
     def half_of(weight, size):
         return lax.dynamic_slice_in_dim(weight, grp * size, size, 0)
 
-    first = jnp.concatenate(
-        [half_of(w[0], in_half) for w in (query_weight, key_weight, value_weight)], axis=1
-    )
-    outs = jnp.concatenate([half_of(out_weight[l], out_half) for l in range(LAYERS)], axis=0)
-    second = jnp.concatenate(
-        [outs] + [half_of(w[1], in_half) for w in (query_weight, key_weight, value_weight)], axis=1
-    )
-    a_ring, a_group = gather_halves(first, ring)
-    second, _ = lax.optimization_barrier((second, a_ring[-1]))
-    b_ring, b_group = gather_halves(second, ring)
-    a_pieces = interleave(a_ring, a_group)
-    b_pieces = interleave(b_ring, b_group)
-
-    all_docs = lax.all_gather(doc_ids, "sp", axis=0, tiled=True)
-    padded = jnp.concatenate([jnp.full((reach,), -1, jnp.int32), all_docs])
-    doc_row = lax.dynamic_slice_in_dim(padded, place * rows, reach + rows, 0)[None, :]
+    def joined(layer):
+        shards = (query_weight, key_weight, value_weight)
+        return jnp.concatenate([half_of(w[layer], in_half) for w in shards], axis=1)
+
+    first = joined(0)
+    out_first = half_of(out_weight[0], out_half)
+    a_ring, a_group = [ring_step(first, ring)], []
+    own_next = half_of(out_weight[1], out_half)
+    own_next = jnp.concatenate([own_next[:, : cols // 2], own_next[:, cols // 2 :]], axis=0)
+    second = jnp.concatenate([own_next, joined(1)], axis=1)
+    second = tie(second, a_ring[0])
+    docs = [tie(doc_ids, a_ring[0])]
+    docs = [shifted(docs[0], "sp", back) for back in range(depth, 0, -1)] + docs
+    for step in range(1, count - 1):
+        source = tie(a_ring[-1], *a_group[-1:], *(docs if step > 1 else [second]))
+        a_group.append(swap_groups(a_ring[-1]))
+        a_ring.append(ring_step(source, ring))
+    last, base = a_ring[-1], a_group[-1]
+    a_group.append(swap_groups(tie(last, base)))
+    c_ring, c_group = [ring_step(tie(second, last, base), ring)], []
+    doc_row = jnp.concatenate(docs)[None, :]
     doc_col = doc_ids[:, None]
     flat = flat_biases(rel_bias, rows)
 
-    residual = lax.dynamic_slice_in_dim(stream, t * cols, cols, 1)
+    residual = tie(lax.dynamic_slice_in_dim(stream, t * cols, cols, 1), a_ring[0])
     x_pieces = [stream]
+    piece_cols = own_next.shape[1]
     for layer in range(LAYERS):
         own = [w[layer] for w in (query_weight, key_weight, value_weight)]
-        pieces = a_pieces if layer == 0 else b_pieces
-        col = 0 if layer == 0 else cols // own[0].shape[1]
+        ring_pieces, group_pieces = (a_ring, a_group) if layer == 0 else (c_ring, c_group)
+        col = 0 if layer == 0 else piece_cols // own[0].shape[1]
         query, kv = project(
             x_pieces, norm_gain[layer], query_gain[layer][None], key_gain[layer][None],
-            own, pieces, col, order, count,
+            own, interleave(ring_pieces, group_pieces), col,
+            tie(order, c_ring[0]) if layer == 0 else order, count,
         )
         received = [shifted(kv, "sp", back) for back in range(depth, 0, -1)]
+        attend_order = out_order = order
+        if layer == 0:
+            o_ring, o_group = [ring_step(tie(out_first, kv), ring)], []
+            c_group.append(swap_groups(tie(c_ring[0], kv)))
+            for step in range(1, count - 1):
+                near = received[-1] if step == 1 else o_group[-1]
+                o_group.append(swap_groups(tie(o_ring[-1], near)))
+                o_ring.append(ring_step(tie(o_ring[-1], near), ring))
+            attend_order = tie(order, o_ring[-1], o_group[-1], c_group[-1])
+            o_group.append(swap_groups(tie(o_ring[-1], attend_order)))
+            c_ring.append(ring_step(tie(c_ring[0], received[0], attend_order), ring))
         attended = attend_kernel(
-            query, received + [kv], doc_col, doc_row, flat, order, count, head_size
+            query, received + [kv], doc_col, doc_row, flat, attend_order, count, head_size
         )
         all_heads = lax.all_gather(attended, "tp", axis=1, tiled=True)
-        block = output(all_heads, residual, out_weight[layer], b_pieces, layer, order, count)
+        if layer == 0:
+            out_order = tie(order, c_ring[-1])
+            for step in range(2, count - 1):
+                c_group.append(swap_groups(tie(c_ring[-1], all_heads)))
+                c_ring.append(ring_step(tie(c_ring[-1], all_heads), ring))
+            o_pieces = interleave(o_ring, o_group)
+        else:
+            o_pieces = interleave(c_ring, c_group)
+        block = output(all_heads, residual, out_weight[layer], o_pieces, out_order, count)
         x_pieces = exchange_columns(block, tp_count)
+        if layer == 0:
+            c_group.append(swap_groups(c_ring[-1]))
         residual = block
     return assemble(x_pieces, order, count)
 
@@ -455,10 +482,10 @@
     out_rows, cols = out_weight.shape[1:]
     fits = (
         lax.axis_size("grp") == 2 and LAYERS == 2
-        and 2 < count <= 4 and tp_count & (tp_count - 1) == 0
+        and count == 4 and tp_count & (tp_count - 1) == 0
         and in_rows % 256 == 0 and out_rows % 256 == 0
         and 2 * (out_rows // 2) == in_rows // 2
-        and width % 128 == 0 and cols % width == 0
+        and width % 128 == 0 and cols % (2 * width) == 0
         and cols % (in_rows // 2) == 0 and tp_count > 1
         and rows <= MAXREL and (LEFT * SEG) % rows == 0 and rows % SEG == 0
     )

time: 198 us -> 188 us (0.949)
  the two profiles are of different devices: /device:TPU:25 before, /device:TPU:17 now
where the time goes in v2:
time: 188 us; the launch traced here: 187 us
  waiting for transfers between devices  81.8 us (44%)
  starting transfers between devices  42.2 us (22%)
  blocking collectives  26.8 us (14%)
  Pallas kernels  19.4 us (10%)
  local copies, waits for them, and re-layouts  15 us (8%)
    ppermute x9, waiting for transfers between devices, ring_step(): lax.ppermute(value, 'sp', [(ring[i], ring[(i + 1) % count]) for i in rang...  40.3 us
    all_gather x2, blocking collectives, on_device_fast(): all_heads = lax.all_gather(attended, 'tp', axis=1, tiled=True)  26.8 us
    pallas_call x7, Pallas kernels, call(): pl.pallas_call(kernel, grid=(1,), in_specs=[pl.BlockSpec(memory_space=SME...  19.4 us
    ppermute x9, starting transfers between devices, ring_step(): lax.ppermute(value, 'sp', [(ring[i], ring[(i + 1) % count]) for i in rang...  17.6 us
    ppermute x6, waiting for transfers between devices, shifted(): lax.ppermute(value, axis, [(source, source + steps) for source in range(i...  16.6 us
    ppermute x9, waiting for transfers between devices, swap_groups(): return lax.ppermute(value, 'grp', [(0, 1), (1, 0)])  15.5 us
    ppermute x6, starting transfers between devices, shifted(): lax.ppermute(value, axis, [(source, source + steps) for source in range(i...  10.7 us
    ppermute x9, starting transfers between devices, swap_groups(): return lax.ppermute(value, 'grp', [(0, 1), (1, 0)])  9.86 us
  transfers between devices with their start and end apart: 30, of which 18 were waited for; matrix products, arithmetic and copies ran while one was open for 4% of the time, Pallas kernels for 3%

profile of v2, /device:TPU:17, one launch (start us, length us, event | category | flops | bytes accessed | tf_op | source)
XLA Modules:
  0.0 187.2 jit_solution(773290755957723109)
XLA Ops:
  0.0 2.0 %slice_bitcast_fusion.4 = (bf16[512,256]{1,0:T(8,128)(2,1)}, bf16[512,256]{1,0:T(8,128)(2,1)}, bf16[1,512,256]{2,1,0:T(8,128)(2,1)S(1)}, bf16[1,512,256]{2,1,0:T(8,128)(2,1)S(1)}) fusion(bf16[2,512,256]{2,1,0:T(8,128)(2,1)} %param.17), kind=kLoop, calls=%fused_computation.27 | loop fusion | bytes 1572864 | tf_op jit(solution)/shard_map/squeeze | solution.py:411
  4.2 1.3 collective-permute-start
  5.6 1.0 slice_bitcast_fusion.7
  7.5 7.6 %collective-permute-done.refs_7_.refs_8_.refs_9_ = bf16[256,768]{1,0:T(8,128)(2,1)S(1)} collective-permute-done((bf16[256,768]{1,0:T(8,128)(2,1)S(1)}, bf16[256,768]{1,0:T(8,128)(2,1)S(1)}, u32[]{:S(2)}, u32[]{:S(2)}) %collective-permute-start) | collective-permute-done | bytes 393248 | tf_op jit(solution)/shard_map/ppermute | solution.py:173
  15.5 1.2 collective-permute-start.2
  16.8 1.3 collective-permute-start.3
  18.1 2.9 %collective-permute-start.4 = (s32[256]{0:T(256)S(1)}, s32[256]{0:T(256)S(1)}, u32[]{:S(2)}, u32[]{:S(2)}) collective-permute-start(s32[256]{0:T(256)S(1)} %copy-done.24), channel_id=1, source_target_pairs={{0,4},{4,8},{8,12},{1,5},{5,9},{9,13},{2,6},{6,10},{10,14},{3,7},{... | collective-permute-start | bytes 3080 | tf_op jit(solution)/shard_map/ppermute | solution.py:20
  22.2 3.0 %collective-permute-done.3 = s32[256]{0:T(256)S(1)} collective-permute-done((s32[256]{0:T(256)S(1)}, s32[256]{0:T(256)S(1)}, u32[]{:S(2)}, u32[]{:S(2)}) %collective-permute-start.3) | collective-permute-done | bytes 1056 | tf_op jit(solution)/shard_map/ppermute | solution.py:20
  25.4 1.2 collective-permute-start.6
  28.5 5.9 %collective-permute-done.5.refs_19_.refs_20_.refs_21_ = bf16[256,768]{1,0:T(8,128)(2,1)S(1)} collective-permute-done((bf16[256,768]{1,0:T(8,128)(2,1)S(1)}, bf16[256,768]{1,0:T(8,128)(2,1)S(1)}, u32[]{:S(2)}, u32[]{:S(2)}) %collective-permute-start.5) | collective-permute-done | bytes 393248 | tf_op jit(solution)/shard_map/ppermute | solution.py:173
  34.5 1.6 collective-permute-start.8
  36.1 1.4 fusion.3
  37.5 8.1 %collective-permute-done.7.refs_10_.refs_11_.refs_12_.refs_0_ = bf16[256,1024]{1,0:T(8,128)(2,1)S(1)} collective-permute-done((bf16[256,1024]{1,0:T(8,128)(2,1)}, bf16[256,1024]{1,0:T(8,128)(2,1)S(1)}, u32[]{:S(2)}, u32[]{:S(2)}) %collective-permute-start.7) | collective-permute-done | bytes 524320 | tf_op jit(solution)/shard_map/ppermute | solution.py:173
  45.7 0.9 copy-done.3
  46.6 0.9 copy-done.4
  47.6 0.9 copy-done.5
  48.5 3.8 %shard_map.118 = (bf16[256,256]{1,0:T(8,128)(2,1)S(1)}, bf16[256,512]{1,0:T(8,128)(2,1)}) custom-call(s32[6]{0:T(128)S(1)} %pad_add_fusion.1.order_ref, bf16[256,2048]{1,0:T(8,128)(2,1)S(1)} %copy-done, f32[8,1,256]{2,1,0:T(1,128)S(1)} %bitcast.41, f32[1,64]{1,0:T(1,128)S(1)} %get-tuple-element.75.refs_2_, f32[1,64]{1,0:T(1,128)S(1)} %get-tuple-element.68.refs_3_, ...), custom_call_target="tpu_custom_call" | custom-call | tf_op jit(solution)/shard_map/pallas_call | solution.py:203
  52.3 1.9 %collective-permute-start.11 = (bf16[256,512]{1,0:T(8,128)(2,1)}, bf16[256,512]{1,0:T(8,128)(2,1)S(1)}, u32[]{:S(2)}, u32[]{:S(2)}) collective-permute-start(bf16[256,512]{1,0:T(8,128)(2,1)} %get-tuple-element.33.refs_2_), channel_id=1, source_target_pairs={{0,4},{4,8},{8,12},{1,5},{5,9},{9,13},{2,6},{6,10},{10,14},{3,7},{... | collective-permute-start | bytes 786440 | tf_op jit(solution)/shard_map/ppermute | solution.py:20
  54.2 1.3 collective-permute-start.16
  55.6 4.8 %collective-permute-done.10.refs_0_ = bf16[128,512]{1,0:T(8,128)(2,1)S(1)} collective-permute-done((bf16[128,512]{1,0:T(8,128)(2,1)S(1)}, bf16[128,512]{1,0:T(8,128)(2,1)S(1)}, u32[]{:S(2)}, u32[]{:S(2)}) %collective-permute-start.10) | collective-permute-done | bytes 131104 | tf_op jit(solution)/shard_map/ppermute | solution.py:173
  61.3 1.2 collective-permute-start.13
  62.5 1.3 collective-permute-start.9
  63.8 3.0 %collective-permute-done.12.refs_2_ = bf16[128,512]{1,0:T(8,128)(2,1)S(1)} collective-permute-done((bf16[128,512]{1,0:T(8,128)(2,1)S(1)}, bf16[128,512]{1,0:T(8,128)(2,1)S(1)}, u32[]{:S(2)}, u32[]{:S(2)}) %collective-permute-start.12) | collective-permute-done | bytes 131104 | tf_op jit(solution)/shard_map/ppermute | solution.py:173
  69.3 4.0 %collective-permute-done.14.refs_4_ = bf16[128,512]{1,0:T(8,128)(2,1)S(1)} collective-permute-done((bf16[128,512]{1,0:T(8,128)(2,1)S(1)}, bf16[128,512]{1,0:T(8,128)(2,1)S(1)}, u32[]{:S(2)}, u32[]{:S(2)}) %collective-permute-start.14) | collective-permute-done | bytes 131104 | tf_op jit(solution)/shard_map/ppermute | solution.py:173
  73.2 14.5 %collective-permute-start.17 = (bf16[256,1024]{1,0:T(8,128)(2,1)S(1)}, bf16[256,1024]{1,0:T(8,128)(2,1)S(1)}, u32[]{:S(2)}, u32[]{:S(2)}) collective-permute-start(bf16[256,1024]{1,0:T(8,128)(2,1)S(1)} %collective-permute-done.7.refs_10_.refs_11_.refs_12_.refs_0_), channel_id=1, source_target_pairs={{0,8},{8,12},{12,4},{4,0},{1,9},{9,13},{13,5},{5,1},{2,10},{10,14}... | collective-permute-start | bytes 1572872 | tf_op jit(solution)/shard_map/ppermute | solution.py:173
  88.6 4.4 %shard_map.119 = bf16[256,256]{1,0:T(8,128)(2,1)S(1)} custom-call(s32[6]{0:T(128)S(1)} %pad_add_fusion.1.order_ref, bf16[256,256]{1,0:T(8,128)(2,1)S(1)} %copy-done.10, bf16[256,512]{1,0:T(8,128)(2,1)S(1)} %collective-permute-done.9.refs_0_, bf16[256,512]{1,0:T(8,128)(2,1)S(1)} %collective-permute-done.11.refs_1_, ...), custom_call_target="tpu_custom_call" | custom-call | tf_op jit(solution)/shard_map/pallas_call | solution.py:203
  93.1 15.6 %all_gather.6.a_ref = bf16[256,1024]{1,0:T(8,128)(2,1)S(1)} all-gather(bf16[256,256]{1,0:T(8,128)(2,1)S(1)} %shard_map.119), channel_id=1, replica_groups=mesh['grp'=2,'sp'=4,'tp'=4] {'tp'}, dimensions={1}, use_global_device_ids=true | all-gather | bytes 655360 | tf_op jit(solution)/shard_map/all_gather | solution.py:460
  108.7 0.9 collective-permute-start.18
  109.6 1.0 constant_dynamic-slice_fusion.r_ref
  110.7 3.0 %collective-permute-done.18.refs_5_ = bf16[128,512]{1,0:T(8,128)(2,1)S(1)} collective-permute-done((bf16[128,512]{1,0:T(8,128)(2,1)S(1)}, bf16[128,512]{1,0:T(8,128)(2,1)S(1)}, u32[]{:S(2)}, u32[]{:S(2)}) %collective-permute-start.18) | collective-permute-done | bytes 131104 | tf_op jit(solution)/shard_map/ppermute | solution.py:181
  113.7 1.3 shard_map.120.refs_0_.r_ref
  116.1 6.8 %collective-permute-done.23.refs_22_.refs_23_.refs_24_.refs_4_ = bf16[256,1024]{1,0:T(8,128)(2,1)S(1)} collective-permute-done((bf16[256,1024]{1,0:T(8,128)(2,1)S(1)}, bf16[256,1024]{1,0:T(8,128)(2,1)S(1)}, u32[]{:S(2)}, u32[]{:S(2)}) %collective-permute-start.23) | collective-permute-done | bytes 524320 | tf_op jit(solution)/shard_map/ppermute | solution.py:173
  123.8 1.3 collective-permute-start.19
  125.1 1.2 collective-permute-done.19.refs_1_
  126.7 1.2 collective-permute-done.22.refs_19_.refs_20_.refs_21_.refs_3_
  127.9 11.2 %collective-permute-done.24.refs_25_.refs_26_.refs_27_.refs_5_ = bf16[256,1024]{1,0:T(8,128)(2,1)S(1)} collective-permute-done((bf16[256,1024]{1,0:T(8,128)(2,1)S(1)}, bf16[256,1024]{1,0:T(8,128)(2,1)S(1)}, u32[]{:S(2)}, u32[]{:S(2)}) %collective-permute-start.24) | collective-permute-done | bytes 524320 | tf_op jit(solution)/shard_map/ppermute | solution.py:181
  139.7 2.9 %shard_map.121 = (bf16[256,256]{1,0:T(8,128)(2,1)S(1)}, bf16[256,512]{1,0:T(8,128)(2,1)S(1)}) custom-call(s32[6]{0:T(128)S(1)} %copy-done.13, bf16[256,512]{1,0:T(8,128)(2,1)S(1)} %shard_map.120.refs_0_.r_ref, bf16[256,512]{1,0:T(8,128)(2,1)S(1)} %collective-permute-done.19.refs_1_, bf16[256,512]{1,0:T(8,128)(2,1)S(1)} %collective-permute-done.20.refs_2_, ...), custom_call_target="tpu_custom_call" | custom-call | tf_op jit(solution)/shard_map/pallas_call | solution.py:203
  142.7 1.3 collective-permute-start.25
  144.0 2.1 %collective-permute-start.26 = (bf16[256,512]{1,0:T(8,128)(2,1)S(1)}, bf16[256,512]{1,0:T(8,128)(2,1)S(1)}, u32[]{:S(2)}, u32[]{:S(2)}) collective-permute-start(bf16[256,512]{1,0:T(8,128)(2,1)S(1)} %get-tuple-element.46.refs_2_), channel_id=1, source_target_pairs={{0,4},{4,8},{8,12},{1,5},{5,9},{9,13},{2,6},{6,10},{10,14},{3,7},{... | collective-permute-start | bytes 786440 | tf_op jit(solution)/shard_map/ppermute | solution.py:20
  146.1 5.2 %collective-permute-done.25.refs_0_ = bf16[256,512]{1,0:T(8,128)(2,1)S(1)} collective-permute-done((bf16[256,512]{1,0:T(8,128)(2,1)S(1)}, bf16[256,512]{1,0:T(8,128)(2,1)S(1)}, u32[]{:S(2)}, u32[]{:S(2)}) %collective-permute-start.25) | collective-permute-done | bytes 262176 | tf_op jit(solution)/shard_map/ppermute | solution.py:20
  151.3 7.8 %collective-permute-done.26.refs_1_ = bf16[256,512]{1,0:T(8,128)(2,1)S(1)} collective-permute-done((bf16[256,512]{1,0:T(8,128)(2,1)S(1)}, bf16[256,512]{1,0:T(8,128)(2,1)S(1)}, u32[]{:S(2)}, u32[]{:S(2)}) %collective-permute-start.26) | collective-permute-done | bytes 262176 | tf_op jit(solution)/shard_map/ppermute | solution.py:20
  159.1 4.0 %shard_map.122 = bf16[256,256]{1,0:T(8,128)(2,1)S(1)} custom-call(s32[6]{0:T(128)S(1)} %copy-done.13, bf16[256,256]{1,0:T(8,128)(2,1)S(1)} %get-tuple-element.45.q_ref, bf16[256,512]{1,0:T(8,128)(2,1)S(1)} %collective-permute-done.25.refs_0_, bf16[256,512]{1,0:T(8,128)(2,1)S(1)} %collective-permute-done.26.refs_1_, ...), custom_call_target="tpu_custom_call" | custom-call | tf_op jit(solution)/shard_map/pallas_call | solution.py:203
  163.2 11.1 %all_gather.7.a_ref = bf16[256,1024]{1,0:T(8,128)(2,1)S(1)} all-gather(bf16[256,256]{1,0:T(8,128)(2,1)S(1)} %shard_map.122), channel_id=1, replica_groups=mesh['grp'=2,'sp'=4,'tp'=4] {'tp'}, dimensions={1}, use_global_device_ids=true | all-gather | bytes 655360 | tf_op jit(solution)/shard_map/all_gather | solution.py:460
  174.3 1.3 shard_map.123.refs_0_
  176.7 6.7 %collective-permute-done.28.refs_2_ = bf16[256,512]{1,0:T(8,128)(2,1)S(1)} collective-permute-done((bf16[256,512]{1,0:T(8,128)(2,1)S(1)}, bf16[256,512]{1,0:T(8,128)(2,1)S(1)}, u32[]{:S(2)}, u32[]{:S(2)}) %collective-permute-start.28) | collective-permute-done | bytes 262176 | tf_op jit(solution)/shard_map/ppermute | solution.py:189
  183.4 1.0 collective-permute-start.29
  184.4 1.2 collective-permute-done.29.refs_3_
  185.6 1.6 shard_map.124
  (111 shorter events, 15.1 us)
Async XLA Ops:
  4.2 11.0 %collective-permute-start = (bf16[256,768]{1,0:T(8,128)(2,1)S(1)}, bf16[256,768]{1,0:T(8,128)(2,1)S(1)}, u32[]{:S(2)}, u32[]{:S(2)}) collective-permute-start(bf16[256,768]{1,0:T(8,128)(2,1)S(1)} %pad_maximum_fusion.1), channel_id=1, source_target_pairs={{0,8},{8,12},{12,4},{4,0},{1,9},{9,13},{13,5},{5,1},{2,10},{10,14}... | collective-permute-start | bytes 1179656 | tf_op jit(solution)/shard_map/ppermute | solution.py:173
  6.6 39.1 %copy-start = (bf16[256,2048]{1,0:T(8,128)(2,1)S(1)}, bf16[256,2048]{1,0:T(8,128)(2,1)}, u32[]{:S(2)}) copy-start(bf16[256,2048]{1,0:T(8,128)(2,1)} %refs_0_.1) | copy-start | bytes 3145732
  6.6 10.2 %copy-start.24 = (s32[256]{0:T(256)S(1)}, s32[256]{0:T(256)}, u32[]{:S(2)}) copy-start(s32[256]{0:T(256)} %param.13) | copy-start | bytes 3076
  6.6 20.6 %copy-start.18 = (s32[4]{0:T(128)S(1)}, s32[4]{0:T(128)}, u32[]{:S(2)}) copy-start(s32[4]{0:T(128)} %constant.52.clone) | copy-start | bytes 52
  15.1 10.1 %collective-permute-start.1 = (bf16[256,768]{1,0:T(8,128)(2,1)S(1)}, bf16[256,768]{1,0:T(8,128)(2,1)S(1)}, u32[]{:S(2)}, u32[]{:S(2)}) collective-permute-start(bf16[256,768]{1,0:T(8,128)(2,1)S(1)} %collective-permute-done.refs_7_.refs_8_.refs_9_), channel_id=1, source_target_pairs={{0,8},{8,12},{12,4},{4,0},{1,9},{9,13},{13,5},{5,1},{2,10},{10,14}... | collective-permute-start | bytes 1179656 | tf_op jit(solution)/shard_map/ppermute | solution.py:173
  15.5 9.7 %collective-permute-start.2 = (bf16[256,768]{1,0:T(8,128)(2,1)S(1)}, bf16[256,768]{1,0:T(8,128)(2,1)S(1)}, u32[]{:S(2)}, u32[]{:S(2)}) collective-permute-start(bf16[256,768]{1,0:T(8,128)(2,1)S(1)} %collective-permute-done.refs_7_.refs_8_.refs_9_), channel_id=1, source_target_pairs={{0,16},{16,0},{1,17},{17,1},{2,18},{18,2},{3,19},{19,3},{4,20},{20... | collective-permute-start | bytes 1179656 | tf_op jit(solution)/shard_map/ppermute | solution.py:181
  16.8 8.4 %collective-permute-start.3 = (s32[256]{0:T(256)S(1)}, s32[256]{0:T(256)S(1)}, u32[]{:S(2)}, u32[]{:S(2)}) collective-permute-start(s32[256]{0:T(256)S(1)} %copy-done.24), channel_id=1, source_target_pairs={{0,8},{4,12},{1,9},{5,13},{2,10},{6,14},{3,11},{7,15},{16,24},{20,... | collective-permute-start | bytes 3080 | tf_op jit(solution)/shard_map/ppermute | solution.py:20
  18.1 7.1 %collective-permute-start.4 = (s32[256]{0:T(256)S(1)}, s32[256]{0:T(256)S(1)}, u32[]{:S(2)}, u32[]{:S(2)}) collective-permute-start(s32[256]{0:T(256)S(1)} %copy-done.24), channel_id=1, source_target_pairs={{0,4},{4,8},{8,12},{1,5},{5,9},{9,13},{2,6},{6,10},{10,14},{3,7},{... | collective-permute-start | bytes 3080 | tf_op jit(solution)/shard_map/ppermute | solution.py:20
  25.2 2.0 %copy-start.25 = (s32[256]{0:T(256)}, s32[256]{0:T(256)S(1)}, u32[]{:S(2)}) copy-start(s32[256]{0:T(256)S(1)} %collective-permute-done.4) | copy-start | bytes 3076
  25.2 9.2 %collective-permute-start.5 = (bf16[256,768]{1,0:T(8,128)(2,1)S(1)}, bf16[256,768]{1,0:T(8,128)(2,1)S(1)}, u32[]{:S(2)}, u32[]{:S(2)}) collective-permute-start(bf16[256,768]{1,0:T(8,128)(2,1)S(1)} %collective-permute-done.1.refs_13_.refs_14_.refs_15_), channel_id=1, source_target_pairs={{0,8},{8,12},{12,4},{4,0},{1,9},{9,13},{13,5},{5,1},{2,10},{10,14}... | collective-permute-start | bytes 1179656 | tf_op jit(solution)/shard_map/ppermute | solution.py:173
  25.4 9.0 %collective-permute-start.6 = (bf16[256,768]{1,0:T(8,128)(2,1)S(1)}, bf16[256,768]{1,0:T(8,128)(2,1)S(1)}, u32[]{:S(2)}, u32[]{:S(2)}) collective-permute-start(bf16[256,768]{1,0:T(8,128)(2,1)S(1)} %collective-permute-done.1.refs_13_.refs_14_.refs_15_), channel_id=1, source_target_pairs={{0,16},{16,0},{1,17},{17,1},{2,18},{18,2},{3,19},{19,3},{4,20},{20... | collective-permute-start | bytes 1179656 | tf_op jit(solution)/shard_map/ppermute | solution.py:181
  34.4 11.3 %collective-permute-start.7 = (bf16[256,1024]{1,0:T(8,128)(2,1)}, bf16[256,1024]{1,0:T(8,128)(2,1)S(1)}, u32[]{:S(2)}, u32[]{:S(2)}) collective-permute-start(bf16[256,1024]{1,0:T(8,128)(2,1)} %pad_maximum_fusion), channel_id=1, source_target_pairs={{0,8},{8,12},{12,4},{4,0},{1,9},{9,13},{13,5},{5,1},{2,10},{10,14}... | collective-permute-start | bytes 1572872 | tf_op jit(solution)/shard_map/ppermute | solution.py:173
  34.5 54.1 %copy-start.12 = (s32[6]{0:T(128)}, s32[6]{0:T(128)S(1)}, u32[]{:S(2)}) copy-start(s32[6]{0:T(128)S(1)} %pad_add_fusion.1.order_ref) | copy-start | bytes 76
  34.5 11.2 %collective-permute-start.8 = (bf16[256,768]{1,0:T(8,128)(2,1)S(1)}, bf16[256,768]{1,0:T(8,128)(2,1)S(1)}, u32[]{:S(2)}, u32[]{:S(2)}) collective-permute-start(bf16[256,768]{1,0:T(8,128)(2,1)S(1)} %collective-permute-done.5.refs_19_.refs_20_.refs_21_), channel_id=1, source_target_pairs={{0,16},{16,0},{1,17},{17,1},{2,18},{18,2},{3,19},{19,3},{4,20},{20... | collective-permute-start | bytes 1179656 | tf_op jit(solution)/shard_map/ppermute | solution.py:181
  48.5 7.0 %copy-start.19 = (bf16[1,256,512]{2,1,0:T(8,128)(2,1)S(1)}, bf16[1,256,512]{2,1,0:T(8,128)(2,1)}, u32[]{:S(2)}) copy-start(bf16[1,256,512]{2,1,0:T(8,128)(2,1)} %get-tuple-element.49) | copy-start | bytes 786436
  52.3 3.2 %copy-start.9 = (bf16[256,256]{1,0:T(8,128)(2,1)}, bf16[256,256]{1,0:T(8,128)(2,1)S(1)}, u32[]{:S(2)}) copy-start(bf16[256,256]{1,0:T(8,128)(2,1)S(1)} %get-tuple-element.41.q_ref) | copy-start | bytes 393220
  52.3 8.7 %collective-permute-start.11 = (bf16[256,512]{1,0:T(8,128)(2,1)}, bf16[256,512]{1,0:T(8,128)(2,1)S(1)}, u32[]{:S(2)}, u32[]{:S(2)}) collective-permute-start(bf16[256,512]{1,0:T(8,128)(2,1)} %get-tuple-element.33.refs_2_), channel_id=1, source_target_pairs={{0,4},{4,8},{8,12},{1,5},{5,9},{9,13},{2,6},{6,10},{10,14},{3,7},{... | collective-permute-start | bytes 786440 | tf_op jit(solution)/shard_map/ppermute | solution.py:20
  54.2 19.0 %collective-permute-start.16 = (bf16[256,1024]{1,0:T(8,128)(2,1)S(1)}, bf16[256,1024]{1,0:T(8,128)(2,1)S(1)}, u32[]{:S(2)}, u32[]{:S(2)}) collective-permute-start(bf16[256,1024]{1,0:T(8,128)(2,1)S(1)} %collective-permute-done.7.refs_10_.refs_11_.refs_12_.refs_0_), channel_id=1, source_target_pairs={{0,16},{16,0},{1,17},{17,1},{2,18},{18,2},{3,19},{19,3},{4,20},{20... | collective-permute-start | bytes 1572872 | tf_op jit(solution)/shard_map/ppermute | solution.py:181
  55.5 13.3 %copy-start.23 = (f32[4,513]{1,0:T(4,128)S(1)}, f32[4,513]{1,0:T(4,128)}, u32[]{:S(2)}) copy-start(f32[4,513]{1,0:T(4,128)} %param.21) | copy-start | bytes 24628
  55.5 4.9 %collective-permute-start.10 = (bf16[128,512]{1,0:T(8,128)(2,1)S(1)}, bf16[128,512]{1,0:T(8,128)(2,1)S(1)}, u32[]{:S(2)}, u32[]{:S(2)}) collective-permute-start(bf16[128,512]{1,0:T(8,128)(2,1)S(1)} %dynamic-slice_bitcast_fusion), channel_id=1, source_target_pairs={{0,8},{8,12},{12,4},{4,0},{1,9},{9,13},{13,5},{5,1},{2,10},{10,14}... | collective-permute-start | bytes 393224 | tf_op jit(solution)/shard_map/ppermute | solution.py:173
  55.6 33.0 %copy-start.10 = (bf16[256,256]{1,0:T(8,128)(2,1)S(1)}, bf16[256,256]{1,0:T(8,128)(2,1)}, u32[]{:S(2)}) copy-start(bf16[256,256]{1,0:T(8,128)(2,1)} %copy-done.9) | copy-start | bytes 393220
  61.0 5.9 %collective-permute-start.12 = (bf16[128,512]{1,0:T(8,128)(2,1)S(1)}, bf16[128,512]{1,0:T(8,128)(2,1)S(1)}, u32[]{:S(2)}, u32[]{:S(2)}) collective-permute-start(bf16[128,512]{1,0:T(8,128)(2,1)S(1)} %collective-permute-done.10.refs_0_), channel_id=1, source_target_pairs={{0,8},{8,12},{12,4},{4,0},{1,9},{9,13},{13,5},{5,1},{2,10},{10,14}... | collective-permute-start | bytes 393224 | tf_op jit(solution)/shard_map/ppermute | solution.py:173
  61.3 5.6 %collective-permute-start.13 = (bf16[128,512]{1,0:T(8,128)(2,1)S(1)}, bf16[128,512]{1,0:T(8,128)(2,1)S(1)}, u32[]{:S(2)}, u32[]{:S(2)}) collective-permute-start(bf16[128,512]{1,0:T(8,128)(2,1)S(1)} %collective-permute-done.10.refs_0_), channel_id=1, source_target_pairs={{0,16},{16,0},{1,17},{17,1},{2,18},{18,2},{3,19},{19,3},{4,20},{20... | collective-permute-start | bytes 393224 | tf_op jit(solution)/shard_map/ppermute | solution.py:181
  62.5 10.7 %collective-permute-start.9 = (bf16[256,512]{1,0:T(8,128)(2,1)}, bf16[256,512]{1,0:T(8,128)(2,1)S(1)}, u32[]{:S(2)}, u32[]{:S(2)}) collective-permute-start(bf16[256,512]{1,0:T(8,128)(2,1)} %get-tuple-element.33.refs_2_), channel_id=1, source_target_pairs={{0,8},{4,12},{1,9},{5,13},{2,10},{6,14},{3,11},{7,15},{16,24},{20,... | collective-permute-start | bytes 786440 | tf_op jit(solution)/shard_map/ppermute | solution.py:20
  66.9 6.3 %collective-permute-start.14 = (bf16[128,512]{1,0:T(8,128)(2,1)S(1)}, bf16[128,512]{1,0:T(8,128)(2,1)S(1)}, u32[]{:S(2)}, u32[]{:S(2)}) collective-permute-start(bf16[128,512]{1,0:T(8,128)(2,1)S(1)} %collective-permute-done.12.refs_2_), channel_id=1, source_target_pairs={{0,8},{8,12},{12,4},{4,0},{1,9},{9,13},{13,5},{5,1},{2,10},{10,14}... | collective-permute-start | bytes 393224 | tf_op jit(solution)/shard_map/ppermute | solution.py:173
  67.8 5.5 %collective-permute-start.15 = (bf16[128,512]{1,0:T(8,128)(2,1)S(1)}, bf16[128,512]{1,0:T(8,128)(2,1)S(1)}, u32[]{:S(2)}, u32[]{:S(2)}) collective-permute-start(bf16[128,512]{1,0:T(8,128)(2,1)S(1)} %collective-permute-done.12.refs_2_), channel_id=1, source_target_pairs={{0,16},{16,0},{1,17},{17,1},{2,18},{18,2},{3,19},{19,3},{4,20},{20... | collective-permute-start | bytes 393224 | tf_op jit(solution)/shard_map/ppermute | solution.py:181
  73.2 35.5 %collective-permute-start.17 = (bf16[256,1024]{1,0:T(8,128)(2,1)S(1)}, bf16[256,1024]{1,0:T(8,128)(2,1)S(1)}, u32[]{:S(2)}, u32[]{:S(2)}) collective-permute-start(bf16[256,1024]{1,0:T(8,128)(2,1)S(1)} %collective-permute-done.7.refs_10_.refs_11_.refs_12_.refs_0_), channel_id=1, source_target_pairs={{0,8},{8,12},{12,4},{4,0},{1,9},{9,13},{13,5},{5,1},{2,10},{10,14}... | collective-permute-start | bytes 1572872 | tf_op jit(solution)/shard_map/ppermute | solution.py:173
  88.6 4.5 %copy-start.14 = (s32[1,768]{1,0:T(1,128)}, s32[1,768]{1,0:T(1,128)S(1)}, u32[]{:S(2)}) copy-start(s32[1,768]{1,0:T(1,128)S(1)} %broadcast_in_dim.21.refs_4_) | copy-start | bytes 9220
  108.7 14.2 %collective-permute-start.23 = (bf16[256,1024]{1,0:T(8,128)(2,1)S(1)}, bf16[256,1024]{1,0:T(8,128)(2,1)S(1)}, u32[]{:S(2)}, u32[]{:S(2)}) collective-permute-start(bf16[256,1024]{1,0:T(8,128)(2,1)S(1)} %collective-permute-done.17.refs_16_.refs_17_.refs_18_.refs_2_), channel_id=1, source_target_pairs={{0,8},{8,12},{12,4},{4,0},{1,9},{9,13},{13,5},{5,1},{2,10},{10,14}... | collective-permute-start | bytes 1572872 | tf_op jit(solution)/shard_map/ppermute | solution.py:173
  108.7 5.0 %collective-permute-start.18 = (bf16[128,512]{1,0:T(8,128)(2,1)S(1)}, bf16[128,512]{1,0:T(8,128)(2,1)S(1)}, u32[]{:S(2)}, u32[]{:S(2)}) collective-permute-start(bf16[128,512]{1,0:T(8,128)(2,1)S(1)} %collective-permute-done.14.refs_4_), channel_id=1, source_target_pairs={{0,16},{16,0},{1,17},{17,1},{2,18},{18,2},{3,19},{19,3},{4,20},{20... | collective-permute-start | bytes 393224 | tf_op jit(solution)/shard_map/ppermute | solution.py:181
  109.6 4.0 %copy-start.2 = (bf16[256,512]{1,0:T(8,128)(2,1)S(1)}, bf16[256,512]{1,0:T(8,128)(2,1)}, u32[]{:S(2)}) copy-start(bf16[256,512]{1,0:T(8,128)(2,1)} %get-tuple-element.48.own_ref) | copy-start | bytes 786436
  110.7 3.0 %copy-start.13 = (s32[6]{0:T(128)S(1)}, s32[6]{0:T(128)}, u32[]{:S(2)}) copy-start(s32[6]{0:T(128)} %copy-done.12) | copy-start | bytes 76
  113.7 25.4 %copy-start.6 = (bf16[512,256]{1,0:T(8,128)(2,1)S(1)}, bf16[512,256]{1,0:T(8,128)(2,1)}, u32[]{:S(2)}) copy-start(bf16[512,256]{1,0:T(8,128)(2,1)} %get-tuple-element.51.refs_9_) | copy-start | bytes 786436
  113.7 25.4 %copy-start.7 = (bf16[512,256]{1,0:T(8,128)(2,1)S(1)}, bf16[512,256]{1,0:T(8,128)(2,1)}, u32[]{:S(2)}) copy-start(bf16[512,256]{1,0:T(8,128)(2,1)} %get-tuple-element.55.refs_8_) | copy-start | bytes 786436
  113.7 25.4 %copy-start.8 = (bf16[512,256]{1,0:T(8,128)(2,1)S(1)}, bf16[512,256]{1,0:T(8,128)(2,1)}, u32[]{:S(2)}) copy-start(bf16[512,256]{1,0:T(8,128)(2,1)} %get-tuple-element.59.refs_7_) | copy-start | bytes 786436
  115.0 24.1 %copy-start.11 = (f32[1,2048]{1,0:T(1,128)S(1)}, f32[1,2048]{1,0:T(1,128)}, u32[]{:S(2)}) copy-start(f32[1,2048]{1,0:T(1,128)} %get-tuple-element.65) | copy-start | bytes 24580
  115.0 10.1 %collective-permute-start.20 = (bf16[256,512]{1,0:T(8,128)(2,1)S(1)}, bf16[256,512]{1,0:T(8,128)(2,1)S(1)}, u32[]{:S(2)}, u32[]{:S(2)}) collective-permute-start(bf16[256,512]{1,0:T(8,128)(2,1)S(1)} %shard_map.120.refs_0_.r_ref), channel_id=1, source_target_pairs={{0,2},{1,3},{2,0},{3,1},{4,6},{5,7},{6,4},{7,5},{8,10},{9,11},{10,... | collective-permute-start | bytes 786440 | tf_op jit(solution)/shard_map/ppermute | solution.py:189
  115.6 12.2 %collective-permute-start.22 = (bf16[256,1024]{1,0:T(8,128)(2,1)S(1)}, bf16[256,1024]{1,0:T(8,128)(2,1)S(1)}, u32[]{:S(2)}, u32[]{:S(2)}) collective-permute-start(bf16[256,1024]{1,0:T(8,128)(2,1)S(1)} %collective-permute-done.17.refs_16_.refs_17_.refs_18_.refs_2_), channel_id=1, source_target_pairs={{0,16},{16,0},{1,17},{17,1},{2,18},{18,2},{3,19},{19,3},{4,20},{20... | collective-permute-start | bytes 1572872 | tf_op jit(solution)/shard_map/ppermute | solution.py:181
  122.9 16.2 %collective-permute-start.24 = (bf16[256,1024]{1,0:T(8,128)(2,1)S(1)}, bf16[256,1024]{1,0:T(8,128)(2,1)S(1)}, u32[]{:S(2)}, u32[]{:S(2)}) collective-permute-start(bf16[256,1024]{1,0:T(8,128)(2,1)S(1)} %collective-permute-done.23.refs_22_.refs_23_.refs_24_.refs_4_), channel_id=1, source_target_pairs={{0,16},{16,0},{1,17},{17,1},{2,18},{18,2},{3,19},{19,3},{4,20},{20... | collective-permute-start | bytes 1572872 | tf_op jit(solution)/shard_map/ppermute | solution.py:181
  123.8 2.5 %collective-permute-start.19 = (bf16[256,512]{1,0:T(8,128)(2,1)S(1)}, bf16[256,512]{1,0:T(8,128)(2,1)S(1)}, u32[]{:S(2)}, u32[]{:S(2)}) collective-permute-start(bf16[256,512]{1,0:T(8,128)(2,1)S(1)} %shard_map.120.refs_0_.r_ref), channel_id=1, source_target_pairs={{0,1},{1,0},{2,3},{3,2},{4,5},{5,4},{6,7},{7,6},{8,9},{9,8},{10,11... | collective-permute-start | bytes 786440 | tf_op jit(solution)/shard_map/ppermute | solution.py:189
  125.1 1.5 collective-permute-start.21
  142.7 16.5 %copy-start.15 = (s32[1,768]{1,0:T(1,128)S(1)}, s32[1,768]{1,0:T(1,128)}, u32[]{:S(2)}) copy-start(s32[1,768]{1,0:T(1,128)} %copy-done.14) | copy-start | bytes 9220
  142.7 8.6 %collective-permute-start.25 = (bf16[256,512]{1,0:T(8,128)(2,1)S(1)}, bf16[256,512]{1,0:T(8,128)(2,1)S(1)}, u32[]{:S(2)}, u32[]{:S(2)}) collective-permute-start(bf16[256,512]{1,0:T(8,128)(2,1)S(1)} %get-tuple-element.46.refs_2_), channel_id=1, source_target_pairs={{0,8},{4,12},{1,9},{5,13},{2,10},{6,14},{3,11},{7,15},{16,24},{20,... | collective-permute-start | bytes 786440 | tf_op jit(solution)/shard_map/ppermute | solution.py:20
  144.0 15.1 %collective-permute-start.26 = (bf16[256,512]{1,0:T(8,128)(2,1)S(1)}, bf16[256,512]{1,0:T(8,128)(2,1)S(1)}, u32[]{:S(2)}, u32[]{:S(2)}) collective-permute-start(bf16[256,512]{1,0:T(8,128)(2,1)S(1)} %get-tuple-element.46.refs_2_), channel_id=1, source_target_pairs={{0,4},{4,8},{8,12},{1,5},{5,9},{9,13},{2,6},{6,10},{10,14},{3,7},{... | collective-permute-start | bytes 786440 | tf_op jit(solution)/shard_map/ppermute | solution.py:20
  163.1 11.2 %copy-start.1 = (bf16[256,512]{1,0:T(8,128)(2,1)S(1)}, bf16[256,512]{1,0:T(8,128)(2,1)}, u32[]{:S(2)}) copy-start(bf16[256,512]{1,0:T(8,128)(2,1)} %get-tuple-element.47.own_ref) | copy-start | bytes 786436
  175.6 7.8 %collective-permute-start.28 = (bf16[256,512]{1,0:T(8,128)(2,1)S(1)}, bf16[256,512]{1,0:T(8,128)(2,1)S(1)}, u32[]{:S(2)}, u32[]{:S(2)}) collective-permute-start(bf16[256,512]{1,0:T(8,128)(2,1)S(1)} %shard_map.123.refs_0_), channel_id=1, source_target_pairs={{0,2},{1,3},{2,0},{3,1},{4,6},{5,7},{6,4},{7,5},{8,10},{9,11},{10,... | collective-permute-start | bytes 786440 | tf_op jit(solution)/shard_map/ppermute | solution.py:189
  176.2 8.2 %collective-permute-start.27 = (bf16[256,512]{1,0:T(8,128)(2,1)S(1)}, bf16[256,512]{1,0:T(8,128)(2,1)S(1)}, u32[]{:S(2)}, u32[]{:S(2)}) collective-permute-start(bf16[256,512]{1,0:T(8,128)(2,1)S(1)} %shard_map.123.refs_0_), channel_id=1, source_target_pairs={{0,1},{1,0},{2,3},{3,2},{4,5},{5,4},{6,7},{7,6},{8,9},{9,8},{10,11... | collective-permute-start | bytes 786440 | tf_op jit(solution)/shard_map/ppermute | solution.py:189
  183.4 2.2 %collective-permute-start.29 = (bf16[256,512]{1,0:T(8,128)(2,1)S(1)}, bf16[256,512]{1,0:T(8,128)(2,1)S(1)}, u32[]{:S(2)}, u32[]{:S(2)}) collective-permute-start(bf16[256,512]{1,0:T(8,128)(2,1)S(1)} %collective-permute-done.28.refs_2_), channel_id=1, source_target_pairs={{0,1},{1,0},{2,3},{3,2},{4,5},{5,4},{6,7},{7,6},{8,9},{9,8},{10,11... | collective-permute-start | bytes 786440 | tf_op jit(solution)/shard_map/ppermute | solution.py:189
  (12 other events, 11.4 us)

commit v3 on v2

--- a/solution.py
+++ b/solution.py
@@ -219,21 +219,23 @@
     return jnp.concatenate(parts, axis=1)
 
 
-def project(x_pieces, gain, q_gain, k_gain, own, pieces, piece_col, order, count):
+def project(x_pieces, gain, q_gain, k_gain, own, layer, pieces, order, count):
     rows, piece_width = x_pieces[0].shape
-    half = own[0].shape[0] // 2
-    width = own[0].shape[1]
+    half = own[0].shape[1] // 2
+    width = own[0].shape[2]
     dims = len(x_pieces) * piece_width
     blocks = dims // half
     per_piece = piece_width // half
     head_size = q_gain.shape[1]
     gain_blocks = gain.reshape(blocks, 1, half)
-    operands = list(x_pieces) + [gain_blocks, q_gain, k_gain] + list(own)
+    operands = list(x_pieces) + [gain_blocks, q_gain, k_gain]
     specs = [full_spec(a) for a in operands]
+    operands += list(own)
+    specs += [window_spec((1, 2 * half, width), (layer, 0, 0)) for _ in own]
     for piece in pieces:
         for j in range(3):
             operands.append(piece)
-            specs.append(window_spec((half, width), (0, piece_col + j)))
+            specs.append(window_spec((half, width), (0, j)))
     n_x, n_p = len(x_pieces), len(pieces)
 
     def kernel(order_ref, *refs):
@@ -257,8 +259,8 @@
         sums = []
         for j in range(3):
             src = order_ref[0]
-            acc = jnp.dot(xs[2 * src], own_refs[j][:half], preferred_element_type=f32)
-            acc += jnp.dot(xs[2 * src + 1], own_refs[j][half:], preferred_element_type=f32)
+            acc = jnp.dot(xs[2 * src], own_refs[j][0, :half], preferred_element_type=f32)
+            acc += jnp.dot(xs[2 * src + 1], own_refs[j][0, half:], preferred_element_type=f32)
             for k in range(n_p):
                 src = order_ref[k // 2 + 1]
                 part = grp if k % 2 == 0 else 1 - grp
@@ -316,16 +318,14 @@
     return call(kernel, order, operands, specs, [jax.ShapeDtypeStruct((rows, width), bf16)], [])[0]
 
 
-def output(attended, residual, own, pieces, order, count):
+def output(attended, residual, own, layer, pieces, order, count):
     rows, dims = attended.shape
-    half = own.shape[0] // 2
-    cols = own.shape[1]
+    half = own.shape[1] // 2
+    cols = own.shape[2]
     blocks = dims // half
     operands = [attended, residual, own] + list(pieces)
-    specs = [full_spec(a) for a in operands[:3]]
-    packed = pieces[0].shape[0] != half
-    shape = (2 * half, cols // 2) if packed else (half, cols)
-    specs += [window_spec(shape, (0, 0)) for _ in pieces]
+    specs = [full_spec(attended), full_spec(residual)]
+    specs += [window_spec((1, 2 * half, cols), (layer, 0, 0))] + [full_spec(p) for p in pieces]
 
     def kernel(order_ref, a_ref, r_ref, own_ref, *refs):
         piece_refs, (out_ref, xs) = refs[: len(pieces)], refs[len(pieces) :]
@@ -333,15 +333,12 @@
             xs[b] = a_ref[:, b * half : (b + 1) * half]
         grp = order_ref[count]
         src = order_ref[0]
-        acc = jnp.dot(xs[2 * src], own_ref[:half], preferred_element_type=f32)
-        acc += jnp.dot(xs[2 * src + 1], own_ref[half:], preferred_element_type=f32)
+        acc = jnp.dot(xs[2 * src], own_ref[0, :half], preferred_element_type=f32)
+        acc += jnp.dot(xs[2 * src + 1], own_ref[0, half:], preferred_element_type=f32)
         for k in range(len(pieces)):
             src = order_ref[k // 2 + 1]
             part = grp if k % 2 == 0 else 1 - grp
-            weight = piece_refs[k][...]
-            if packed:
-                weight = jnp.concatenate([weight[:half], weight[half:]], axis=1)
-            acc += jnp.dot(xs[2 * src + part], weight, preferred_element_type=f32)
+            acc += jnp.dot(xs[2 * src + part], piece_refs[k][...], preferred_element_type=f32)
         out_ref[...] = (r_ref[...].astype(f32) + acc).astype(bf16)
 
     return call(
@@ -411,12 +408,11 @@
         return jnp.concatenate([half_of(w[layer], in_half) for w in shards], axis=1)
 
     first = joined(0)
-    out_first = half_of(out_weight[0], out_half)
     a_ring, a_group = [ring_step(first, ring)], []
-    own_next = half_of(out_weight[1], out_half)
-    own_next = jnp.concatenate([own_next[:, : cols // 2], own_next[:, cols // 2 :]], axis=0)
-    second = jnp.concatenate([own_next, joined(1)], axis=1)
+    second = joined(1)
+    out_halves = [half_of(out_weight[l], out_half) for l in range(LAYERS)]
     second = tie(second, a_ring[0])
+    out_halves = [tie(h, a_ring[0]) for h in out_halves]
     docs = [tie(doc_ids, a_ring[0])]
     docs = [shifted(docs[0], "sp", back) for back in range(depth, 0, -1)] + docs
     for step in range(1, count - 1):
@@ -426,50 +422,54 @@
     last, base = a_ring[-1], a_group[-1]
     a_group.append(swap_groups(tie(last, base)))
     c_ring, c_group = [ring_step(tie(second, last, base), ring)], []
+    o_ring, o_group = [ring_step(tie(out_halves[0], last, base), ring)], []
     doc_row = jnp.concatenate(docs)[None, :]
     doc_col = doc_ids[:, None]
     flat = flat_biases(rel_bias, rows)
 
     residual = tie(lax.dynamic_slice_in_dim(stream, t * cols, cols, 1), a_ring[0])
     x_pieces = [stream]
-    piece_cols = own_next.shape[1]
+    weights = (query_weight, key_weight, value_weight)
     for layer in range(LAYERS):
-        own = [w[layer] for w in (query_weight, key_weight, value_weight)]
         ring_pieces, group_pieces = (a_ring, a_group) if layer == 0 else (c_ring, c_group)
-        col = 0 if layer == 0 else piece_cols // own[0].shape[1]
+        ahead = o_ring + c_ring[:1] if layer == 0 else o_ring
         query, kv = project(
             x_pieces, norm_gain[layer], query_gain[layer][None], key_gain[layer][None],
-            own, interleave(ring_pieces, group_pieces), col,
-            tie(order, c_ring[0]) if layer == 0 else order, count,
-        )
-        received = [shifted(kv, "sp", back) for back in range(depth, 0, -1)]
-        attend_order = out_order = order
+            weights, layer, interleave(ring_pieces, group_pieces), tie(order, *ahead), count,
+        )
+        received = [shifted(kv, "sp", 1)]
+        o_group.append(swap_groups(tie(o_ring[-1], kv)))
+        beside = [o_group[-1]]
         if layer == 0:
-            o_ring, o_group = [ring_step(tie(out_first, kv), ring)], []
             c_group.append(swap_groups(tie(c_ring[0], kv)))
-            for step in range(1, count - 1):
-                near = received[-1] if step == 1 else o_group[-1]
-                o_group.append(swap_groups(tie(o_ring[-1], near)))
-                o_ring.append(ring_step(tie(o_ring[-1], near), ring))
-            attend_order = tie(order, o_ring[-1], o_group[-1], c_group[-1])
-            o_group.append(swap_groups(tie(o_ring[-1], attend_order)))
-            c_ring.append(ring_step(tie(c_ring[0], received[0], attend_order), ring))
+            beside.append(c_group[-1])
+        for _ in range(depth - 1):
+            received.insert(0, shifted(tie(received[0], beside[0]), "sp", 1))
+        o_ring.append(ring_step(tie(o_ring[-1], received[-1], beside[0]), ring))
+        attend_order = tie(order, o_ring[-1], *beside)
+        middle = [tie(o_ring[-1], received[0])]
+        o_group.append(swap_groups(middle[0]))
+        o_ring.append(ring_step(middle[0], ring))
+        if layer == 0:
+            c_ring.append(ring_step(tie(c_ring[0], received[0], o_ring[1]), ring))
         attended = attend_kernel(
             query, received + [kv], doc_col, doc_row, flat, attend_order, count, head_size
         )
+        attended = tie(attended, o_ring[-1], o_group[-1])
+        o_group.append(swap_groups(tie(o_ring[-1], attended)))
         all_heads = lax.all_gather(attended, "tp", axis=1, tiled=True)
+        out_order = order
         if layer == 0:
             out_order = tie(order, c_ring[-1])
-            for step in range(2, count - 1):
-                c_group.append(swap_groups(tie(c_ring[-1], all_heads)))
-                c_ring.append(ring_step(tie(c_ring[-1], all_heads), ring))
-            o_pieces = interleave(o_ring, o_group)
-        else:
-            o_pieces = interleave(c_ring, c_group)
-        block = output(all_heads, residual, out_weight[layer], o_pieces, out_order, count)
+            c_group.append(swap_groups(tie(c_ring[-1], all_heads)))
+            c_ring.append(ring_step(tie(c_ring[-1], all_heads), ring))
+        block = output(
+            all_heads, residual, out_weight, layer, interleave(o_ring, o_group), out_order, count
+        )
         x_pieces = exchange_columns(block, tp_count)
         if layer == 0:
             c_group.append(swap_groups(c_ring[-1]))
+            o_ring, o_group = [ring_step(tie(out_halves[1], c_ring[-1]), ring)], []
         residual = block
     return assemble(x_pieces, order, count)
 

time: 188 us -> 181 us (0.963)
  the two profiles are of different devices: /device:TPU:17 before, /device:TPU:25 now
where the time goes in v3:
time: 181 us; the launch traced here: 178 us
  waiting for transfers between devices  60.5 us (33%)
  starting transfers between devices  40.3 us (22%)
  blocking collectives  29.1 us (16%)
  local copies, waits for them, and re-layouts  25 us (14%)
  Pallas kernels  19.9 us (11%)
  other arithmetic  2.65 us (1%)
    all_gather x2, blocking collectives, on_device_fast(): all_heads = lax.all_gather(attended, 'tp', axis=1, tiled=True)  29.1 us
    ppermute x12, waiting for transfers between devices, ring_step(): lax.ppermute(value, 'sp', [(ring[i], ring[(i + 1) % count]) for i in rang...  24.9 us
    pallas_call x7, Pallas kernels, call(): pl.pallas_call(kernel, grid=(1,), in_specs=[pl.BlockSpec(memory_space=SME...  19.9 us
    ppermute x12, waiting for transfers between devices, swap_groups(): return lax.ppermute(value, 'grp', [(0, 1), (1, 0)])  19.1 us
    unnamed x78, local copies, waits for them, and re-layouts  15.8 us
    ppermute x12, starting transfers between devices, swap_groups(): return lax.ppermute(value, 'grp', [(0, 1), (1, 0)])  13.1 us
    ppermute x12, starting transfers between devices, ring_step(): lax.ppermute(value, 'sp', [(ring[i], ring[(i + 1) % count]) for i in rang...  13.1 us
    ppermute x6, waiting for transfers between devices, exchange_columns(): lax.ppermute(p, 'tp', pairs)  10.7 us
  transfers between devices with their start and end apart: 36, of which 18 were waited for; matrix products, arithmetic and copies ran while one was open for 6% of the time, Pallas kernels for 6%

profile of v3, /device:TPU:25, one launch (start us, length us, event | category | flops | bytes accessed | tf_op | source)
XLA Modules:
  0.0 177.8 jit_solution(15056791478637129228)
XLA Ops:
  0.0 1.1 fusion.3
  3.3 9.1 %collective-permute-done.refs_7_.refs_8_.refs_9_ = bf16[256,768]{1,0:T(8,128)(2,1)S(1)} collective-permute-done((bf16[256,768]{1,0:T(8,128)(2,1)S(1)}, bf16[256,768]{1,0:T(8,128)(2,1)S(1)}, u32[]{:S(2)}, u32[]{:S(2)}) %collective-permute-start) | collective-permute-done | bytes 393248 | tf_op jit(solution)/shard_map/ppermute | solution.py:173
  13.4 1.2 collective-permute-start.2
  15.4 1.4 collective-permute-start.4
  16.8 1.3 collective-permute-start.3
  19.2 2.4 %collective-permute-done.4 = s32[256]{0:T(256)S(1)} collective-permute-done((s32[256]{0:T(256)S(1)}, s32[256]{0:T(256)S(1)}, u32[]{:S(2)}, u32[]{:S(2)}) %collective-permute-start.4) | collective-permute-done | bytes 1056 | tf_op jit(solution)/shard_map/ppermute | solution.py:20
  23.0 1.3 collective-permute-start.5
  24.3 1.2 collective-permute-start.6
  26.2 6.3 %collective-permute-done.6.refs_16_.refs_17_.refs_18_ = bf16[256,768]{1,0:T(8,128)(2,1)S(1)} collective-permute-done((bf16[256,768]{1,0:T(8,128)(2,1)S(1)}, bf16[256,768]{1,0:T(8,128)(2,1)S(1)}, u32[]{:S(2)}, u32[]{:S(2)}) %collective-permute-start.6) | collective-permute-done | bytes 393248 | tf_op jit(solution)/shard_map/ppermute | solution.py:181
  34.1 1.2 collective-permute-start.9
  35.3 1.0 fusion.1
  36.3 1.7 dynamic-slice_bitcast_fusion
  40.3 3.6 %collective-permute-done.8.refs_0_ = bf16[128,512]{1,0:T(8,128)(2,1)S(1)} collective-permute-done((bf16[128,512]{1,0:T(8,128)(2,1)}, bf16[128,512]{1,0:T(8,128)(2,1)S(1)}, u32[]{:S(2)}, u32[]{:S(2)}) %collective-permute-start.8) | collective-permute-done | bytes 131104 | tf_op jit(solution)/shard_map/ppermute | solution.py:173
  45.9 1.2 copy-done.9
  47.1 3.6 %shard_map.118 = (bf16[256,256]{1,0:T(8,128)(2,1)S(1)}, bf16[256,512]{1,0:T(8,128)(2,1)S(1)}) custom-call(s32[6]{0:T(128)S(1)} %pad_add_fusion.1.order_ref, bf16[256,2048]{1,0:T(8,128)(2,1)S(1)} %copy-done.9, f32[8,1,256]{2,1,0:T(1,128)S(1)} %bitcast.25, f32[1,64]{1,0:T(1,128)S(1)} %get-tuple-element.95.refs_2_, f32[1,64]{1,0:T(1,128)S(1)} %get-tuple-element.86.refs_3_, ...), custom_call_target="tpu_custom_call" | custom-call | tf_op jit(solution)/shard_map/pallas_call | solution.py:203
  51.4 1.3 collective-permute-start.10
  54.3 2.9 %collective-permute-done.11.refs_1_ = bf16[128,512]{1,0:T(8,128)(2,1)S(1)} collective-permute-done((bf16[128,512]{1,0:T(8,128)(2,1)S(1)}, bf16[128,512]{1,0:T(8,128)(2,1)S(1)}, u32[]{:S(2)}, u32[]{:S(2)}) %collective-permute-start.11) | collective-permute-done | bytes 131104 | tf_op jit(solution)/shard_map/ppermute | solution.py:181
  58.5 1.3 collective-permute-start.12
  61.4 3.3 %collective-permute-start.13 = (bf16[128,512]{1,0:T(8,128)(2,1)S(1)}, bf16[128,512]{1,0:T(8,128)(2,1)}, u32[]{:S(2)}, u32[]{:S(2)}) collective-permute-start(bf16[128,512]{1,0:T(8,128)(2,1)S(1)} %collective-permute-done.8.refs_0_), channel_id=1, source_target_pairs={{0,8},{8,12},{12,4},{4,0},{1,9},{9,13},{13,5},{5,1},{2,10},{10,14}... | collective-permute-start | bytes 393224 | tf_op jit(solution)/shard_map/ppermute | solution.py:173
  65.9 1.2 collective-permute-done.13.refs_2_
  67.8 1.2 collective-permute-start.17
  69.1 1.6 collective-permute-start.16
  77.2 4.0 %shard_map.119 = bf16[256,256]{1,0:T(8,128)(2,1)S(1)} custom-call(s32[6]{0:T(128)S(1)} %copy-done.21, bf16[256,256]{1,0:T(8,128)(2,1)S(1)} %copy-done.19, bf16[256,512]{1,0:T(8,128)(2,1)S(1)} %copy-done.15, bf16[256,512]{1,0:T(8,128)(2,1)S(1)} %copy-done.13, bf16[256,512]{1,0:T(8,128)(2,1)S(1)} %copy-done.11, s32[256,1]{1,0:T(8,128)S(1)} %copy.13.refs_3_, ...), custom_call_target="tpu_custom_call" | custom-call | tf_op jit(solution)/shard_map/pallas_call | solution.py:203
  81.3 16.2 %all_gather.6.a_ref = bf16[256,1024]{1,0:T(8,128)(2,1)} all-gather(bf16[256,256]{1,0:T(8,128)(2,1)S(1)} %shard_map.119), channel_id=1, replica_groups=mesh['grp'=2,'sp'=4,'tp'=4] {'tp'}, dimensions={1}, use_global_device_ids=true | all-gather | bytes 655360 | tf_op jit(solution)/shard_map/all_gather | solution.py:460
  97.5 1.4 collective-permute-start.18
  98.9 1.6 collective-permute-start.20
  101.6 2.6 %collective-permute-done.20.refs_5_ = bf16[128,512]{1,0:T(8,128)(2,1)} collective-permute-done((bf16[128,512]{1,0:T(8,128)(2,1)}, bf16[128,512]{1,0:T(8,128)(2,1)}, u32[]{:S(2)}, u32[]{:S(2)}) %collective-permute-start.20) | collective-permute-done | bytes 131104 | tf_op jit(solution)/shard_map/ppermute | solution.py:181
  105.1 1.9 %shard_map.120.refs_0_.r_ref = bf16[256,512]{1,0:T(8,128)(2,1)S(1)} custom-call(s32[6]{0:T(128)S(1)} %copy-done.22, bf16[256,1024]{1,0:T(8,128)(2,1)S(1)} %copy-done.8, bf16[256,512]{1,0:T(8,128)(2,1)S(1)} %constant_dynamic-slice_fusion.r_ref, bf16[2,256,512]{2,1,0:T(8,128)(2,1)S(1)} %copy-done.3, bf16[128,512]{1,0:T(8,128)(2,1)S(1)} %collective-permute-done.8.refs_0_, ...), custom_call_target="tpu_custom_call" | custom-call | tf_op jit(solution)/shard_map/pallas_call | solution.py:203
  107.6 1.3 collective-permute-start.24
  109.4 1.6 collective-permute-start.21
  111.0 2.8 %collective-permute-done.22.refs_2_ = bf16[256,512]{1,0:T(8,128)(2,1)S(1)} collective-permute-done((bf16[256,512]{1,0:T(8,128)(2,1)S(1)}, bf16[256,512]{1,0:T(8,128)(2,1)S(1)}, u32[]{:S(2)}, u32[]{:S(2)}) %collective-permute-start.22) | collective-permute-done | bytes 262176 | tf_op jit(solution)/shard_map/ppermute | solution.py:189
  113.8 2.0 %collective-permute-start.23 = (bf16[256,512]{1,0:T(8,128)(2,1)S(1)}, bf16[256,512]{1,0:T(8,128)(2,1)S(1)}, u32[]{:S(2)}, u32[]{:S(2)}) collective-permute-start(bf16[256,512]{1,0:T(8,128)(2,1)S(1)} %collective-permute-done.22.refs_2_), channel_id=1, source_target_pairs={{0,1},{1,0},{2,3},{3,2},{4,5},{5,4},{6,7},{7,6},{8,9},{9,8},{10,11... | collective-permute-start | bytes 786440 | tf_op jit(solution)/shard_map/ppermute | solution.py:189
  116.1 4.8 %collective-permute-done.19.refs_0_ = bf16[128,512]{1,0:T(8,128)(2,1)S(1)} collective-permute-done((bf16[128,512]{1,0:T(8,128)(2,1)S(1)}, bf16[128,512]{1,0:T(8,128)(2,1)S(1)}, u32[]{:S(2)}, u32[]{:S(2)}) %collective-permute-start.19) | collective-permute-done | bytes 131104 | tf_op jit(solution)/shard_map/ppermute | solution.py:173
  120.9 4.4 %collective-permute-done.25.refs_25_.refs_26_.refs_27_ = bf16[256,768]{1,0:T(8,128)(2,1)S(1)} collective-permute-done((bf16[256,768]{1,0:T(8,128)(2,1)}, bf16[256,768]{1,0:T(8,128)(2,1)S(1)}, u32[]{:S(2)}, u32[]{:S(2)}) %collective-permute-start.25) | collective-permute-done | bytes 393248 | tf_op jit(solution)/shard_map/ppermute | solution.py:181
  125.9 3.5 %shard_map.121 = (bf16[256,256]{1,0:T(8,128)(2,1)S(1)}, bf16[256,512]{1,0:T(8,128)(2,1)S(1)}) custom-call(s32[6]{0:T(128)S(1)} %copy-done.22, bf16[256,512]{1,0:T(8,128)(2,1)S(1)} %shard_map.120.refs_0_.r_ref, bf16[256,512]{1,0:T(8,128)(2,1)S(1)} %collective-permute-done.21.refs_1_, bf16[256,512]{1,0:T(8,128)(2,1)S(1)} %collective-permute-done.22.refs_2_, ...), custom_call_target="tpu_custom_call" | custom-call | tf_op jit(solution)/shard_map/pallas_call | solution.py:203
  129.4 1.3 collective-permute-start.26
  130.7 1.2 collective-permute-start.27
  131.9 2.7 %collective-permute-done.27.refs_1_ = bf16[128,512]{1,0:T(8,128)(2,1)S(1)} collective-permute-done((bf16[128,512]{1,0:T(8,128)(2,1)S(1)}, bf16[128,512]{1,0:T(8,128)(2,1)S(1)}, u32[]{:S(2)}, u32[]{:S(2)}) %collective-permute-start.27) | collective-permute-done | bytes 131104 | tf_op jit(solution)/shard_map/ppermute | solution.py:181
  134.6 2.3 %collective-permute-done.26.refs_1_ = bf16[256,512]{1,0:T(8,128)(2,1)S(1)} collective-permute-done((bf16[256,512]{1,0:T(8,128)(2,1)S(1)}, bf16[256,512]{1,0:T(8,128)(2,1)S(1)}, u32[]{:S(2)}, u32[]{:S(2)}) %collective-permute-start.26) | collective-permute-done | bytes 262176 | tf_op jit(solution)/shard_map/ppermute | solution.py:20
  136.9 1.3 collective-permute-start.29
  138.2 1.9 %collective-permute-start.28 = (bf16[128,512]{1,0:T(8,128)(2,1)S(1)}, bf16[128,512]{1,0:T(8,128)(2,1)S(1)}, u32[]{:S(2)}, u32[]{:S(2)}) collective-permute-start(bf16[128,512]{1,0:T(8,128)(2,1)S(1)} %collective-permute-done.19.refs_0_), channel_id=1, source_target_pairs={{0,8},{8,12},{12,4},{4,0},{1,9},{9,13},{13,5},{5,1},{2,10},{10,14}... | collective-permute-start | bytes 393224 | tf_op jit(solution)/shard_map/ppermute | solution.py:173
  140.1 6.2 %collective-permute-done.28.refs_2_ = bf16[128,512]{1,0:T(8,128)(2,1)S(1)} collective-permute-done((bf16[128,512]{1,0:T(8,128)(2,1)S(1)}, bf16[128,512]{1,0:T(8,128)(2,1)S(1)}, u32[]{:S(2)}, u32[]{:S(2)}) %collective-permute-start.28) | collective-permute-done | bytes 131104 | tf_op jit(solution)/shard_map/ppermute | solution.py:173
  147.2 4.0 %shard_map.122 = bf16[256,256]{1,0:T(8,128)(2,1)S(1)} custom-call(s32[6]{0:T(128)S(1)} %copy-done.22, bf16[256,256]{1,0:T(8,128)(2,1)S(1)} %get-tuple-element.70.q_ref, bf16[256,512]{1,0:T(8,128)(2,1)S(1)} %collective-permute-done.29.refs_0_, bf16[256,512]{1,0:T(8,128)(2,1)S(1)} %collective-permute-done.26.refs_1_, ...), custom_call_target="tpu_custom_call" | custom-call | tf_op jit(solution)/shard_map/pallas_call | solution.py:203
  152.1 12.9 %all_gather.7.a_ref = bf16[256,1024]{1,0:T(8,128)(2,1)S(1)} all-gather(bf16[256,256]{1,0:T(8,128)(2,1)S(1)} %shard_map.122), channel_id=1, replica_groups=mesh['grp'=2,'sp'=4,'tp'=4] {'tp'}, dimensions={1}, use_global_device_ids=true | all-gather | bytes 655360 | tf_op jit(solution)/shard_map/all_gather | solution.py:460
  165.0 1.3 shard_map.123.refs_0_
  167.4 6.7 %collective-permute-done.34.refs_2_ = bf16[256,512]{1,0:T(8,128)(2,1)S(1)} collective-permute-done((bf16[256,512]{1,0:T(8,128)(2,1)S(1)}, bf16[256,512]{1,0:T(8,128)(2,1)S(1)}, u32[]{:S(2)}, u32[]{:S(2)}) %collective-permute-start.34) | collective-permute-done | bytes 262176 | tf_op jit(solution)/shard_map/ppermute | solution.py:189
  175.1 1.2 collective-permute-done.35.refs_3_
  176.3 1.6 shard_map.124
  (139 shorter events, 34.2 us)
Async XLA Ops:
  2.4 10.1 %collective-permute-start = (bf16[256,768]{1,0:T(8,128)(2,1)S(1)}, bf16[256,768]{1,0:T(8,128)(2,1)S(1)}, u32[]{:S(2)}, u32[]{:S(2)}) collective-permute-start(bf16[256,768]{1,0:T(8,128)(2,1)S(1)} %pad_maximum_fusion), channel_id=1, source_target_pairs={{0,8},{8,12},{12,4},{4,0},{1,9},{9,13},{13,5},{5,1},{2,10},{10,14}... | collective-permute-start | bytes 1179656 | tf_op jit(solution)/shard_map/ppermute | solution.py:173
  2.5 12.1 %copy-start.3 = (bf16[2,256,512]{2,1,0:T(8,128)(2,1)S(1)}, bf16[2,256,512]{2,1,0:T(8,128)(2,1)}, u32[]{:S(2)}) copy-start(bf16[2,256,512]{2,1,0:T(8,128)(2,1)} %own_ref.3) | copy-start | bytes 1572868
  3.3 12.1 %copy-start.32 = (s32[256]{0:T(256)S(1)}, s32[256]{0:T(256)}, u32[]{:S(2)}) copy-start(s32[256]{0:T(256)} %param.13) | copy-start | bytes 3076
  3.3 14.8 %copy-start.35 = (f32[2,64]{1,0:T(2,128)S(1)}, f32[2,64]{1,0:T(2,128)}, u32[]{:S(2)}) copy-start(f32[2,64]{1,0:T(2,128)} %param.20) | copy-start | bytes 1540
  3.3 14.8 %copy-start.36 = (f32[2,64]{1,0:T(2,128)S(1)}, f32[2,64]{1,0:T(2,128)}, u32[]{:S(2)}) copy-start(f32[2,64]{1,0:T(2,128)} %param.19) | copy-start | bytes 1540
  12.4 9.7 %collective-permute-start.1 = (bf16[256,768]{1,0:T(8,128)(2,1)S(1)}, bf16[256,768]{1,0:T(8,128)(2,1)S(1)}, u32[]{:S(2)}, u32[]{:S(2)}) collective-permute-start(bf16[256,768]{1,0:T(8,128)(2,1)S(1)} %collective-permute-done.refs_7_.refs_8_.refs_9_), channel_id=1, source_target_pairs={{0,8},{8,12},{12,4},{4,0},{1,9},{9,13},{13,5},{5,1},{2,10},{10,14}... | collective-permute-start | bytes 1179656 | tf_op jit(solution)/shard_map/ppermute | solution.py:173
  13.4 8.9 %collective-permute-start.2 = (bf16[256,768]{1,0:T(8,128)(2,1)S(1)}, bf16[256,768]{1,0:T(8,128)(2,1)S(1)}, u32[]{:S(2)}, u32[]{:S(2)}) collective-permute-start(bf16[256,768]{1,0:T(8,128)(2,1)S(1)} %collective-permute-done.refs_7_.refs_8_.refs_9_), channel_id=1, source_target_pairs={{0,16},{16,0},{1,17},{17,1},{2,18},{18,2},{3,19},{19,3},{4,20},{20... | collective-permute-start | bytes 1179656 | tf_op jit(solution)/shard_map/ppermute | solution.py:181
  15.4 10.2 %copy-start.30 = (f32[2,2048]{1,0:T(2,128)S(1)}, f32[2,2048]{1,0:T(2,128)}, u32[]{:S(2)}) copy-start(f32[2,2048]{1,0:T(2,128)} %param.14) | copy-start | bytes 49156
  15.4 6.2 %collective-permute-start.4 = (s32[256]{0:T(256)S(1)}, s32[256]{0:T(256)S(1)}, u32[]{:S(2)}, u32[]{:S(2)}) collective-permute-start(s32[256]{0:T(256)S(1)} %copy-done.32), channel_id=1, source_target_pairs={{0,4},{4,8},{8,12},{1,5},{5,9},{9,13},{2,6},{6,10},{10,14},{3,7},{... | collective-permute-start | bytes 3080 | tf_op jit(solution)/shard_map/ppermute | solution.py:20
  16.8 5.3 %collective-permute-start.3 = (s32[256]{0:T(256)S(1)}, s32[256]{0:T(256)S(1)}, u32[]{:S(2)}, u32[]{:S(2)}) collective-permute-start(s32[256]{0:T(256)S(1)} %copy-done.32), channel_id=1, source_target_pairs={{0,8},{4,12},{1,9},{5,13},{2,10},{6,14},{3,11},{7,15},{16,24},{20,... | collective-permute-start | bytes 3080 | tf_op jit(solution)/shard_map/ppermute | solution.py:20
  22.1 4.1 %copy-start.34 = (s32[256]{0:T(256)}, s32[256]{0:T(256)S(1)}, u32[]{:S(2)}) copy-start(s32[256]{0:T(256)S(1)} %collective-permute-done.3) | copy-start | bytes 3076
  23.0 10.2 %collective-permute-start.5 = (bf16[256,768]{1,0:T(8,128)(2,1)S(1)}, bf16[256,768]{1,0:T(8,128)(2,1)}, u32[]{:S(2)}, u32[]{:S(2)}) collective-permute-start(bf16[256,768]{1,0:T(8,128)(2,1)S(1)} %collective-permute-done.1.refs_13_.refs_14_.refs_15_), channel_id=1, source_target_pairs={{0,8},{8,12},{12,4},{4,0},{1,9},{9,13},{13,5},{5,1},{2,10},{10,14}... | collective-permute-start | bytes 1179656 | tf_op jit(solution)/shard_map/ppermute | solution.py:173
  24.3 8.1 %collective-permute-start.6 = (bf16[256,768]{1,0:T(8,128)(2,1)S(1)}, bf16[256,768]{1,0:T(8,128)(2,1)S(1)}, u32[]{:S(2)}, u32[]{:S(2)}) collective-permute-start(bf16[256,768]{1,0:T(8,128)(2,1)S(1)} %collective-permute-done.1.refs_13_.refs_14_.refs_15_), channel_id=1, source_target_pairs={{0,16},{16,0},{1,17},{17,1},{2,18},{18,2},{3,19},{19,3},{4,20},{20... | collective-permute-start | bytes 1179656 | tf_op jit(solution)/shard_map/ppermute | solution.py:181
  33.2 10.7 %collective-permute-start.7 = (bf16[256,768]{1,0:T(8,128)(2,1)}, bf16[256,768]{1,0:T(8,128)(2,1)S(1)}, u32[]{:S(2)}, u32[]{:S(2)}) collective-permute-start(bf16[256,768]{1,0:T(8,128)(2,1)} %pad_maximum_fusion.1), channel_id=1, source_target_pairs={{0,8},{8,12},{12,4},{4,0},{1,9},{9,13},{13,5},{5,1},{2,10},{10,14}... | collective-permute-start | bytes 1179656 | tf_op jit(solution)/shard_map/ppermute | solution.py:173
  34.1 9.8 %collective-permute-start.9 = (bf16[256,768]{1,0:T(8,128)(2,1)}, bf16[256,768]{1,0:T(8,128)(2,1)}, u32[]{:S(2)}, u32[]{:S(2)}) collective-permute-start(bf16[256,768]{1,0:T(8,128)(2,1)} %collective-permute-done.5.refs_19_.refs_20_.refs_21_), channel_id=1, source_target_pairs={{0,16},{16,0},{1,17},{17,1},{2,18},{18,2},{3,19},{19,3},{4,20},{20... | collective-permute-start | bytes 1179656 | tf_op jit(solution)/shard_map/ppermute | solution.py:181
  36.3 7.5 %copy-start = (bf16[2,512,256]{2,1,0:T(8,128)(2,1)S(1)}, bf16[2,512,256]{2,1,0:T(8,128)(2,1)}, u32[]{:S(2)}) copy-start(bf16[2,512,256]{2,1,0:T(8,128)(2,1)} %refs_7_.1) | copy-start | bytes 1572868
  38.0 5.8 %collective-permute-start.8 = (bf16[128,512]{1,0:T(8,128)(2,1)}, bf16[128,512]{1,0:T(8,128)(2,1)S(1)}, u32[]{:S(2)}, u32[]{:S(2)}) collective-permute-start(bf16[128,512]{1,0:T(8,128)(2,1)} %get-tuple-element.47), channel_id=1, source_target_pairs={{0,8},{8,12},{12,4},{4,0},{1,9},{9,13},{13,5},{5,1},{2,10},{10,14}... | collective-permute-start | bytes 393224 | tf_op jit(solution)/shard_map/ppermute | solution.py:173
  47.1 17.6 %copy-start.31 = (f32[4,513]{1,0:T(4,128)S(1)}, f32[4,513]{1,0:T(4,128)}, u32[]{:S(2)}) copy-start(f32[4,513]{1,0:T(4,128)} %param.21) | copy-start | bytes 24628
  51.4 7.1 %collective-permute-start.10 = (bf16[256,512]{1,0:T(8,128)(2,1)S(1)}, bf16[256,512]{1,0:T(8,128)(2,1)S(1)}, u32[]{:S(2)}, u32[]{:S(2)}) collective-permute-start(bf16[256,512]{1,0:T(8,128)(2,1)S(1)} %get-tuple-element.50.refs_2_), channel_id=1, source_target_pairs={{0,4},{4,8},{8,12},{1,5},{5,9},{9,13},{2,6},{6,10},{10,14},{3,7},{... | collective-permute-start | bytes 786440 | tf_op jit(solution)/shard_map/ppermute | solution.py:20
  53.4 3.8 %collective-permute-start.11 = (bf16[128,512]{1,0:T(8,128)(2,1)S(1)}, bf16[128,512]{1,0:T(8,128)(2,1)S(1)}, u32[]{:S(2)}, u32[]{:S(2)}) collective-permute-start(bf16[128,512]{1,0:T(8,128)(2,1)S(1)} %collective-permute-done.8.refs_0_), channel_id=1, source_target_pairs={{0,16},{16,0},{1,17},{17,1},{2,18},{18,2},{3,19},{19,3},{4,20},{20... | collective-permute-start | bytes 393224 | tf_op jit(solution)/shard_map/ppermute | solution.py:181
  58.5 8.7 %collective-permute-start.12 = (bf16[256,512]{1,0:T(8,128)(2,1)S(1)}, bf16[256,512]{1,0:T(8,128)(2,1)S(1)}, u32[]{:S(2)}, u32[]{:S(2)}) collective-permute-start(bf16[256,512]{1,0:T(8,128)(2,1)S(1)} %collective-permute-done.10.refs_1_), channel_id=1, source_target_pairs={{0,4},{4,8},{8,12},{1,5},{5,9},{9,13},{2,6},{6,10},{10,14},{3,7},{... | collective-permute-start | bytes 786440 | tf_op jit(solution)/shard_map/ppermute | solution.py:20
  60.5 12.4 %collective-permute-start.15 = (bf16[256,768]{1,0:T(8,128)(2,1)S(1)}, bf16[256,768]{1,0:T(8,128)(2,1)S(1)}, u32[]{:S(2)}, u32[]{:S(2)}) collective-permute-start(bf16[256,768]{1,0:T(8,128)(2,1)S(1)} %collective-permute-done.7.refs_10_.refs_11_.refs_12_), channel_id=1, source_target_pairs={{0,16},{16,0},{1,17},{17,1},{2,18},{18,2},{3,19},{19,3},{4,20},{20... | collective-permute-start | bytes 1179656 | tf_op jit(solution)/shard_map/ppermute | solution.py:181
  61.4 5.7 %collective-permute-start.13 = (bf16[128,512]{1,0:T(8,128)(2,1)S(1)}, bf16[128,512]{1,0:T(8,128)(2,1)}, u32[]{:S(2)}, u32[]{:S(2)}) collective-permute-start(bf16[128,512]{1,0:T(8,128)(2,1)S(1)} %collective-permute-done.8.refs_0_), channel_id=1, source_target_pairs={{0,8},{8,12},{12,4},{4,0},{1,9},{9,13},{13,5},{5,1},{2,10},{10,14}... | collective-permute-start | bytes 393224 | tf_op jit(solution)/shard_map/ppermute | solution.py:173
  67.8 13.4 %collective-permute-start.17 = (bf16[128,512]{1,0:T(8,128)(2,1)}, bf16[128,512]{1,0:T(8,128)(2,1)}, u32[]{:S(2)}, u32[]{:S(2)}) collective-permute-start(bf16[128,512]{1,0:T(8,128)(2,1)} %collective-permute-done.13.refs_2_), channel_id=1, source_target_pairs={{0,16},{16,0},{1,17},{17,1},{2,18},{18,2},{3,19},{19,3},{4,20},{20... | collective-permute-start | bytes 393224 | tf_op jit(solution)/shard_map/ppermute | solution.py:181
  69.1 12.2 %collective-permute-start.16 = (bf16[128,512]{1,0:T(8,128)(2,1)}, bf16[128,512]{1,0:T(8,128)(2,1)}, u32[]{:S(2)}, u32[]{:S(2)}) collective-permute-start(bf16[128,512]{1,0:T(8,128)(2,1)} %collective-permute-done.13.refs_2_), channel_id=1, source_target_pairs={{0,8},{8,12},{12,4},{4,0},{1,9},{9,13},{13,5},{5,1},{2,10},{10,14}... | collective-permute-start | bytes 393224 | tf_op jit(solution)/shard_map/ppermute | solution.py:173
  70.7 26.8 %collective-permute-start.14 = (bf16[256,768]{1,0:T(8,128)(2,1)S(1)}, bf16[256,768]{1,0:T(8,128)(2,1)S(1)}, u32[]{:S(2)}, u32[]{:S(2)}) collective-permute-start(bf16[256,768]{1,0:T(8,128)(2,1)S(1)} %collective-permute-done.7.refs_10_.refs_11_.refs_12_), channel_id=1, source_target_pairs={{0,8},{8,12},{12,4},{4,0},{1,9},{9,13},{13,5},{5,1},{2,10},{10,14}... | collective-permute-start | bytes 1179656 | tf_op jit(solution)/shard_map/ppermute | solution.py:173
  72.8 8.4 %copy-start.24 = (s32[1,768]{1,0:T(1,128)}, s32[1,768]{1,0:T(1,128)S(1)}, u32[]{:S(2)}) copy-start(s32[1,768]{1,0:T(1,128)S(1)} %broadcast_in_dim.21.refs_4_) | copy-start | bytes 9220
  97.5 11.4 %collective-permute-start.18 = (bf16[256,768]{1,0:T(8,128)(2,1)S(1)}, bf16[256,768]{1,0:T(8,128)(2,1)}, u32[]{:S(2)}, u32[]{:S(2)}) collective-permute-start(bf16[256,768]{1,0:T(8,128)(2,1)S(1)} %collective-permute-done.14.refs_16_.refs_17_.refs_18_), channel_id=1, source_target_pairs={{0,8},{8,12},{12,4},{4,0},{1,9},{9,13},{13,5},{5,1},{2,10},{10,14}... | collective-permute-start | bytes 1179656 | tf_op jit(solution)/shard_map/ppermute | solution.py:173
  98.9 5.3 %collective-permute-start.20 = (bf16[128,512]{1,0:T(8,128)(2,1)}, bf16[128,512]{1,0:T(8,128)(2,1)}, u32[]{:S(2)}, u32[]{:S(2)}) collective-permute-start(bf16[128,512]{1,0:T(8,128)(2,1)} %collective-permute-done.16.refs_4_), channel_id=1, source_target_pairs={{0,16},{16,0},{1,17},{17,1},{2,18},{18,2},{3,19},{19,3},{4,20},{20... | collective-permute-start | bytes 393224 | tf_op jit(solution)/shard_map/ppermute | solution.py:181
  105.1 10.7 %copy-start.29 = (bf16[128,512]{1,0:T(8,128)(2,1)S(1)}, bf16[128,512]{1,0:T(8,128)(2,1)}, u32[]{:S(2)}) copy-start(bf16[128,512]{1,0:T(8,128)(2,1)} %get-tuple-element.61) | copy-start | bytes 393220
  107.0 18.3 %copy-start.23 = (f32[1,2048]{1,0:T(1,128)S(1)}, f32[1,2048]{1,0:T(1,128)}, u32[]{:S(2)}) copy-start(f32[1,2048]{1,0:T(1,128)} %get-tuple-element.83) | copy-start | bytes 24580
  107.0 6.8 %collective-permute-start.22 = (bf16[256,512]{1,0:T(8,128)(2,1)S(1)}, bf16[256,512]{1,0:T(8,128)(2,1)S(1)}, u32[]{:S(2)}, u32[]{:S(2)}) collective-permute-start(bf16[256,512]{1,0:T(8,128)(2,1)S(1)} %shard_map.120.refs_0_.r_ref), channel_id=1, source_target_pairs={{0,2},{1,3},{2,0},{3,1},{4,6},{5,7},{6,4},{7,5},{8,10},{9,11},{10,... | collective-permute-start | bytes 786440 | tf_op jit(solution)/shard_map/ppermute | solution.py:189
  107.6 13.2 %collective-permute-start.24 = (bf16[256,768]{1,0:T(8,128)(2,1)S(1)}, bf16[256,768]{1,0:T(8,128)(2,1)S(1)}, u32[]{:S(2)}, u32[]{:S(2)}) collective-permute-start(bf16[256,768]{1,0:T(8,128)(2,1)S(1)} %collective-permute-done.14.refs_16_.refs_17_.refs_18_), channel_id=1, source_target_pairs={{0,16},{16,0},{1,17},{17,1},{2,18},{18,2},{3,19},{19,3},{4,20},{20... | collective-permute-start | bytes 1179656 | tf_op jit(solution)/shard_map/ppermute | solution.py:181
  108.9 16.4 %collective-permute-start.25 = (bf16[256,768]{1,0:T(8,128)(2,1)}, bf16[256,768]{1,0:T(8,128)(2,1)S(1)}, u32[]{:S(2)}, u32[]{:S(2)}) collective-permute-start(bf16[256,768]{1,0:T(8,128)(2,1)} %collective-permute-done.18.refs_22_.refs_23_.refs_24_), channel_id=1, source_target_pairs={{0,16},{16,0},{1,17},{17,1},{2,18},{18,2},{3,19},{19,3},{4,20},{20... | collective-permute-start | bytes 1179656 | tf_op jit(solution)/shard_map/ppermute | solution.py:181
  109.4 11.4 %collective-permute-start.21 = (bf16[256,512]{1,0:T(8,128)(2,1)S(1)}, bf16[256,512]{1,0:T(8,128)(2,1)S(1)}, u32[]{:S(2)}, u32[]{:S(2)}) collective-permute-start(bf16[256,512]{1,0:T(8,128)(2,1)S(1)} %shard_map.120.refs_0_.r_ref), channel_id=1, source_target_pairs={{0,1},{1,0},{2,3},{3,2},{4,5},{5,4},{6,7},{7,6},{8,9},{9,8},{10,11... | collective-permute-start | bytes 786440 | tf_op jit(solution)/shard_map/ppermute | solution.py:189
  113.8 7.0 %collective-permute-start.23 = (bf16[256,512]{1,0:T(8,128)(2,1)S(1)}, bf16[256,512]{1,0:T(8,128)(2,1)S(1)}, u32[]{:S(2)}, u32[]{:S(2)}) collective-permute-start(bf16[256,512]{1,0:T(8,128)(2,1)S(1)} %collective-permute-done.22.refs_2_), channel_id=1, source_target_pairs={{0,1},{1,0},{2,3},{3,2},{4,5},{5,4},{6,7},{7,6},{8,9},{9,8},{10,11... | collective-permute-start | bytes 786440 | tf_op jit(solution)/shard_map/ppermute | solution.py:189
  115.8 5.1 %collective-permute-start.19 = (bf16[128,512]{1,0:T(8,128)(2,1)S(1)}, bf16[128,512]{1,0:T(8,128)(2,1)S(1)}, u32[]{:S(2)}, u32[]{:S(2)}) collective-permute-start(bf16[128,512]{1,0:T(8,128)(2,1)S(1)} %copy-done.29), channel_id=1, source_target_pairs={{0,8},{8,12},{12,4},{4,0},{1,9},{9,13},{13,5},{5,1},{2,10},{10,14}... | collective-permute-start | bytes 393224 | tf_op jit(solution)/shard_map/ppermute | solution.py:173
  129.4 17.8 %copy-start.25 = (s32[1,768]{1,0:T(1,128)S(1)}, s32[1,768]{1,0:T(1,128)}, u32[]{:S(2)}) copy-start(s32[1,768]{1,0:T(1,128)} %copy-done.24) | copy-start | bytes 9220
  129.4 7.5 %collective-permute-start.26 = (bf16[256,512]{1,0:T(8,128)(2,1)S(1)}, bf16[256,512]{1,0:T(8,128)(2,1)S(1)}, u32[]{:S(2)}, u32[]{:S(2)}) collective-permute-start(bf16[256,512]{1,0:T(8,128)(2,1)S(1)} %get-tuple-element.66.refs_2_), channel_id=1, source_target_pairs={{0,4},{4,8},{8,12},{1,5},{5,9},{9,13},{2,6},{6,10},{10,14},{3,7},{... | collective-permute-start | bytes 786440 | tf_op jit(solution)/shard_map/ppermute | solution.py:20
  130.7 3.9 %collective-permute-start.27 = (bf16[128,512]{1,0:T(8,128)(2,1)S(1)}, bf16[128,512]{1,0:T(8,128)(2,1)S(1)}, u32[]{:S(2)}, u32[]{:S(2)}) collective-permute-start(bf16[128,512]{1,0:T(8,128)(2,1)S(1)} %collective-permute-done.19.refs_0_), channel_id=1, source_target_pairs={{0,16},{16,0},{1,17},{17,1},{2,18},{18,2},{3,19},{19,3},{4,20},{20... | collective-permute-start | bytes 393224 | tf_op jit(solution)/shard_map/ppermute | solution.py:181
  136.9 9.4 %collective-permute-start.29 = (bf16[256,512]{1,0:T(8,128)(2,1)S(1)}, bf16[256,512]{1,0:T(8,128)(2,1)S(1)}, u32[]{:S(2)}, u32[]{:S(2)}) collective-permute-start(bf16[256,512]{1,0:T(8,128)(2,1)S(1)} %collective-permute-done.26.refs_1_), channel_id=1, source_target_pairs={{0,4},{4,8},{8,12},{1,5},{5,9},{9,13},{2,6},{6,10},{10,14},{3,7},{... | collective-permute-start | bytes 786440 | tf_op jit(solution)/shard_map/ppermute | solution.py:20
  138.2 8.2 %collective-permute-start.28 = (bf16[128,512]{1,0:T(8,128)(2,1)S(1)}, bf16[128,512]{1,0:T(8,128)(2,1)S(1)}, u32[]{:S(2)}, u32[]{:S(2)}) collective-permute-start(bf16[128,512]{1,0:T(8,128)(2,1)S(1)} %collective-permute-done.19.refs_0_), channel_id=1, source_target_pairs={{0,8},{8,12},{12,4},{4,0},{1,9},{9,13},{13,5},{5,1},{2,10},{10,14}... | collective-permute-start | bytes 393224 | tf_op jit(solution)/shard_map/ppermute | solution.py:173
  146.4 4.9 %collective-permute-start.31 = (bf16[128,512]{1,0:T(8,128)(2,1)S(1)}, bf16[128,512]{1,0:T(8,128)(2,1)S(1)}, u32[]{:S(2)}, u32[]{:S(2)}) collective-permute-start(bf16[128,512]{1,0:T(8,128)(2,1)S(1)} %collective-permute-done.28.refs_2_), channel_id=1, source_target_pairs={{0,16},{16,0},{1,17},{17,1},{2,18},{18,2},{3,19},{19,3},{4,20},{20... | collective-permute-start | bytes 393224 | tf_op jit(solution)/shard_map/ppermute | solution.py:181
  147.2 4.0 %collective-permute-start.30 = (bf16[128,512]{1,0:T(8,128)(2,1)S(1)}, bf16[128,512]{1,0:T(8,128)(2,1)S(1)}, u32[]{:S(2)}, u32[]{:S(2)}) collective-permute-start(bf16[128,512]{1,0:T(8,128)(2,1)S(1)} %collective-permute-done.28.refs_2_), channel_id=1, source_target_pairs={{0,8},{8,12},{12,4},{4,0},{1,9},{9,13},{13,5},{5,1},{2,10},{10,14}... | collective-permute-start | bytes 393224 | tf_op jit(solution)/shard_map/ppermute | solution.py:173
  151.3 13.7 %collective-permute-start.32 = (bf16[128,512]{1,0:T(8,128)(2,1)S(1)}, bf16[128,512]{1,0:T(8,128)(2,1)S(1)}, u32[]{:S(2)}, u32[]{:S(2)}) collective-permute-start(bf16[128,512]{1,0:T(8,128)(2,1)S(1)} %collective-permute-done.30.refs_4_), channel_id=1, source_target_pairs={{0,16},{16,0},{1,17},{17,1},{2,18},{18,2},{3,19},{19,3},{4,20},{20... | collective-permute-start | bytes 393224 | tf_op jit(solution)/shard_map/ppermute | solution.py:181
  166.3 7.8 %collective-permute-start.34 = (bf16[256,512]{1,0:T(8,128)(2,1)S(1)}, bf16[256,512]{1,0:T(8,128)(2,1)S(1)}, u32[]{:S(2)}, u32[]{:S(2)}) collective-permute-start(bf16[256,512]{1,0:T(8,128)(2,1)S(1)} %shard_map.123.refs_0_), channel_id=1, source_target_pairs={{0,2},{1,3},{2,0},{3,1},{4,6},{5,7},{6,4},{7,5},{8,10},{9,11},{10,... | collective-permute-start | bytes 786440 | tf_op jit(solution)/shard_map/ppermute | solution.py:189
  166.9 8.2 %collective-permute-start.33 = (bf16[256,512]{1,0:T(8,128)(2,1)S(1)}, bf16[256,512]{1,0:T(8,128)(2,1)S(1)}, u32[]{:S(2)}, u32[]{:S(2)}) collective-permute-start(bf16[256,512]{1,0:T(8,128)(2,1)S(1)} %shard_map.123.refs_0_), channel_id=1, source_target_pairs={{0,1},{1,0},{2,3},{3,2},{4,5},{5,4},{6,7},{7,6},{8,9},{9,8},{10,11... | collective-permute-start | bytes 786440 | tf_op jit(solution)/shard_map/ppermute | solution.py:189
  174.1 2.2 %collective-permute-start.35 = (bf16[256,512]{1,0:T(8,128)(2,1)S(1)}, bf16[256,512]{1,0:T(8,128)(2,1)S(1)}, u32[]{:S(2)}, u32[]{:S(2)}) collective-permute-start(bf16[256,512]{1,0:T(8,128)(2,1)S(1)} %collective-permute-done.34.refs_2_), channel_id=1, source_target_pairs={{0,1},{1,0},{2,3},{3,2},{4,5},{5,4},{6,7},{7,6},{8,9},{9,8},{10,11... | collective-permute-start | bytes 786440 | tf_op jit(solution)/shard_map/ppermute | solution.py:189
  (27 other events, 36.1 us)

commit v4 on v3

--- a/solution.py
+++ b/solution.py
@@ -413,26 +413,26 @@
     out_halves = [half_of(out_weight[l], out_half) for l in range(LAYERS)]
     second = tie(second, a_ring[0])
     out_halves = [tie(h, a_ring[0]) for h in out_halves]
-    docs = [tie(doc_ids, a_ring[0])]
-    docs = [shifted(docs[0], "sp", back) for back in range(depth, 0, -1)] + docs
+    flat = tie(flat_biases(rel_bias, rows), a_ring[0])
+    residual = tie(lax.dynamic_slice_in_dim(stream, t * cols, cols, 1), a_ring[0])
+    small = (flat, order, out_halves[0], residual)
     for step in range(1, count - 1):
-        source = tie(a_ring[-1], *a_group[-1:], *(docs if step > 1 else [second]))
+        source = tie(a_ring[-1], *a_group[-1:], *(small if step > 1 else [second]))
         a_group.append(swap_groups(a_ring[-1]))
         a_ring.append(ring_step(source, ring))
     last, base = a_ring[-1], a_group[-1]
+    docs = [tie(doc_ids, a_ring[1])]
+    docs = [shifted(docs[0], "sp", back) for back in range(depth, 0, -1)] + docs
     a_group.append(swap_groups(tie(last, base)))
     c_ring, c_group = [ring_step(tie(second, last, base), ring)], []
     o_ring, o_group = [ring_step(tie(out_halves[0], last, base), ring)], []
     doc_row = jnp.concatenate(docs)[None, :]
     doc_col = doc_ids[:, None]
-    flat = flat_biases(rel_bias, rows)
-
-    residual = tie(lax.dynamic_slice_in_dim(stream, t * cols, cols, 1), a_ring[0])
     x_pieces = [stream]
     weights = (query_weight, key_weight, value_weight)
     for layer in range(LAYERS):
         ring_pieces, group_pieces = (a_ring, a_group) if layer == 0 else (c_ring, c_group)
-        ahead = o_ring + c_ring[:1] if layer == 0 else o_ring
+        ahead = [*o_ring, c_ring[0], doc_row, doc_col] if layer == 0 else o_ring
         query, kv = project(
             x_pieces, norm_gain[layer], query_gain[layer][None], key_gain[layer][None],
             weights, layer, interleave(ring_pieces, group_pieces), tie(order, *ahead), count,

time: 181 us -> 179 us (0.989)
  local copies, waits for them, and re-layouts: 25 us -> 22.5 us
    ppermute x12, starting transfers between devices: 13.1 us -> 18.9 us  [ring_step(): lax.ppermute(value, 'sp', [(ring[i], ring[(i + 1) % count]) for i in rang...]
    ppermute x12, starting transfers between devices: 13.1 us -> 8.1 us  [swap_groups(): return lax.ppermute(value, 'grp', [(0, 1), (1, 0)])]
    ppermute x12, waiting for transfers between devices: 19.1 us -> 21.4 us  [swap_groups(): return lax.ppermute(value, 'grp', [(0, 1), (1, 0)])]
    unnamed x78 -> x64, local copies, waits for them, and re-layouts: 15.8 us -> 14.4 us
  transfers between devices with their start and end apart: 36 -> 36, of which waited for: 18 -> 21; matrix products, arithmetic and copies ran while one was open for 6% -> 5% of each run, Pallas kernels for 6% -> 6%
where the time goes in v4:
time: 179 us; the launch traced here: 176 us
  waiting for transfers between devices  61.8 us (35%)
  starting transfers between devices  41 us (23%)
  blocking collectives  29.4 us (16%)
  local copies, waits for them, and re-layouts  22.5 us (13%)
  Pallas kernels  18.6 us (10%)
  other arithmetic  2.08 us (1%)
    all_gather x2, blocking collectives, on_device_fast(): all_heads = lax.all_gather(attended, 'tp', axis=1, tiled=True)  29.4 us
    ppermute x12, waiting for transfers between devices, ring_step(): lax.ppermute(value, 'sp', [(ring[i], ring[(i + 1) % count]) for i in rang...  25.5 us
    ppermute x12, waiting for transfers between devices, swap_groups(): return lax.ppermute(value, 'grp', [(0, 1), (1, 0)])  21.4 us
    ppermute x12, starting transfers between devices, ring_step(): lax.ppermute(value, 'sp', [(ring[i], ring[(i + 1) % count]) for i in rang...  18.9 us
    pallas_call x7, Pallas kernels, call(): pl.pallas_call(kernel, grid=(1,), in_specs=[pl.BlockSpec(memory_space=SME...  18.6 us
    unnamed x64, local copies, waits for them, and re-layouts  14.4 us
    ppermute x6, waiting for transfers between devices, exchange_columns(): lax.ppermute(p, 'tp', pairs)  10.3 us
    ppermute x12, starting transfers between devices, swap_groups(): return lax.ppermute(value, 'grp', [(0, 1), (1, 0)])  8.1 us
  transfers between devices with their start and end apart: 36, of which 21 were waited for; matrix products, arithmetic and copies ran while one was open for 5% of the time, Pallas kernels for 6%

profile of v4, /device:TPU:25, one launch (start us, length us, event | category | flops | bytes accessed | tf_op | source)
XLA Modules:
  0.0 175.7 jit_solution(7571046979184946514)
XLA Ops:
  0.0 1.1 fusion.3
  6.9 1.7 constant_dynamic-slice_fusion.r_ref
  9.4 3.0 %collective-permute-done.refs_7_.refs_8_.refs_9_ = bf16[256,768]{1,0:T(8,128)(2,1)S(1)} collective-permute-done((bf16[256,768]{1,0:T(8,128)(2,1)S(1)}, bf16[256,768]{1,0:T(8,128)(2,1)S(1)}, u32[]{:S(2)}, u32[]{:S(2)}) %collective-permute-start) | collective-permute-done | bytes 393248 | tf_op jit(solution)/shard_map/ppermute | solution.py:173
  13.4 1.2 collective-permute-start.2
  16.0 5.6 %collective-permute-done.1.refs_13_.refs_14_.refs_15_ = bf16[256,768]{1,0:T(8,128)(2,1)S(1)} collective-permute-done((bf16[256,768]{1,0:T(8,128)(2,1)S(1)}, bf16[256,768]{1,0:T(8,128)(2,1)S(1)}, u32[]{:S(2)}, u32[]{:S(2)}) %collective-permute-start.1) | collective-permute-done | bytes 393248 | tf_op jit(solution)/shard_map/ppermute | solution.py:173
  23.0 1.2 collective-permute-start.4
  24.2 1.2 collective-permute-start.3
  25.4 5.6 %collective-permute-done.4.refs_16_.refs_17_.refs_18_ = bf16[256,768]{1,0:T(8,128)(2,1)S(1)} collective-permute-done((bf16[256,768]{1,0:T(8,128)(2,1)S(1)}, bf16[256,768]{1,0:T(8,128)(2,1)S(1)}, u32[]{:S(2)}, u32[]{:S(2)}) %collective-permute-start.4) | collective-permute-done | bytes 393248 | tf_op jit(solution)/shard_map/ppermute | solution.py:181
  32.0 2.4 %collective-permute-start.5 = (bf16[256,768]{1,0:T(8,128)(2,1)}, bf16[256,768]{1,0:T(8,128)(2,1)S(1)}, u32[]{:S(2)}, u32[]{:S(2)}) collective-permute-start(bf16[256,768]{1,0:T(8,128)(2,1)} %pad_maximum_fusion.1), channel_id=1, source_target_pairs={{0,8},{8,12},{12,4},{4,0},{1,9},{9,13},{13,5},{5,1},{2,10},{10,14}... | collective-permute-start | bytes 1179656 | tf_op jit(solution)/shard_map/ppermute | solution.py:173
  35.2 1.3 collective-permute-start.8
  36.5 1.3 collective-permute-start.7
  37.8 3.0 %collective-permute-start.6 = (bf16[128,512]{1,0:T(8,128)(2,1)S(1)}, bf16[128,512]{1,0:T(8,128)(2,1)S(1)}, u32[]{:S(2)}, u32[]{:S(2)}) collective-permute-start(bf16[128,512]{1,0:T(8,128)(2,1)S(1)} %get-tuple-element.49), channel_id=1, source_target_pairs={{0,8},{8,12},{12,4},{4,0},{1,9},{9,13},{13,5},{5,1},{2,10},{10,14}... | collective-permute-start | bytes 393224 | tf_op jit(solution)/shard_map/ppermute | solution.py:173
  42.3 1.8 %collective-permute-done.6.refs_0_ = bf16[128,512]{1,0:T(8,128)(2,1)S(1)} collective-permute-done((bf16[128,512]{1,0:T(8,128)(2,1)S(1)}, bf16[128,512]{1,0:T(8,128)(2,1)S(1)}, u32[]{:S(2)}, u32[]{:S(2)}) %collective-permute-start.6) | collective-permute-done | bytes 131104 | tf_op jit(solution)/shard_map/ppermute | solution.py:173
  45.7 2.9 %shard_map.118 = (bf16[256,256]{1,0:T(8,128)(2,1)S(1)}, bf16[256,512]{1,0:T(8,128)(2,1)S(1)}) custom-call(s32[6]{0:T(128)S(1)} %copy-done.18, bf16[256,2048]{1,0:T(8,128)(2,1)S(1)} %copy-done.6, f32[8,1,256]{2,1,0:T(1,128)S(1)} %bitcast.25, f32[1,64]{1,0:T(1,128)S(1)} %get-tuple-element.97.refs_2_, f32[1,64]{1,0:T(1,128)S(1)} %get-tuple-element.88.refs_3_, ...), custom_call_target="tpu_custom_call" | custom-call | tf_op jit(solution)/shard_map/pallas_call | solution.py:203
  49.3 1.3 collective-permute-start.10
  51.3 1.1 collective-permute-start.11
  52.4 2.7 %collective-permute-done.11.refs_1_ = bf16[128,512]{1,0:T(8,128)(2,1)S(1)} collective-permute-done((bf16[128,512]{1,0:T(8,128)(2,1)S(1)}, bf16[128,512]{1,0:T(8,128)(2,1)S(1)}, u32[]{:S(2)}, u32[]{:S(2)}) %collective-permute-start.11) | collective-permute-done | bytes 131104 | tf_op jit(solution)/shard_map/ppermute | solution.py:181
  55.7 2.0 %collective-permute-done.10.refs_1_ = bf16[256,512]{1,0:T(8,128)(2,1)S(1)} collective-permute-done((bf16[256,512]{1,0:T(8,128)(2,1)S(1)}, bf16[256,512]{1,0:T(8,128)(2,1)S(1)}, u32[]{:S(2)}, u32[]{:S(2)}) %collective-permute-start.10) | collective-permute-done | bytes 262176 | tf_op jit(solution)/shard_map/ppermute | solution.py:20
  57.7 1.3 collective-permute-start.12
  59.7 1.2 collective-permute-start.15
  61.0 3.3 %collective-permute-start.13 = (bf16[128,512]{1,0:T(8,128)(2,1)S(1)}, bf16[128,512]{1,0:T(8,128)(2,1)}, u32[]{:S(2)}, u32[]{:S(2)}) collective-permute-start(bf16[128,512]{1,0:T(8,128)(2,1)S(1)} %collective-permute-done.6.refs_0_), channel_id=1, source_target_pairs={{0,8},{8,12},{12,4},{4,0},{1,9},{9,13},{13,5},{5,1},{2,10},{10,14}... | collective-permute-start | bytes 393224 | tf_op jit(solution)/shard_map/ppermute | solution.py:173
  64.2 2.1 %collective-permute-done.13.refs_2_ = bf16[128,512]{1,0:T(8,128)(2,1)} collective-permute-done((bf16[128,512]{1,0:T(8,128)(2,1)S(1)}, bf16[128,512]{1,0:T(8,128)(2,1)}, u32[]{:S(2)}, u32[]{:S(2)}) %collective-permute-start.13) | collective-permute-done | bytes 131104 | tf_op jit(solution)/shard_map/ppermute | solution.py:173
  67.1 2.7 %collective-permute-start.14 = (bf16[256,768]{1,0:T(8,128)(2,1)S(1)}, bf16[256,768]{1,0:T(8,128)(2,1)S(1)}, u32[]{:S(2)}, u32[]{:S(2)}) collective-permute-start(bf16[256,768]{1,0:T(8,128)(2,1)S(1)} %collective-permute-done.5.refs_10_.refs_11_.refs_12_), channel_id=1, source_target_pairs={{0,8},{8,12},{12,4},{4,0},{1,9},{9,13},{13,5},{5,1},{2,10},{10,14}... | collective-permute-start | bytes 1179656 | tf_op jit(solution)/shard_map/ppermute | solution.py:173
  76.4 4.0 %shard_map.119 = bf16[256,256]{1,0:T(8,128)(2,1)S(1)} custom-call(s32[6]{0:T(128)S(1)} %copy-done.19, bf16[256,256]{1,0:T(8,128)(2,1)S(1)} %copy-done.17, bf16[256,512]{1,0:T(8,128)(2,1)S(1)} %copy-done.13, bf16[256,512]{1,0:T(8,128)(2,1)S(1)} %copy-done.11, bf16[256,512]{1,0:T(8,128)(2,1)S(1)} %copy-done.9, s32[256,1]{1,0:T(8,128)S(1)} %copy.13.refs_3_, ...), custom_call_target="tpu_custom_call" | custom-call | tf_op jit(solution)/shard_map/pallas_call | solution.py:203
  80.5 16.3 %all_gather.6.a_ref = bf16[256,1024]{1,0:T(8,128)(2,1)S(1)} all-gather(bf16[256,256]{1,0:T(8,128)(2,1)S(1)} %shard_map.119), channel_id=1, replica_groups=mesh['grp'=2,'sp'=4,'tp'=4] {'tp'}, dimensions={1}, use_global_device_ids=true | all-gather | bytes 655360 | tf_op jit(solution)/shard_map/all_gather | solution.py:460
  96.8 2.3 %collective-permute-start.18 = (bf16[256,768]{1,0:T(8,128)(2,1)S(1)}, bf16[256,768]{1,0:T(8,128)(2,1)S(1)}, u32[]{:S(2)}, u32[]{:S(2)}) collective-permute-start(bf16[256,768]{1,0:T(8,128)(2,1)S(1)} %collective-permute-done.14.refs_16_.refs_17_.refs_18_), channel_id=1, source_target_pairs={{0,8},{8,12},{12,4},{4,0},{1,9},{9,13},{13,5},{5,1},{2,10},{10,14}... | collective-permute-start | bytes 1179656 | tf_op jit(solution)/shard_map/ppermute | solution.py:173
  99.4 4.6 %collective-permute-done.20.refs_5_ = bf16[128,512]{1,0:T(8,128)(2,1)S(1)} collective-permute-done((bf16[128,512]{1,0:T(8,128)(2,1)}, bf16[128,512]{1,0:T(8,128)(2,1)S(1)}, u32[]{:S(2)}, u32[]{:S(2)}) %collective-permute-start.20) | collective-permute-done | bytes 131104 | tf_op jit(solution)/shard_map/ppermute | solution.py:181
  104.0 1.8 %shard_map.120.refs_0_.r_ref = bf16[256,512]{1,0:T(8,128)(2,1)S(1)} custom-call(s32[6]{0:T(128)S(1)} %copy-done.19, bf16[256,1024]{1,0:T(8,128)(2,1)S(1)} %all_gather.6.a_ref, bf16[256,512]{1,0:T(8,128)(2,1)S(1)} %copy-done.7, bf16[2,256,512]{2,1,0:T(8,128)(2,1)S(1)} %copy-done.3, bf16[128,512]{1,0:T(8,128)(2,1)S(1)} %collective-permute-done.6.refs_0_, ...), custom_call_target="tpu_custom_call" | custom-call | tf_op jit(solution)/shard_map/pallas_call | solution.py:203
  107.5 1.1 collective-permute-start.25
  108.6 1.5 collective-permute-start.21
  110.0 2.4 %collective-permute-done.22.refs_2_ = bf16[256,512]{1,0:T(8,128)(2,1)S(1)} collective-permute-done((bf16[256,512]{1,0:T(8,128)(2,1)S(1)}, bf16[256,512]{1,0:T(8,128)(2,1)S(1)}, u32[]{:S(2)}, u32[]{:S(2)}) %collective-permute-start.22) | collective-permute-done | bytes 262176 | tf_op jit(solution)/shard_map/ppermute | solution.py:189
  112.4 2.2 %collective-permute-start.23 = (bf16[256,512]{1,0:T(8,128)(2,1)S(1)}, bf16[256,512]{1,0:T(8,128)(2,1)S(1)}, u32[]{:S(2)}, u32[]{:S(2)}) collective-permute-start(bf16[256,512]{1,0:T(8,128)(2,1)S(1)} %collective-permute-done.22.refs_2_), channel_id=1, source_target_pairs={{0,1},{1,0},{2,3},{3,2},{4,5},{5,4},{6,7},{7,6},{8,9},{9,8},{10,11... | collective-permute-start | bytes 786440 | tf_op jit(solution)/shard_map/ppermute | solution.py:189
  115.0 4.7 %collective-permute-done.19.refs_0_ = bf16[128,512]{1,0:T(8,128)(2,1)S(1)} collective-permute-done((bf16[128,512]{1,0:T(8,128)(2,1)S(1)}, bf16[128,512]{1,0:T(8,128)(2,1)S(1)}, u32[]{:S(2)}, u32[]{:S(2)}) %collective-permute-start.19) | collective-permute-done | bytes 131104 | tf_op jit(solution)/shard_map/ppermute | solution.py:173
  119.7 4.3 %collective-permute-done.25.refs_25_.refs_26_.refs_27_ = bf16[256,768]{1,0:T(8,128)(2,1)S(1)} collective-permute-done((bf16[256,768]{1,0:T(8,128)(2,1)S(1)}, bf16[256,768]{1,0:T(8,128)(2,1)S(1)}, u32[]{:S(2)}, u32[]{:S(2)}) %collective-permute-start.25) | collective-permute-done | bytes 393248 | tf_op jit(solution)/shard_map/ppermute | solution.py:181
  124.6 2.9 %shard_map.121 = (bf16[256,256]{1,0:T(8,128)(2,1)S(1)}, bf16[256,512]{1,0:T(8,128)(2,1)S(1)}) custom-call(s32[6]{0:T(128)S(1)} %copy-done.19, bf16[256,512]{1,0:T(8,128)(2,1)S(1)} %shard_map.120.refs_0_.r_ref, bf16[256,512]{1,0:T(8,128)(2,1)S(1)} %collective-permute-done.21.refs_1_, bf16[256,512]{1,0:T(8,128)(2,1)S(1)} %collective-permute-done.22.refs_2_, ...), custom_call_target="tpu_custom_call" | custom-call | tf_op jit(solution)/shard_map/pallas_call | solution.py:203
  127.6 1.3 collective-permute-start.26
  129.2 3.6 %collective-permute-done.27.refs_1_ = bf16[128,512]{1,0:T(8,128)(2,1)S(1)} collective-permute-done((bf16[128,512]{1,0:T(8,128)(2,1)S(1)}, bf16[128,512]{1,0:T(8,128)(2,1)S(1)}, u32[]{:S(2)}, u32[]{:S(2)}) %collective-permute-start.27) | collective-permute-done | bytes 131104 | tf_op jit(solution)/shard_map/ppermute | solution.py:181
  132.7 2.2 %collective-permute-done.26.refs_1_ = bf16[256,512]{1,0:T(8,128)(2,1)S(1)} collective-permute-done((bf16[256,512]{1,0:T(8,128)(2,1)S(1)}, bf16[256,512]{1,0:T(8,128)(2,1)S(1)}, u32[]{:S(2)}, u32[]{:S(2)}) %collective-permute-start.26) | collective-permute-done | bytes 262176 | tf_op jit(solution)/shard_map/ppermute | solution.py:20
  135.0 1.3 collective-permute-start.29
  136.3 2.0 %collective-permute-start.28 = (bf16[128,512]{1,0:T(8,128)(2,1)S(1)}, bf16[128,512]{1,0:T(8,128)(2,1)S(1)}, u32[]{:S(2)}, u32[]{:S(2)}) collective-permute-start(bf16[128,512]{1,0:T(8,128)(2,1)S(1)} %collective-permute-done.19.refs_0_), channel_id=1, source_target_pairs={{0,8},{8,12},{12,4},{4,0},{1,9},{9,13},{13,5},{5,1},{2,10},{10,14}... | collective-permute-start | bytes 393224 | tf_op jit(solution)/shard_map/ppermute | solution.py:173
  138.3 6.0 %collective-permute-done.28.refs_2_ = bf16[128,512]{1,0:T(8,128)(2,1)S(1)} collective-permute-done((bf16[128,512]{1,0:T(8,128)(2,1)S(1)}, bf16[128,512]{1,0:T(8,128)(2,1)S(1)}, u32[]{:S(2)}, u32[]{:S(2)}) %collective-permute-start.28) | collective-permute-done | bytes 131104 | tf_op jit(solution)/shard_map/ppermute | solution.py:173
  144.5 4.0 %shard_map.122 = bf16[256,256]{1,0:T(8,128)(2,1)S(1)} custom-call(s32[6]{0:T(128)S(1)} %copy-done.19, bf16[256,256]{1,0:T(8,128)(2,1)S(1)} %get-tuple-element.72.q_ref, bf16[256,512]{1,0:T(8,128)(2,1)S(1)} %collective-permute-done.29.refs_0_, bf16[256,512]{1,0:T(8,128)(2,1)S(1)} %collective-permute-done.26.refs_1_, ...), custom_call_target="tpu_custom_call" | custom-call | tf_op jit(solution)/shard_map/pallas_call | solution.py:203
  149.8 13.0 %all_gather.7.a_ref = bf16[256,1024]{1,0:T(8,128)(2,1)S(1)} all-gather(bf16[256,256]{1,0:T(8,128)(2,1)S(1)} %shard_map.122), channel_id=1, replica_groups=mesh['grp'=2,'sp'=4,'tp'=4] {'tp'}, dimensions={1}, use_global_device_ids=true | all-gather | bytes 655360 | tf_op jit(solution)/shard_map/all_gather | solution.py:460
  162.9 1.3 shard_map.123.refs_0_
  165.3 6.7 %collective-permute-done.34.refs_2_ = bf16[256,512]{1,0:T(8,128)(2,1)S(1)} collective-permute-done((bf16[256,512]{1,0:T(8,128)(2,1)S(1)}, bf16[256,512]{1,0:T(8,128)(2,1)S(1)}, u32[]{:S(2)}, u32[]{:S(2)}) %collective-permute-start.34) | collective-permute-done | bytes 262176 | tf_op jit(solution)/shard_map/ppermute | solution.py:189
  172.0 1.0 collective-permute-start.35
  173.0 1.2 collective-permute-done.35.refs_3_
  174.1 1.6 shard_map.124
  (125 shorter events, 31.0 us)
Async XLA Ops:
  0.0 1.2 copy-start.1
  2.4 10.1 %collective-permute-start = (bf16[256,768]{1,0:T(8,128)(2,1)S(1)}, bf16[256,768]{1,0:T(8,128)(2,1)S(1)}, u32[]{:S(2)}, u32[]{:S(2)}) collective-permute-start(bf16[256,768]{1,0:T(8,128)(2,1)S(1)} %pad_maximum_fusion), channel_id=1, source_target_pairs={{0,8},{8,12},{12,4},{4,0},{1,9},{9,13},{13,5},{5,1},{2,10},{10,14}... | collective-permute-start | bytes 1179656 | tf_op jit(solution)/shard_map/ppermute | solution.py:173
  8.6 6.6 %copy-start.3 = (bf16[2,256,512]{2,1,0:T(8,128)(2,1)S(1)}, bf16[2,256,512]{2,1,0:T(8,128)(2,1)}, u32[]{:S(2)}) copy-start(bf16[2,256,512]{2,1,0:T(8,128)(2,1)} %own_ref.3) | copy-start | bytes 1572868
  12.4 9.1 %collective-permute-start.1 = (bf16[256,768]{1,0:T(8,128)(2,1)S(1)}, bf16[256,768]{1,0:T(8,128)(2,1)S(1)}, u32[]{:S(2)}, u32[]{:S(2)}) collective-permute-start(bf16[256,768]{1,0:T(8,128)(2,1)S(1)} %collective-permute-done.refs_7_.refs_8_.refs_9_), channel_id=1, source_target_pairs={{0,8},{8,12},{12,4},{4,0},{1,9},{9,13},{13,5},{5,1},{2,10},{10,14}... | collective-permute-start | bytes 1179656 | tf_op jit(solution)/shard_map/ppermute | solution.py:173
  13.4 8.9 %collective-permute-start.2 = (bf16[256,768]{1,0:T(8,128)(2,1)S(1)}, bf16[256,768]{1,0:T(8,128)(2,1)S(1)}, u32[]{:S(2)}, u32[]{:S(2)}) collective-permute-start(bf16[256,768]{1,0:T(8,128)(2,1)S(1)} %collective-permute-done.refs_7_.refs_8_.refs_9_), channel_id=1, source_target_pairs={{0,16},{16,0},{1,17},{17,1},{2,18},{18,2},{3,19},{19,3},{4,20},{20... | collective-permute-start | bytes 1179656 | tf_op jit(solution)/shard_map/ppermute | solution.py:181
  15.2 19.3 %copy-start.26 = (f32[2,2048]{1,0:T(2,128)S(1)}, f32[2,2048]{1,0:T(2,128)}, u32[]{:S(2)}) copy-start(f32[2,2048]{1,0:T(2,128)} %param.14) | copy-start | bytes 49156
  15.3 28.9 %copy-start.6 = (bf16[256,2048]{1,0:T(8,128)(2,1)S(1)}, bf16[256,2048]{1,0:T(8,128)(2,1)}, u32[]{:S(2)}) copy-start(bf16[256,2048]{1,0:T(8,128)(2,1)} %refs_0_.1) | copy-start | bytes 3145732
  15.3 28.8 %copy-start = (bf16[2,512,256]{2,1,0:T(8,128)(2,1)S(1)}, bf16[2,512,256]{2,1,0:T(8,128)(2,1)}, u32[]{:S(2)}) copy-start(bf16[2,512,256]{2,1,0:T(8,128)(2,1)} %refs_7_.1) | copy-start | bytes 1572868
  16.0 19.2 %copy-start.28 = (s32[256]{0:T(256)S(1)}, s32[256]{0:T(256)}, u32[]{:S(2)}) copy-start(s32[256]{0:T(256)} %param.13) | copy-start | bytes 3076
  16.0 24.8 %copy-start.29 = (f32[2,64]{1,0:T(2,128)S(1)}, f32[2,64]{1,0:T(2,128)}, u32[]{:S(2)}) copy-start(f32[2,64]{1,0:T(2,128)} %param.20) | copy-start | bytes 1540
  16.0 24.8 %copy-start.30 = (f32[2,64]{1,0:T(2,128)S(1)}, f32[2,64]{1,0:T(2,128)}, u32[]{:S(2)}) copy-start(f32[2,64]{1,0:T(2,128)} %param.19) | copy-start | bytes 1540
  23.0 8.0 %collective-permute-start.4 = (bf16[256,768]{1,0:T(8,128)(2,1)S(1)}, bf16[256,768]{1,0:T(8,128)(2,1)S(1)}, u32[]{:S(2)}, u32[]{:S(2)}) collective-permute-start(bf16[256,768]{1,0:T(8,128)(2,1)S(1)} %collective-permute-done.1.refs_13_.refs_14_.refs_15_), channel_id=1, source_target_pairs={{0,16},{16,0},{1,17},{17,1},{2,18},{18,2},{3,19},{19,3},{4,20},{20... | collective-permute-start | bytes 1179656 | tf_op jit(solution)/shard_map/ppermute | solution.py:181
  24.2 7.7 %collective-permute-start.3 = (bf16[256,768]{1,0:T(8,128)(2,1)S(1)}, bf16[256,768]{1,0:T(8,128)(2,1)S(1)}, u32[]{:S(2)}, u32[]{:S(2)}) collective-permute-start(bf16[256,768]{1,0:T(8,128)(2,1)S(1)} %collective-permute-done.1.refs_13_.refs_14_.refs_15_), channel_id=1, source_target_pairs={{0,8},{8,12},{12,4},{4,0},{1,9},{9,13},{13,5},{5,1},{2,10},{10,14}... | collective-permute-start | bytes 1179656 | tf_op jit(solution)/shard_map/ppermute | solution.py:173
  32.0 12.1 %collective-permute-start.5 = (bf16[256,768]{1,0:T(8,128)(2,1)}, bf16[256,768]{1,0:T(8,128)(2,1)S(1)}, u32[]{:S(2)}, u32[]{:S(2)}) collective-permute-start(bf16[256,768]{1,0:T(8,128)(2,1)} %pad_maximum_fusion.1), channel_id=1, source_target_pairs={{0,8},{8,12},{12,4},{4,0},{1,9},{9,13},{13,5},{5,1},{2,10},{10,14}... | collective-permute-start | bytes 1179656 | tf_op jit(solution)/shard_map/ppermute | solution.py:173
  34.3 9.8 %collective-permute-start.9 = (bf16[256,768]{1,0:T(8,128)(2,1)S(1)}, bf16[256,768]{1,0:T(8,128)(2,1)S(1)}, u32[]{:S(2)}, u32[]{:S(2)}) collective-permute-start(bf16[256,768]{1,0:T(8,128)(2,1)S(1)} %collective-permute-done.3.refs_19_.refs_20_.refs_21_), channel_id=1, source_target_pairs={{0,16},{16,0},{1,17},{17,1},{2,18},{18,2},{3,19},{19,3},{4,20},{20... | collective-permute-start | bytes 1179656 | tf_op jit(solution)/shard_map/ppermute | solution.py:181
  35.2 6.2 %collective-permute-start.8 = (s32[256]{0:T(256)S(1)}, s32[256]{0:T(256)S(1)}, u32[]{:S(2)}, u32[]{:S(2)}) collective-permute-start(s32[256]{0:T(256)S(1)} %copy-done.28), channel_id=1, source_target_pairs={{0,4},{4,8},{8,12},{1,5},{5,9},{9,13},{2,6},{6,10},{10,14},{3,7},{... | collective-permute-start | bytes 3080 | tf_op jit(solution)/shard_map/ppermute | solution.py:20
  36.5 5.3 %collective-permute-start.7 = (s32[256]{0:T(256)S(1)}, s32[256]{0:T(256)S(1)}, u32[]{:S(2)}, u32[]{:S(2)}) collective-permute-start(s32[256]{0:T(256)S(1)} %copy-done.28), channel_id=1, source_target_pairs={{0,8},{4,12},{1,9},{5,13},{2,10},{6,14},{3,11},{7,15},{16,24},{20,... | collective-permute-start | bytes 3080 | tf_op jit(solution)/shard_map/ppermute | solution.py:20
  37.8 6.3 %collective-permute-start.6 = (bf16[128,512]{1,0:T(8,128)(2,1)S(1)}, bf16[128,512]{1,0:T(8,128)(2,1)S(1)}, u32[]{:S(2)}, u32[]{:S(2)}) collective-permute-start(bf16[128,512]{1,0:T(8,128)(2,1)S(1)} %get-tuple-element.49), channel_id=1, source_target_pairs={{0,8},{8,12},{12,4},{4,0},{1,9},{9,13},{13,5},{5,1},{2,10},{10,14}... | collective-permute-start | bytes 393224 | tf_op jit(solution)/shard_map/ppermute | solution.py:173
  49.3 8.5 %collective-permute-start.10 = (bf16[256,512]{1,0:T(8,128)(2,1)S(1)}, bf16[256,512]{1,0:T(8,128)(2,1)S(1)}, u32[]{:S(2)}, u32[]{:S(2)}) collective-permute-start(bf16[256,512]{1,0:T(8,128)(2,1)S(1)} %get-tuple-element.53.refs_2_), channel_id=1, source_target_pairs={{0,4},{4,8},{8,12},{1,5},{5,9},{9,13},{2,6},{6,10},{10,14},{3,7},{... | collective-permute-start | bytes 786440 | tf_op jit(solution)/shard_map/ppermute | solution.py:20
  51.3 3.8 %collective-permute-start.11 = (bf16[128,512]{1,0:T(8,128)(2,1)S(1)}, bf16[128,512]{1,0:T(8,128)(2,1)S(1)}, u32[]{:S(2)}, u32[]{:S(2)}) collective-permute-start(bf16[128,512]{1,0:T(8,128)(2,1)S(1)} %collective-permute-done.6.refs_0_), channel_id=1, source_target_pairs={{0,16},{16,0},{1,17},{17,1},{2,18},{18,2},{3,19},{19,3},{4,20},{20... | collective-permute-start | bytes 393224 | tf_op jit(solution)/shard_map/ppermute | solution.py:181
  57.7 8.6 %collective-permute-start.12 = (bf16[256,512]{1,0:T(8,128)(2,1)S(1)}, bf16[256,512]{1,0:T(8,128)(2,1)S(1)}, u32[]{:S(2)}, u32[]{:S(2)}) collective-permute-start(bf16[256,512]{1,0:T(8,128)(2,1)S(1)} %collective-permute-done.10.refs_1_), channel_id=1, source_target_pairs={{0,4},{4,8},{8,12},{1,5},{5,9},{9,13},{2,6},{6,10},{10,14},{3,7},{... | collective-permute-start | bytes 786440 | tf_op jit(solution)/shard_map/ppermute | solution.py:20
  59.7 11.6 %collective-permute-start.15 = (bf16[256,768]{1,0:T(8,128)(2,1)S(1)}, bf16[256,768]{1,0:T(8,128)(2,1)S(1)}, u32[]{:S(2)}, u32[]{:S(2)}) collective-permute-start(bf16[256,768]{1,0:T(8,128)(2,1)S(1)} %collective-permute-done.5.refs_10_.refs_11_.refs_12_), channel_id=1, source_target_pairs={{0,16},{16,0},{1,17},{17,1},{2,18},{18,2},{3,19},{19,3},{4,20},{20... | collective-permute-start | bytes 1179656 | tf_op jit(solution)/shard_map/ppermute | solution.py:181
  61.0 5.4 %collective-permute-start.13 = (bf16[128,512]{1,0:T(8,128)(2,1)S(1)}, bf16[128,512]{1,0:T(8,128)(2,1)}, u32[]{:S(2)}, u32[]{:S(2)}) collective-permute-start(bf16[128,512]{1,0:T(8,128)(2,1)S(1)} %collective-permute-done.6.refs_0_), channel_id=1, source_target_pairs={{0,8},{8,12},{12,4},{4,0},{1,9},{9,13},{13,5},{5,1},{2,10},{10,14}... | collective-permute-start | bytes 393224 | tf_op jit(solution)/shard_map/ppermute | solution.py:173
  67.1 29.8 %collective-permute-start.14 = (bf16[256,768]{1,0:T(8,128)(2,1)S(1)}, bf16[256,768]{1,0:T(8,128)(2,1)S(1)}, u32[]{:S(2)}, u32[]{:S(2)}) collective-permute-start(bf16[256,768]{1,0:T(8,128)(2,1)S(1)} %collective-permute-done.5.refs_10_.refs_11_.refs_12_), channel_id=1, source_target_pairs={{0,8},{8,12},{12,4},{4,0},{1,9},{9,13},{13,5},{5,1},{2,10},{10,14}... | collective-permute-start | bytes 1179656 | tf_op jit(solution)/shard_map/ppermute | solution.py:173
  69.8 10.7 %collective-permute-start.17 = (bf16[128,512]{1,0:T(8,128)(2,1)}, bf16[128,512]{1,0:T(8,128)(2,1)}, u32[]{:S(2)}, u32[]{:S(2)}) collective-permute-start(bf16[128,512]{1,0:T(8,128)(2,1)} %collective-permute-done.13.refs_2_), channel_id=1, source_target_pairs={{0,16},{16,0},{1,17},{17,1},{2,18},{18,2},{3,19},{19,3},{4,20},{20... | collective-permute-start | bytes 393224 | tf_op jit(solution)/shard_map/ppermute | solution.py:181
  70.0 10.5 %collective-permute-start.16 = (bf16[128,512]{1,0:T(8,128)(2,1)}, bf16[128,512]{1,0:T(8,128)(2,1)}, u32[]{:S(2)}, u32[]{:S(2)}) collective-permute-start(bf16[128,512]{1,0:T(8,128)(2,1)} %collective-permute-done.13.refs_2_), channel_id=1, source_target_pairs={{0,8},{8,12},{12,4},{4,0},{1,9},{9,13},{13,5},{5,1},{2,10},{10,14}... | collective-permute-start | bytes 393224 | tf_op jit(solution)/shard_map/ppermute | solution.py:173
  80.4 23.6 %copy-start.7 = (bf16[256,512]{1,0:T(8,128)(2,1)S(1)}, bf16[256,512]{1,0:T(8,128)(2,1)}, u32[]{:S(2)}) copy-start(bf16[256,512]{1,0:T(8,128)(2,1)} %constant_dynamic-slice_fusion.r_ref) | copy-start | bytes 786436
  80.5 23.5 %copy-start.15 = (bf16[128,512]{1,0:T(8,128)(2,1)S(1)}, bf16[128,512]{1,0:T(8,128)(2,1)}, u32[]{:S(2)}) copy-start(bf16[128,512]{1,0:T(8,128)(2,1)} %copy-done.14) | copy-start | bytes 393220
  96.8 17.8 %copy-start.25 = (bf16[128,512]{1,0:T(8,128)(2,1)S(1)}, bf16[128,512]{1,0:T(8,128)(2,1)}, u32[]{:S(2)}) copy-start(bf16[128,512]{1,0:T(8,128)(2,1)} %get-tuple-element.64) | copy-start | bytes 393220
  96.8 10.7 %collective-permute-start.18 = (bf16[256,768]{1,0:T(8,128)(2,1)S(1)}, bf16[256,768]{1,0:T(8,128)(2,1)S(1)}, u32[]{:S(2)}, u32[]{:S(2)}) collective-permute-start(bf16[256,768]{1,0:T(8,128)(2,1)S(1)} %collective-permute-done.14.refs_16_.refs_17_.refs_18_), channel_id=1, source_target_pairs={{0,8},{8,12},{12,4},{4,0},{1,9},{9,13},{13,5},{5,1},{2,10},{10,14}... | collective-permute-start | bytes 1179656 | tf_op jit(solution)/shard_map/ppermute | solution.py:173
  99.2 4.8 %collective-permute-start.20 = (bf16[128,512]{1,0:T(8,128)(2,1)}, bf16[128,512]{1,0:T(8,128)(2,1)S(1)}, u32[]{:S(2)}, u32[]{:S(2)}) collective-permute-start(bf16[128,512]{1,0:T(8,128)(2,1)} %collective-permute-done.16.refs_4_), channel_id=1, source_target_pairs={{0,16},{16,0},{1,17},{17,1},{2,18},{18,2},{3,19},{19,3},{4,20},{20... | collective-permute-start | bytes 393224 | tf_op jit(solution)/shard_map/ppermute | solution.py:181
  105.8 18.1 %copy-start.20 = (f32[1,2048]{1,0:T(1,128)S(1)}, f32[1,2048]{1,0:T(1,128)}, u32[]{:S(2)}) copy-start(f32[1,2048]{1,0:T(1,128)} %get-tuple-element.85) | copy-start | bytes 24580
  105.8 6.6 %collective-permute-start.22 = (bf16[256,512]{1,0:T(8,128)(2,1)S(1)}, bf16[256,512]{1,0:T(8,128)(2,1)S(1)}, u32[]{:S(2)}, u32[]{:S(2)}) collective-permute-start(bf16[256,512]{1,0:T(8,128)(2,1)S(1)} %shard_map.120.refs_0_.r_ref), channel_id=1, source_target_pairs={{0,2},{1,3},{2,0},{3,1},{4,6},{5,7},{6,4},{7,5},{8,10},{9,11},{10,... | collective-permute-start | bytes 786440 | tf_op jit(solution)/shard_map/ppermute | solution.py:189
  106.4 13.2 %collective-permute-start.24 = (bf16[256,768]{1,0:T(8,128)(2,1)S(1)}, bf16[256,768]{1,0:T(8,128)(2,1)S(1)}, u32[]{:S(2)}, u32[]{:S(2)}) collective-permute-start(bf16[256,768]{1,0:T(8,128)(2,1)S(1)} %collective-permute-done.14.refs_16_.refs_17_.refs_18_), channel_id=1, source_target_pairs={{0,16},{16,0},{1,17},{17,1},{2,18},{18,2},{3,19},{19,3},{4,20},{20... | collective-permute-start | bytes 1179656 | tf_op jit(solution)/shard_map/ppermute | solution.py:181
  107.5 16.5 %collective-permute-start.25 = (bf16[256,768]{1,0:T(8,128)(2,1)S(1)}, bf16[256,768]{1,0:T(8,128)(2,1)S(1)}, u32[]{:S(2)}, u32[]{:S(2)}) collective-permute-start(bf16[256,768]{1,0:T(8,128)(2,1)S(1)} %collective-permute-done.18.refs_22_.refs_23_.refs_24_), channel_id=1, source_target_pairs={{0,16},{16,0},{1,17},{17,1},{2,18},{18,2},{3,19},{19,3},{4,20},{20... | collective-permute-start | bytes 1179656 | tf_op jit(solution)/shard_map/ppermute | solution.py:181
  108.6 11.1 %collective-permute-start.21 = (bf16[256,512]{1,0:T(8,128)(2,1)S(1)}, bf16[256,512]{1,0:T(8,128)(2,1)S(1)}, u32[]{:S(2)}, u32[]{:S(2)}) collective-permute-start(bf16[256,512]{1,0:T(8,128)(2,1)S(1)} %shard_map.120.refs_0_.r_ref), channel_id=1, source_target_pairs={{0,1},{1,0},{2,3},{3,2},{4,5},{5,4},{6,7},{7,6},{8,9},{9,8},{10,11... | collective-permute-start | bytes 786440 | tf_op jit(solution)/shard_map/ppermute | solution.py:189
  112.4 7.2 %collective-permute-start.23 = (bf16[256,512]{1,0:T(8,128)(2,1)S(1)}, bf16[256,512]{1,0:T(8,128)(2,1)S(1)}, u32[]{:S(2)}, u32[]{:S(2)}) collective-permute-start(bf16[256,512]{1,0:T(8,128)(2,1)S(1)} %collective-permute-done.22.refs_2_), channel_id=1, source_target_pairs={{0,1},{1,0},{2,3},{3,2},{4,5},{5,4},{6,7},{7,6},{8,9},{9,8},{10,11... | collective-permute-start | bytes 786440 | tf_op jit(solution)/shard_map/ppermute | solution.py:189
  114.6 5.1 %collective-permute-start.19 = (bf16[128,512]{1,0:T(8,128)(2,1)S(1)}, bf16[128,512]{1,0:T(8,128)(2,1)S(1)}, u32[]{:S(2)}, u32[]{:S(2)}) collective-permute-start(bf16[128,512]{1,0:T(8,128)(2,1)S(1)} %copy-done.25), channel_id=1, source_target_pairs={{0,8},{8,12},{12,4},{4,0},{1,9},{9,13},{13,5},{5,1},{2,10},{10,14}... | collective-permute-start | bytes 393224 | tf_op jit(solution)/shard_map/ppermute | solution.py:173
  127.6 7.4 %collective-permute-start.26 = (bf16[256,512]{1,0:T(8,128)(2,1)S(1)}, bf16[256,512]{1,0:T(8,128)(2,1)S(1)}, u32[]{:S(2)}, u32[]{:S(2)}) collective-permute-start(bf16[256,512]{1,0:T(8,128)(2,1)S(1)} %get-tuple-element.68.refs_2_), channel_id=1, source_target_pairs={{0,4},{4,8},{8,12},{1,5},{5,9},{9,13},{2,6},{6,10},{10,14},{3,7},{... | collective-permute-start | bytes 786440 | tf_op jit(solution)/shard_map/ppermute | solution.py:20
  128.9 3.9 %collective-permute-start.27 = (bf16[128,512]{1,0:T(8,128)(2,1)S(1)}, bf16[128,512]{1,0:T(8,128)(2,1)S(1)}, u32[]{:S(2)}, u32[]{:S(2)}) collective-permute-start(bf16[128,512]{1,0:T(8,128)(2,1)S(1)} %collective-permute-done.19.refs_0_), channel_id=1, source_target_pairs={{0,16},{16,0},{1,17},{17,1},{2,18},{18,2},{3,19},{19,3},{4,20},{20... | collective-permute-start | bytes 393224 | tf_op jit(solution)/shard_map/ppermute | solution.py:181
  135.0 9.3 %collective-permute-start.29 = (bf16[256,512]{1,0:T(8,128)(2,1)S(1)}, bf16[256,512]{1,0:T(8,128)(2,1)S(1)}, u32[]{:S(2)}, u32[]{:S(2)}) collective-permute-start(bf16[256,512]{1,0:T(8,128)(2,1)S(1)} %collective-permute-done.26.refs_1_), channel_id=1, source_target_pairs={{0,4},{4,8},{8,12},{1,5},{5,9},{9,13},{2,6},{6,10},{10,14},{3,7},{... | collective-permute-start | bytes 786440 | tf_op jit(solution)/shard_map/ppermute | solution.py:20
  136.3 8.0 %collective-permute-start.28 = (bf16[128,512]{1,0:T(8,128)(2,1)S(1)}, bf16[128,512]{1,0:T(8,128)(2,1)S(1)}, u32[]{:S(2)}, u32[]{:S(2)}) collective-permute-start(bf16[128,512]{1,0:T(8,128)(2,1)S(1)} %collective-permute-done.19.refs_0_), channel_id=1, source_target_pairs={{0,8},{8,12},{12,4},{4,0},{1,9},{9,13},{13,5},{5,1},{2,10},{10,14}... | collective-permute-start | bytes 393224 | tf_op jit(solution)/shard_map/ppermute | solution.py:173
  144.2 4.3 %collective-permute-start.31 = (bf16[128,512]{1,0:T(8,128)(2,1)S(1)}, bf16[128,512]{1,0:T(8,128)(2,1)S(1)}, u32[]{:S(2)}, u32[]{:S(2)}) collective-permute-start(bf16[128,512]{1,0:T(8,128)(2,1)S(1)} %collective-permute-done.28.refs_2_), channel_id=1, source_target_pairs={{0,16},{16,0},{1,17},{17,1},{2,18},{18,2},{3,19},{19,3},{4,20},{20... | collective-permute-start | bytes 393224 | tf_op jit(solution)/shard_map/ppermute | solution.py:181
  144.5 4.6 %collective-permute-start.30 = (bf16[128,512]{1,0:T(8,128)(2,1)S(1)}, bf16[128,512]{1,0:T(8,128)(2,1)S(1)}, u32[]{:S(2)}, u32[]{:S(2)}) collective-permute-start(bf16[128,512]{1,0:T(8,128)(2,1)S(1)} %collective-permute-done.28.refs_2_), channel_id=1, source_target_pairs={{0,8},{8,12},{12,4},{4,0},{1,9},{9,13},{13,5},{5,1},{2,10},{10,14}... | collective-permute-start | bytes 393224 | tf_op jit(solution)/shard_map/ppermute | solution.py:173
  149.1 13.8 %collective-permute-start.32 = (bf16[128,512]{1,0:T(8,128)(2,1)S(1)}, bf16[128,512]{1,0:T(8,128)(2,1)S(1)}, u32[]{:S(2)}, u32[]{:S(2)}) collective-permute-start(bf16[128,512]{1,0:T(8,128)(2,1)S(1)} %collective-permute-done.30.refs_4_), channel_id=1, source_target_pairs={{0,16},{16,0},{1,17},{17,1},{2,18},{18,2},{3,19},{19,3},{4,20},{20... | collective-permute-start | bytes 393224 | tf_op jit(solution)/shard_map/ppermute | solution.py:181
  164.2 7.8 %collective-permute-start.34 = (bf16[256,512]{1,0:T(8,128)(2,1)S(1)}, bf16[256,512]{1,0:T(8,128)(2,1)S(1)}, u32[]{:S(2)}, u32[]{:S(2)}) collective-permute-start(bf16[256,512]{1,0:T(8,128)(2,1)S(1)} %shard_map.123.refs_0_), channel_id=1, source_target_pairs={{0,2},{1,3},{2,0},{3,1},{4,6},{5,7},{6,4},{7,5},{8,10},{9,11},{10,... | collective-permute-start | bytes 786440 | tf_op jit(solution)/shard_map/ppermute | solution.py:189
  164.8 8.2 %collective-permute-start.33 = (bf16[256,512]{1,0:T(8,128)(2,1)S(1)}, bf16[256,512]{1,0:T(8,128)(2,1)S(1)}, u32[]{:S(2)}, u32[]{:S(2)}) collective-permute-start(bf16[256,512]{1,0:T(8,128)(2,1)S(1)} %shard_map.123.refs_0_), channel_id=1, source_target_pairs={{0,1},{1,0},{2,3},{3,2},{4,5},{5,4},{6,7},{7,6},{8,9},{9,8},{10,11... | collective-permute-start | bytes 786440 | tf_op jit(solution)/shard_map/ppermute | solution.py:189
  172.0 2.2 %collective-permute-start.35 = (bf16[256,512]{1,0:T(8,128)(2,1)S(1)}, bf16[256,512]{1,0:T(8,128)(2,1)S(1)}, u32[]{:S(2)}, u32[]{:S(2)}) collective-permute-start(bf16[256,512]{1,0:T(8,128)(2,1)S(1)} %collective-permute-done.34.refs_2_), channel_id=1, source_target_pairs={{0,1},{1,0},{2,3},{3,2},{4,5},{5,4},{6,7},{7,6},{8,9},{9,8},{10,11... | collective-permute-start | bytes 786440 | tf_op jit(solution)/shard_map/ppermute | solution.py:189
  (20 other events, 15.1 us)
